TPU v7x, 1024 devices: a whole 4x8x16 slice. The times are simulated.
1024 devices in a mesh: sp: 128 (over z, y), tp: 8 (over x, core).
Axes of the slice: x: 4, y: 8, z: 16, core: 2. Of those that a mesh axis runs over, the one named last changes fastest.
Arguments:
- tokens: bfloat16 [16384, 2048], P('sp', 'tp'), may hold values from -28 to 28
- norm_gain: bfloat16 [1, 2048], P(None, 'tp'), may hold values from 0.099609375 to 1.8984375
- conv_b_w: bfloat16 [2048, 1024], P(None, 'tp'), may hold values from -0.125 to 0.125
- conv_c_w: bfloat16 [2048, 1024], P(None, 'tp'), may hold values from -0.125 to 0.125
- conv_u_w: bfloat16 [2048, 1024], P(None, 'tp'), may hold values from -0.125 to 0.125
- conv_taps: bfloat16 [3, 1024], P(None, 'tp'), may hold values from -3.5 to 3.5
- query_w: bfloat16 [2048, 2048], P(None, 'tp'), may hold values from -0.125 to 0.125
- key_w: bfloat16 [2048, 2048], P(None, 'tp'), may hold values from -0.125 to 0.125
- value_w: bfloat16 [2048, 2048], P(None, 'tp'), may hold values from -0.125 to 0.125
- outgate_w: bfloat16 [2048, 2048], P(None, 'tp'), may hold values from -0.125 to 0.125
- gate_w: bfloat16 [2048, 2, 8], P(None, None, 'tp'), may hold values from -0.125 to 0.125
- gate_bias: float32 [2, 8], P(None, 'tp'), may hold values from -5 to 150
- mem_gain: bfloat16 [2048], P('tp'), may hold values from 0.099609375 to 1.8984375
- conv_out_w: bfloat16 [1024, 2048], P('tp'), may hold values from -0.1875 to 0.1875
- mem_out_w: bfloat16 [2048, 2048], P('tp'), may hold values from -0.125 to 0.125
Outputs:
- layer_out: bfloat16 [16384, 2048], P(('sp', 'tp'))
All inputs are finite; a program needn't handle non-finite values.
Results may differ from a plain program's by a relative error of at most 0.014.
The roundings to bfloat16 on the way count: a program that leaves them out, or rounds other values in their place, can miss the bound.
Values may be sent and summed in bfloat16 or wider, within the bound.
No kernel may reach another device: no remote copies, remote signals or barrier semaphores. Data moves between devices by JAX's collectives and lax.ppermute only.
A program may use at most 64 MiB of HBM per device.

v0:
```python
import jax
import jax.numpy as jnp
from jax import lax
from jax.sharding import Mesh
from jax.sharding import PartitionSpec as P

HEAD_DIM = 256
BLOCK = 128
MDIM = 2048
SP = ("sp_0", "sp_1")
SP_TP = ("sp_0", "sp_1", "tp")


EPS = 1e-06
LOWEST = -1e30
HIGH = lax.Precision.HIGHEST


def in_one_piece(arrays, axis, dim, along):
    ends, at = ([], 0)
    for a in arrays[:-1]:
        at += a.shape[along]
        ends.append(at)
    both = jnp.concatenate(arrays, axis=along)
    return tuple(jnp.split(lax.all_gather(both, axis, axis=dim, tiled=True), ends, axis=along))


def shifted(value, axis, by):
    count = lax.axis_size(axis)
    pairs = [(i, i + by) for i in range(count) if 0 <= i + by < count]
    return lax.ppermute(value, axis, pairs)


def neutral_like(value, identity):
    return jax.tree.map(
        lambda a, e: jnp.broadcast_to(jnp.asarray(e, a.dtype), a.shape), value, identity
    )


def all_in_one(value, axis):
    leaves = jax.tree.leaves(value)
    order = sorted(range(len(leaves)), key=lambda k: -leaves[k].size)
    width = (1, *leaves[order[0]].shape)[-1]
    lines = [
        jnp.pad(leaves[k].reshape(-1), (0, -leaves[k].size % width)).reshape(-1, width)
        for k in order
    ]
    both, at, found = (lax.all_gather(jnp.concatenate(lines), axis), 0, {})
    for k, line in zip(order, lines):
        piece = both[:, at : at + len(line)].reshape(len(both), -1)
        found[k] = piece[:, : leaves[k].size].reshape(-1, *leaves[k].shape)
        at += len(line)
    numbers = iter(range(len(leaves)))
    return jax.tree.map(lambda _: found[next(numbers)], value)


def carried_in(value, axes, combine, identity):
    before = start = neutral_like(value, identity)
    total = value
    for axis in reversed(axes):
        count, position = (lax.axis_size(axis), lax.axis_index(axis))
        pieces = all_in_one(total, axis)
        inside, total = (start, start)
        for k in range(count):
            passed = k < position
            total = combine(total, jax.tree.map(lambda part: part[k], pieces))
            inside = jax.tree.map(lambda new, old: jnp.where(passed, new, old), total, inside)
        before = combine(inside, before)
    return before


def from_everyone(value, axis):
    copies = jnp.broadcast_to(value, (lax.axis_size(axis), *value.shape))
    return lax.all_to_all(copies, axis, split_axis=0, concat_axis=0, tiled=True)


def taken_together(value, axis):
    everything = from_everyone(value, axis)
    return jnp.sum(everything, axis=0)


def cut_along(value, dim, count):
    before, after = (value.shape[:dim], value.shape[dim + 1 :])
    return jnp.moveaxis(value.reshape(*before, count, -1, *after), dim, 0)


def sent_and_summed(value, axis, dim):
    parts = cut_along(value, dim, lax.axis_size(axis))
    arrived = lax.all_to_all(parts, axis, split_axis=0, concat_axis=0, tiled=True)
    return arrived.astype(jnp.float32).sum(axis=0)


def local_pass(queries, keys, values, input_pre, log_forget):
    count, width = queries.shape
    blocks = count // BLOCK

    def step(carry, inputs):
        memory, normer, stabil, decay_sum = carry
        query_block, key_block, value_block, input_gate, forget_block = inputs
        causal = jnp.tril(jnp.ones((BLOCK, BLOCK), dtype=bool))
        running = jnp.cumsum(forget_block)
        decays = jnp.where(
            causal, running[:, None] - running[None, :] + input_gate[None, :], -jnp.inf
        )
        inter = running + stabil
        row_max = jnp.maximum(inter, jnp.max(decays, axis=1))
        weights = jnp.exp(decays - row_max[:, None])
        scores = jnp.dot(query_block, key_block.T, precision=HIGH) * weights
        carried = jnp.exp(inter - row_max)
        numer_part = carried[:, None] * jnp.dot(query_block, memory, precision=HIGH) + jnp.dot(
            scores, value_block, precision=HIGH
        )
        denom_part = carried * jnp.dot(query_block, normer, precision=HIGH) + jnp.sum(
            scores, axis=1
        )
        new_stabil = row_max[-1]
        key_weight = jnp.exp(running[-1] - running + input_gate - new_stabil)
        fade = jnp.exp(running[-1] + stabil - new_stabil)
        memory = fade * memory + jnp.dot(
            (key_weight[:, None] * key_block).T, value_block, precision=HIGH
        )
        normer = fade * normer + jnp.dot(key_weight, key_block, precision=HIGH)
        outputs = (numer_part, denom_part, row_max, decay_sum + running)
        return ((memory, normer, new_stabil, decay_sum + running[-1]), outputs)

    inputs = (
        queries.reshape(blocks, BLOCK, width),
        keys.reshape(blocks, BLOCK, width),
        values.reshape(blocks, BLOCK, width),
        input_pre.reshape(blocks, BLOCK),
        log_forget.reshape(blocks, BLOCK),
    )
    start = (
        jnp.zeros((width, width), jnp.float32),
        jnp.zeros((width,), jnp.float32),
        jnp.zeros((), jnp.float32),
        jnp.zeros((), jnp.float32),
    )
    final, rows = lax.scan(step, start, inputs)
    memory, normer, stabil, decay_sum = final
    numer_rows, denom_rows, row_max, row_decay = rows
    return (
        numer_rows.reshape(count, width),
        denom_rows.reshape(count),
        row_max.reshape(count),
        row_decay.reshape(count),
        decay_sum,
        stabil,
        memory,
        normer,
    )


def finish(queries, numer_rows, denom_rows, row_max, row_decay, stabil_in, memory_in, normer_in):
    from_before = jnp.dot(queries, memory_in, precision=HIGH)
    normer_before = jnp.dot(queries, normer_in, precision=HIGH)
    top = jnp.maximum(row_max, row_decay + stabil_in)
    own_scale = jnp.exp(row_max - top)
    past_scale = jnp.exp(row_decay + stabil_in - top)
    numer_all = own_scale[:, None] * numer_rows + past_scale[:, None] * from_before
    denom_all = own_scale * denom_rows + past_scale * normer_before
    return numer_all / jnp.maximum(jnp.abs(denom_all), jnp.exp(-top))[:, None]


def join_state(earlier, later):
    sum_early, stab_early, mem_early, norm_early = earlier[:4]
    sum_late, stab_late, mem_late, norm_late = later[:4]
    top = jnp.maximum(sum_late + stab_early, stab_late)
    early_scale = jnp.exp(sum_late + stab_early - top)
    late_scale = jnp.exp(stab_late - top)
    joined = (
        sum_early + sum_late,
        top,
        early_scale[:, None, None] * mem_early + late_scale[:, None, None] * mem_late,
        early_scale[:, None] * norm_early + late_scale[:, None] * norm_late,
    )
    if len(earlier) > 4:
        edge = jnp.where(later[5][0] > 0, later[4], earlier[4])
        joined = joined + (edge, jnp.maximum(earlier[5], later[5]))
    return joined


def body(
    tokens,
    norm_gain,
    conv_b_w,
    conv_c_w,
    conv_u_w,
    conv_taps,
    query_w,
    key_w,
    value_w,
    outgate_w,
    gate_w,
    gate_bias,
    mem_gain,
    conv_out_w,
    mem_out_w,
):
    count = tokens.shape[0]
    model = conv_b_w.shape[0]
    weights = (
        conv_b_w,
        conv_c_w,
        conv_u_w,
        query_w,
        key_w,
        value_w,
        outgate_w,
        gate_w.reshape(model, -1),
    )
    piece, gain_piece = in_one_piece((tokens, norm_gain), "tp", 1, 0)
    wide = piece.astype(jnp.float32)
    scaled = (wide * gain_piece.astype(jnp.float32)).astype(jnp.bfloat16)
    squares = jnp.sum(wide * wide, axis=1)
    totals = tuple(
        (jnp.dot(scaled, weight, preferred_element_type=jnp.float32) for weight in weights)
    )
    folded = (squares,) + totals
    inv_rms = lax.rsqrt(folded[0] / model + EPS)[:, None]

    def project(total):
        return lax.optimization_barrier((inv_rms * total).astype(jnp.bfloat16)).astype(jnp.float32)

    gate_b, gate_c, gate_u, queries, keys, values, outgate = [
        project(total) for total in folded[1:8]
    ]
    heads = gate_bias.shape[1]
    gates = inv_rms * folded[8]
    input_pre = gates[:, :heads] + gate_bias[0]
    forget_pre = gates[:, heads:] + gate_bias[1]
    mixed_in = (gate_c * gate_u).astype(jnp.bfloat16)
    reach = conv_taps.shape[0] - 1
    head_q = queries.reshape(count, heads, HEAD_DIM)
    head_k = keys.reshape(count, heads, HEAD_DIM) * HEAD_DIM ** (-0.5)
    head_v = values.reshape(count, heads, HEAD_DIM)
    local = jax.vmap(local_pass, in_axes=1, out_axes=(1, 1, 1, 1, 0, 0, 0, 0))(
        head_q, head_k, head_v, input_pre, jax.nn.log_sigmoid(forget_pre)
    )
    numer_rows, denom_rows, row_max, row_decay, decay_sum, stabil, memory, normer = local
    identity = (
        jnp.zeros((heads,), jnp.float32),
        jnp.full((heads,), LOWEST, jnp.float32),
        jnp.zeros((heads, HEAD_DIM, HEAD_DIM), jnp.float32),
        jnp.zeros((heads, HEAD_DIM), jnp.float32),
    )
    before = shifted(mixed_in[count - reach :], SP, 1)
    incoming = carried_in((decay_sum, stabil, memory, normer), SP, join_state, identity)
    padded = jnp.concatenate([before, mixed_in], axis=0).astype(jnp.float32)
    taps = conv_taps.astype(jnp.float32)
    conv_sum = taps[0] * padded[0:count]
    for offset in range(1, reach + 1):
        conv_sum = conv_sum + taps[offset] * padded[offset : offset + count]
    y_conv = (gate_b * conv_sum).astype(jnp.bfloat16)
    mem_raw = jax.vmap(finish, in_axes=(1, 1, 1, 1, 1, 0, 0, 0), out_axes=1)(
        head_q, numer_rows, denom_rows, row_max, row_decay, incoming[1], incoming[2], incoming[3]
    )
    flat_raw = mem_raw.reshape(count, -1)
    own_squares = jnp.sum(flat_raw * flat_raw, axis=1)
    all_squares = taken_together(own_squares, "tp")
    mem_norm = flat_raw * lax.rsqrt(all_squares / MDIM + EPS)[:, None]
    mem_norm = mem_norm * mem_gain.astype(jnp.float32)[None, :]
    y_mem = (jax.nn.sigmoid(outgate) * mem_norm).astype(jnp.bfloat16)
    summed = sent_and_summed(
        (
            jnp.dot(y_conv, conv_out_w, preferred_element_type=jnp.float32)
            + jnp.dot(y_mem, mem_out_w, preferred_element_type=jnp.float32)
        ).astype(jnp.bfloat16),
        "tp",
        0,
    )
    return summed.astype(jnp.bfloat16)


def solution(mesh):
    finer = Mesh(mesh.devices.reshape(16, 8, mesh.shape["tp"]), ("sp_0", "sp_1", "tp"))
    in_specs = (
        P(SP, "tp"),
        P(None, "tp"),
        P(None, "tp"),
        P(None, "tp"),
        P(None, "tp"),
        P(None, "tp"),
        P(None, "tp"),
        P(None, "tp"),
        P(None, "tp"),
        P(None, "tp"),
        P(None, None, "tp"),
        P(None, "tp"),
        P("tp"),
        P("tp", None),
        P("tp", None),
    )
    out_specs = P(SP_TP, None)
    return jax.shard_map(body, mesh=finer, in_specs=in_specs, out_specs=out_specs, check_vma=False)
```

profile of v0, /device:TPU:1, one launch (start us, length us, event | category | flops | bytes accessed | tf_op | source)
XLA Modules:
  0.0 271.7 jit_solution(10815656453530606041)
XLA Ops:
  6.5 1.0 pad_maximum_fusion
  7.6 27.1 %all_gather.15 = bf16[129,2048]{1,0:T(8,128)(2,1)S(1)} all-gather(bf16[129,256]{1,0:T(8,128)(2,1)S(1)} %pad_maximum_fusion), channel_id=1, replica_groups=mesh['sp_0'=16,'sp_1'=8,'tp'=8] {'tp'}, dimensions={1}, use_global_device_ids=true | all-gather | bytes 594432 | tf_op jit(solution)/shard_map/all_gather | solution.py:25
  34.6 0.2 fusion.18
  34.8 1.4 fusion.336
  36.2 0.9 convolution_multiply_fusion.10
  37.2 1.3 fusion.314
  38.5 0.3 reduce_window_sum.14
  38.8 0.6 slice.482
  39.5 0.6 slice.483
  40.2 0.6 pad.14
  42.0 0.6 pad.13
  42.7 0.3 fusion.5
  43.1 1.9 exponential_multiply_fusion
  45.0 2.1 fusion.109
  47.0 1.5 fusion.6
  48.6 0.4 convolution_add_fusion.1
  49.0 0.7 maximum_bitcast_fusion
  49.8 39.2 %all-gather.7.cloned.1.call-done = f32[8,259,256]{2,1,0:T(8,128)} async-done(((f32[1,259,256]{2,1,0:T(8,128)}), f32[8,259,256]{2,1,0:T(8,128)}) %all-gather.7.cloned.1.call-update) | async-done | bytes 2121744 | tf_op jit(solution)/shard_map/all_gather | solution.py:48
  89.0 0.9 fusion.331
  89.9 0.6 fusion.334
  90.5 0.6 fusion.335
  112.2 0.8 fusion.219
  113.0 1.7 fusion.41
  114.7 0.7 maximum_bitcast_fusion.1
  115.5 1.4 fusion.9
  116.9 1.3 fusion.10
  118.3 0.5 slice.584
  118.8 2.5 collective-permute-start
  121.5 1.4 fusion.8
  122.9 0.3 fusion.4
  123.2 1.0 fusion.7
  125.1 66.6 %all-gather.9.cloned.1.call-done = f32[16,259,256]{2,1,0:T(8,128)} async-done(((f32[1,259,256]{2,1,0:T(8,128)}), f32[16,259,256]{2,1,0:T(8,128)}) %all-gather.9.cloned.1.call-update) | async-done | bytes 4243472 | tf_op jit(solution)/shard_map/all_gather | solution.py:48
  191.7 1.0 fusion.330
  192.8 0.7 fusion.332
  193.4 0.6 fusion.333
  225.9 0.2 fusion.337
  226.2 0.2 convolution_multiply_fusion.1
  226.4 1.2 fusion.17
  227.5 0.2 fusion.16
  227.7 3.9 %convolution_multiply_fusion = f32[128,256]{1,0:T(8,128)S(1)} fusion(bf16[128,256]{1,0:T(8,128)(2,1)S(1)} %fusion.7, f32[16,259,256]{2,1,0:T(8,128)} %all-gather.9.cloned.1.call-done, f32[1,256,256]{2,1,0:T(8,128)S(1)} %get-tuple-element.31, f32[1,256,256]{2,1,0:T(8,128)S(1)} %get-tuple-element.32, f32[8,259,256]{2,1,0:T(8,128)} %all-gather.7.cloned.1.call-done, ...), kind=kOutput, calls=%fused_computation.9 | convolution fusion | flops 106790912 | bytes 6525440 | tf_op jit(solution)/shard_map/vmap()/dot_general | solution.py:155
  231.6 0.4 multiply_reduce_fusion
  232.0 0.6 broadcast_in_dim.43
  232.6 13.9 %all-to-all-start = ((f32[8,1,128]{2,1,0:T(1,128)}), f32[8,1,128]{2,1,0:T(1,128)S(1)}, u32[]{:S(2)}, u32[]{:S(2)}) async-start(f32[8,1,128]{2,1,0:T(1,128)} %broadcast_in_dim.43), calls=%async_computation | async-start | bytes 8192 | tf_op jit(solution)/shard_map/all_to_all | solution.py:74
  246.5 4.5 %all-to-all-done = f32[8,1,128]{2,1,0:T(1,128)S(1)} async-done(((f32[8,1,128]{2,1,0:T(1,128)}), f32[8,1,128]{2,1,0:T(1,128)S(1)}, u32[]{:S(2)}, u32[]{:S(2)}) %all-to-all-start) | async-done | bytes 4128 | tf_op jit(solution)/shard_map/all_to_all | solution.py:74
  251.1 0.4 fusion.180
  251.4 0.3 fusion
  251.7 12.4 %all_to_all.11 = bf16[8,16,2048]{2,1,0:T(8,128)(2,1)S(1)} all-to-all(bf16[8,16,2048]{2,1,0:T(8,128)(2,1)S(1)} %bitcast.246), channel_id=1, replica_groups=mesh['sp_0'=16,'sp_1'=8,'tp'=8] {'tp'}, dimensions={0} | all-to-all | bytes 1048576 | tf_op jit(solution)/shard_map/all_to_all | solution.py:89
  264.2 0.7 reduce_sum.53
  (39 shorter events, 0.3 us)
Async XLA Ops:
  6.5 244.5 %copy-start = (bf16[256,2048]{1,0:T(8,128)(2,1)S(1)}, bf16[256,2048]{1,0:T(8,128)(2,1)}, u32[]{:S(2)}) copy-start(bf16[256,2048]{1,0:T(8,128)(2,1)} %param.29) | copy-start | bytes 3145732
  6.5 36.2 %copy-start.3 = (bf16[2048,256]{1,0:T(8,128)(2,1)S(1)}, bf16[2048,256]{1,0:T(8,128)(2,1)}, u32[]{:S(2)}) copy-start(bf16[2048,256]{1,0:T(8,128)(2,1)} %param.22) | copy-start | bytes 3145732
  6.5 82.4 %all-gather.7.cloned.1.call-start = ((), (), s32[]{:S(2)}) async-start(), calls=%async_computation.2 | async-start | bytes 2433024 | tf_op jit(solution)/shard_map/all_gather | solution.py:48
  36.2 86.7 %copy-start.7 = (f32[128]{0:T(128)}, f32[128]{0:T(128)S(1)}, u32[]{:S(2)}) copy-start(f32[128]{0:T(128)S(1)} %add_rsqrt_fusion.1) | copy-start | bytes 1540
  49.7 142.0 %all-gather.9.cloned.1.call-start = ((), (), s32[]{:S(2)}) async-start(), calls=%async_computation.3 | async-start | bytes 4595712 | tf_op jit(solution)/shard_map/all_gather | solution.py:48
  114.7 6.7 %copy-start.6 = (bf16[256]{0:T(256)(128)(2,1)S(1)}, bf16[256]{0:T(256)(128)(2,1)}, u32[]{:S(2)}) copy-start(bf16[256]{0:T(256)(128)(2,1)} %param.27) | copy-start | bytes 1540
  114.7 6.7 %copy-start.2 = (bf16[3,128]{1,0:T(4,128)(2,1)S(1)}, bf16[3,128]{1,0:T(4,128)(2,1)}, u32[]{:S(2)}) copy-start(bf16[3,128]{1,0:T(4,128)(2,1)} %param.20) | copy-start | bytes 2308
  115.5 7.4 %copy-start.4 = (bf16[2048,256]{1,0:T(8,128)(2,1)S(1)}, bf16[2048,256]{1,0:T(8,128)(2,1)}, u32[]{:S(2)}) copy-start(bf16[2048,256]{1,0:T(8,128)(2,1)} %param.24) | copy-start | bytes 3145732
  118.8 127.7 %collective-permute-start = (bf16[2,128]{1,0:T(2,128)(2,1)}, bf16[2,128]{1,0:T(2,128)(2,1)S(1)}, u32[]{:S(2)}, u32[]{:S(2)}) collective-permute-start(bf16[2,128]{1,0:T(2,128)(2,1)} %slice.584), channel_id=1, source_target_pairs={{0,8},{8,16},{16,24},{24,32},{32,40},{40,48},{48,56},{56,64},{64,7... | collective-permute-start | bytes 1544 | tf_op jit(solution)/shard_map/ppermute | solution.py:31
  121.4 1.8 copy-start.5
  231.6 19.8 %copy-start.1 = (bf16[128,2048]{1,0:T(8,128)(2,1)S(1)}, bf16[128,2048]{1,0:T(8,128)(2,1)}, u32[]{:S(2)}) copy-start(bf16[128,2048]{1,0:T(8,128)(2,1)} %param.28) | copy-start | bytes 1572868
  232.6 18.5 %all-to-all-start = ((f32[8,1,128]{2,1,0:T(1,128)}), f32[8,1,128]{2,1,0:T(1,128)S(1)}, u32[]{:S(2)}, u32[]{:S(2)}) async-start(f32[8,1,128]{2,1,0:T(1,128)} %broadcast_in_dim.43), calls=%async_computation | async-start | bytes 8192 | tf_op jit(solution)/shard_map/all_to_all | solution.py:74
Sparse Core Ops, SparseCore 0:
  49.9 39.0 all-gather.6
  115.6 76.0 all-gather.8
where the time goes:
time: 273 us; the launch traced here: 272 us
  waiting for transfers between devices  110 us (40%)
  between operations  68.7 us (25%)
  blocking collectives  39.5 us (14%)
  matrix products  17.4 us (6%)
  starting transfers between devices  16.5 us (6%)
  other arithmetic  9.63 us (4%)
  local copies, waits for them, and re-layouts  9.61 us (4%)
    all_gather x2, waiting for transfers between devices, all_in_one(): both, at, found = (lax.all_gather(jnp.concatenate(lines), axis), 0, {})  106 us
    all_gather x1, blocking collectives, in_one_piece(): lax.all_gather(both, axis, axis=dim, tiled=True)  27.1 us
    all_to_all x1, starting transfers between devices, from_everyone(): return lax.all_to_all(copies, axis, split_axis=0, concat_axis=0, tiled=True)  13.9 us
    all_to_all x1, blocking collectives, sent_and_summed(): lax.all_to_all(parts, axis, split_axis=0, concat_axis=0, tiled=True)  12.4 us
    dot_general x8, matrix products, body(): jnp.dot(scaled, weight, preferred_element_type=jnp.float32)  8.27 us
  transfers between devices with their start and end apart: 4, of which 3 were waited for; matrix products, arithmetic and copies ran while one was open for 6% of the time, Pallas kernels for 0%

commit v1 on v0

v1 whole, which is shorter than its diff:
```python
import functools

import jax
import jax.numpy as jnp
from jax import lax
from jax.experimental import pallas as pl
from jax.experimental.pallas import tpu as pltpu
from jax.sharding import Mesh
from jax.sharding import PartitionSpec as P

N = 128
HD = 256
MDIM = 2048
EPS = 1e-06
LOWEST = -1e30
ROWS = 80
TP = ("x", "c")
SP = ("z", "y")
BF = jnp.bfloat16
F32 = jnp.float32
INTERPRET = False


def call(kernel, outs, *args, name=None):
    return pl.pallas_call(
        kernel,
        out_shape=[jax.ShapeDtypeStruct(s, d) for s, d in outs],
        interpret=INTERPRET,
        name=name,
    )(*args)


def iota(dim):
    return lax.broadcasted_iota(jnp.int32, (N, N), dim)


def to_row(col):
    return jnp.sum(jnp.where(iota(0) == iota(1), col, 0.0), axis=0, keepdims=True)


def to_col(row):
    return jnp.sum(jnp.where(iota(0) == iota(1), row, 0.0), axis=1, keepdims=True)


def pieces(x):
    hi = x.astype(BF)
    rest = x - hi.astype(F32)
    mid = rest.astype(BF)
    low = (rest - mid.astype(F32)).astype(BF)
    return hi, mid, low


def dot(a, b):
    return jnp.dot(a, b, preferred_element_type=F32)


def dot_two(a, b):
    hi = a.astype(BF)
    return dot(hi, b) + dot((a - hi.astype(F32)).astype(BF), b)


def prepare(tok, gain, out):
    wide = tok[...].astype(F32)
    out[0, :N, :] = (wide * gain[...].astype(F32)).astype(BF)
    squares = to_row(jnp.sum(wide * wide, axis=1, keepdims=True))
    hi, mid, low = pieces(squares)
    zero = jnp.zeros((13, N), F32)
    tail = jnp.concatenate([hi.astype(F32), mid.astype(F32), low.astype(F32), zero], axis=0)
    out[0, N:, :N] = tail.astype(BF)
    out[0, N:, N:] = jnp.zeros((16, N), BF)


def log_sigmoid(x):
    e = jnp.exp(-jnp.abs(x))
    series = e * (1.0 - e * (0.5 - e * (1.0 / 3.0 - e * 0.25)))
    return -(jnp.maximum(-x, 0.0) + jnp.where(e < 0.01, series, jnp.log(1.0 + e)))


def states(tok, kw, vw, gw, bias, message, keys, values, aux):
    groups, _, part = tok.shape
    k_sum = jnp.zeros((N, HD), F32)
    v_sum = jnp.zeros((N, HD), F32)
    g_sum = jnp.zeros((N, 2), F32)
    sq = jnp.zeros((1, N), F32)
    for g in range(groups):
        piece = tok[g, :N, :]
        at = pl.ds(g * part, part)
        k_sum += dot(piece, kw[at, :])
        v_sum += dot(piece, vw[at, :])
        g_sum += dot(piece, gw[at, :])
        tail = tok[g, N:, :N].astype(F32)
        sq += tail[0:1] + tail[1:2] + tail[2:3]
    inv = lax.rsqrt(to_col(sq) / (groups * part) + EPS)
    k = (inv * k_sum).astype(BF)
    v = (inv * v_sum).astype(BF)
    keys[...] = k
    values[...] = v
    gates = inv * g_sum
    i_col = gates[:, 0:1] + bias[0:1, 0:1]
    lf_col = log_sigmoid(gates[:, 1:2] + bias[1:2, 0:1])
    lf_row = to_row(lf_col)
    i_row = to_row(i_col)
    lower = iota(1) <= iota(0)
    b_col = jnp.sum(jnp.where(lower, lf_row, 0.0), axis=1, keepdims=True)
    b_row = jnp.sum(jnp.where(iota(0) <= iota(1), lf_col, 0.0), axis=0, keepdims=True)
    b_all = jnp.sum(lf_col, axis=0, keepdims=True)
    after = jnp.sum(jnp.where(iota(1) > iota(0), lf_row, 0.0), axis=1, keepdims=True)
    weight = after + i_col
    top = jnp.max(weight, axis=0, keepdims=True)
    weight = jnp.exp(weight - top)
    kf = k.astype(F32) * HD**-0.5
    weighted = weight * kf
    hi = weighted.astype(BF)
    low = (weighted - hi.astype(F32)).astype(BF)
    across = (((0,), (0,)), ((), ()))
    memory = lax.dot_general(hi, v, across, preferred_element_type=F32)
    memory += lax.dot_general(low, v, across, preferred_element_type=F32)
    normer = jnp.sum(weighted, axis=0, keepdims=True)
    n_hi = normer.astype(BF).astype(F32)
    n_low = normer - n_hi
    lane = lambda a: jnp.broadcast_to(a, (1, N)).astype(F32)
    rest = [n_hi[:, :N], n_hi[:, N:], n_low[:, :N], n_low[:, N:]]
    rest += [lane(p) for p in pieces(b_all)] + [lane(p) for p in pieces(top)]
    rest = jnp.concatenate(rest + [jnp.zeros((16 - len(rest), N), F32)], axis=0).astype(BF)
    count, cut = message.shape[0], HD // message.shape[0]
    for y in range(count):
        rows = memory[y * cut : (y + 1) * cut].astype(BF)
        message[y, :cut, :] = rows[:, :N]
        message[y, cut : 2 * cut, :] = rows[:, N:]
        message[y, 2 * cut :, :] = rest
    aux[...] = jnp.concatenate([b_row, i_row, to_row(inv), jnp.zeros((5, N), F32)], axis=0)


def unpack(tail):
    t = tail.astype(F32)
    return t[0:2] + t[2:4], t[4:5] + t[5:6] + t[6:7], t[7:8] + t[8:9] + t[9:10]


def scales(sums, tops, upto):
    run, logs = jnp.zeros((1, N), F32), [None] * upto
    for j in reversed(range(upto)):
        logs[j] = tops[j] + run
        run = run + sums[j]
    return logs, run


def biggest(logs):
    top = jnp.full((1, N), LOWEST, F32)
    for a in logs:
        top = jnp.maximum(top, a)
    return top


def row_total(arrived, message):
    count, rows, _ = arrived.shape
    body = rows - 16
    extra = [unpack(arrived[j, body:, :]) for j in range(count)]
    logs, run = scales([e[1] for e in extra], [e[2] for e in extra], count)
    top = biggest(logs)
    total = jnp.zeros((body, N), F32)
    normer = jnp.zeros((2, N), F32)
    for j in range(count):
        w = jnp.exp(logs[j] - top)
        total += w * arrived[j, :body, :].astype(F32)
        normer += w * extra[j][0]
    n_hi = normer.astype(BF).astype(F32)
    rest = [n_hi, normer - n_hi] + [p.astype(F32) for p in pieces(run)]
    rest += [p.astype(F32) for p in pieces(top)] + [jnp.zeros((6, N), F32)]
    rest = jnp.concatenate(rest, axis=0).astype(BF)
    total = total.astype(BF)
    for z in range(message.shape[0]):
        message[z, :body, :] = total
        message[z, body:, :] = rest


def prefixes(place, row, column, message, own):
    z, y = place[0], place[1]
    count, rows, _ = row.shape
    body = rows - 16
    depth = column.shape[0]
    past = [unpack(column[j, body:, :]) for j in range(depth)]
    run, logs = jnp.zeros((1, N), F32), [None] * depth
    for j in reversed(range(depth)):
        logs[j] = jnp.where(j < z, past[j][2] + run, LOWEST)
        run = jnp.where(j < z, run + past[j][1], run)
    z_top = biggest(logs)
    before = jnp.zeros((body, N), F32)
    z_norm = jnp.zeros((2, N), F32)
    for j in range(depth):
        w = jnp.where(j < z, jnp.exp(logs[j] - z_top), 0.0)
        before += w * column[j, :body, :].astype(F32)
        z_norm += w * past[j][0]
    extra = [unpack(row[j, body:, :]) for j in range(count)]
    mine = jnp.zeros((3, N), F32)
    for t in range(count):
        logs, run = scales([e[1] for e in extra], [e[2] for e in extra], t)
        top = jnp.maximum(biggest(logs), z_top + run)
        w = jnp.exp(z_top + run - top)
        state = w * before
        norm = w * z_norm
        for j in range(t):
            w = jnp.exp(logs[j] - top)
            state += w * row[j, :body, :].astype(F32)
            norm += w * extra[j][0]
        message[t, :, :] = state.astype(BF)
        mine = jnp.where(t == y, jnp.concatenate([norm, top], axis=0), mine)
    own[...] = jnp.concatenate([mine, jnp.zeros((5, N), F32)], axis=0)


def inside(tok, aux, k_ref, v_ref, qw, ow, bw, cw, uw, gain, queries, numer, cols, gate, gate_b, mixed):
    groups, _, part = tok.shape
    sums = [jnp.zeros((N, w.shape[1]), F32) for w in (qw, ow, bw, cw, uw)]
    for g in range(groups):
        piece = tok[g, :N, :]
        at = pl.ds(g * part, part)
        sums = [s + dot(piece, w[at, :]) for s, w in zip(sums, (qw, ow, bw, cw, uw))]
    b_row, i_row = aux[0:1, :], aux[1:2, :]
    inv = to_col(aux[2:3, :])
    q, og, gb, gc, gu = [(inv * s).astype(BF) for s in sums]
    queries[...] = q
    gate_b[...] = gb
    mixed[...] = (gc.astype(F32) * gu.astype(F32)).astype(BF)
    gate[...] = jax.nn.sigmoid(og.astype(F32)) * gain[...].astype(F32)
    b_col = to_col(b_row)
    causal = iota(1) <= iota(0)
    decays = jnp.where(causal, b_col - b_row + i_row, LOWEST)
    top = jnp.max(decays, axis=1, keepdims=True)
    weights = jnp.where(causal, jnp.exp(decays - top), 0.0)
    scores = lax.dot_general(q, k_ref[...], (((1,), (1,)), ((), ())), preferred_element_type=F32)
    scores = scores * HD**-0.5 * weights
    numer[...] = dot_two(scores, v_ref[...])
    denom = jnp.sum(scores, axis=1, keepdims=True)
    lane = iota(1)
    cols[...] = jnp.where(lane == 0, b_col, jnp.where(lane == 1, top, jnp.where(lane == 2, denom, 0.0)))


def convolve(halo, mixed, gate_b, taps, weight, out):
    now = mixed[...].astype(F32)
    prev = halo[...].astype(F32)
    row = iota(0)
    one = jnp.where(row == 0, prev[1:2], pltpu.roll(now, 1, 0))
    two = jnp.where(row == 0, prev[0:1], jnp.where(row == 1, prev[1:2], pltpu.roll(now, 2, 0)))
    t = taps[...].astype(F32)
    total = t[0:1] * two + t[1:2] * one + t[2:3] * now
    y = (gate_b[...].astype(F32) * total).astype(BF)
    count, rows, _ = out.shape
    done = dot(y, weight[...]).astype(BF)
    for g in range(count):
        out[g, :, :] = done[g * rows : (g + 1) * rows]


def finish(arrived, own, queries, numer, cols, gate, weight, out):
    count, rows, _ = arrived.shape
    half = rows // 2
    q = queries[...]
    left = arrived[:, :half, :].reshape(HD, N)
    right = arrived[:, half:, :].reshape(HD, N)
    past = jnp.concatenate([dot(q, left), dot(q, right)], axis=1)
    qf = q.astype(F32)
    past_den = jnp.sum(qf[:, :N] * own[0:1, :] + qf[:, N:] * own[1:2, :], axis=1, keepdims=True)
    b_col, top, denom = cols[:, 0:1], cols[:, 1:2], cols[:, 2:3]
    inter = b_col + own[2:3, 0:1]
    most = jnp.maximum(inter, top)
    old, new = jnp.exp(inter - most), jnp.exp(top - most)
    den = old * past_den + new * denom
    raw = (old * past + new * numer[...]) / jnp.maximum(jnp.abs(den), jnp.exp(-most))
    squares = jnp.sum(raw * raw, axis=1, keepdims=True)
    y = (gate[...] * raw).astype(BF)
    done = dot(y, weight[...]).astype(BF)
    parts = [p.astype(F32) for p in pieces(squares)]
    lane = iota(1)
    tail = jnp.where(lane == 0, parts[0], jnp.where(lane == 1, parts[1], jnp.where(lane == 2, parts[2], 0.0)))
    tail = tail.astype(BF)
    groups, size, width = out.shape
    for g in range(groups):
        out[g, :, : width - N] = done[g * size : (g + 1) * size]
        out[g, :, width - N :] = tail[g * size : (g + 1) * size]


def gather_up(conv, mem, out):
    groups, _, width = conv.shape
    squares = jnp.zeros((conv.shape[1], 1), F32)
    for g in range(groups):
        tail = mem[g, :, width:].astype(F32)
        squares += tail[:, 0:1] + tail[:, 1:2] + tail[:, 2:3]
    scale = lax.rsqrt(squares / MDIM + EPS)
    c = jnp.zeros(conv.shape[1:], F32)
    m = jnp.zeros(conv.shape[1:], F32)
    for g in range(groups):
        c += conv[g].astype(F32)
        m += mem[g, :, :width].astype(F32)
    out[...] = (c + scale * m).astype(BF)


def exchange(value, axis):
    return lax.all_to_all(value, axis, split_axis=0, concat_axis=0, tiled=True)


def body(tokens, norm_gain, conv_b_w, conv_c_w, conv_u_w, conv_taps, query_w, key_w, value_w, outgate_w,
         gate_w, gate_bias, mem_gain, conv_out_w, mem_out_w):
    model = key_w.shape[0]
    nz, ny = lax.axis_size("z"), lax.axis_size("y")
    groups = lax.axis_size(TP)
    (local,) = call(prepare, [((1, N + 16, tokens.shape[1]), BF)], tokens, norm_gain, name="prepare")
    tok = lax.all_gather(local, TP, axis=0, tiled=True)
    slices = 2 * HD // ny
    message, keys, values, aux = call(
        states,
        [((ny, slices + 16, N), BF), ((N, HD), BF), ((N, HD), BF), ((8, N), F32)],
        tok, key_w, value_w, gate_w.reshape(model, 2), gate_bias, name="states",
    )
    row = exchange(message, "y")
    queries, numer, cols, gate, gate_b, mixed = call(
        inside,
        [((N, HD), BF), ((N, HD), F32), ((N, N), F32), ((N, HD), F32), ((N, N), BF), ((N, N), BF)],
        tok, aux, keys, values, query_w, outgate_w, conv_b_w, conv_c_w, conv_u_w, mem_gain[None, :], name="inside",
    )
    count = nz * ny
    halo = lax.ppermute(mixed[N - 2 :], SP, [(i, i + 1) for i in range(count - 1)])
    (total,) = call(row_total, [((nz, slices + 16, N), BF)], row, name="row_total")
    column = exchange(total, "z")
    (conv,) = call(convolve, [((groups, N // groups, model), BF)], halo, mixed, gate_b, conv_taps, conv_out_w, name="convolve")
    conv = exchange(conv, TP)
    place = jnp.stack([lax.axis_index("z"), lax.axis_index("y")]).astype(jnp.int32)
    back, own = pl.pallas_call(
        prefixes,
        out_shape=[jax.ShapeDtypeStruct((ny, slices, N), BF), jax.ShapeDtypeStruct((8, N), F32)],
        in_specs=[
            pl.BlockSpec(memory_space=pltpu.SMEM),
            pl.BlockSpec(memory_space=pltpu.VMEM),
            pl.BlockSpec(memory_space=pltpu.VMEM),
        ],
        interpret=INTERPRET,
        name="prefixes",
    )(place, row, column)
    state = exchange(back, "y")
    (mem,) = call(
        finish, [((groups, N // groups, model + N), BF)], state, own, queries, numer, cols, gate, mem_out_w, name="finish"
    )
    mem = exchange(mem, TP)
    (out,) = call(gather_up, [((N // groups, model), BF)], conv, mem, name="gather_up")
    return out


def solution(mesh):
    sp = mesh.shape["sp"]
    ny = 8 if sp % 8 == 0 else sp
    finer = Mesh(mesh.devices.reshape(sp // ny, ny, mesh.shape["tp"] // 2, 2), ("z", "y", "x", "c"))
    cols = P(None, TP)
    in_specs = (
        P(SP, TP), cols, cols, cols, cols, cols, cols, cols, cols, cols,
        P(None, None, TP), cols, P(TP), P(TP, None), P(TP, None),
    )
    return jax.shard_map(body, mesh=finer, in_specs=in_specs, out_specs=P(SP + TP, None), check_vma=False)
```

time: 273 us -> 134 us (0.49)
  waiting for transfers between devices: 110 us -> 20.3 us
  between operations: 68.7 us -> 0.04 us
  Pallas kernels: 0 us -> 20.2 us
  blocking collectives: 39.5 us -> 58 us
  matrix products: 17.4 us -> 0 us
  starting transfers between devices: 16.5 us -> 27.8 us
  other arithmetic: 9.63 us -> 0.67 us
  local copies, waits for them, and re-layouts: 9.61 us -> 5.41 us
    all_gather x2 -> x0, waiting for transfers between devices: 106 us -> none  [all_in_one(): both, at, found = (lax.all_gather(jnp.concatenate(lines), axis), 0, {})]
    pallas_call x0 -> x8, Pallas kernels: none -> 20.2 us  [the longest x7 18.2 us: call(): pl.pallas_call(kernel, out_shape=[jax.ShapeDtypeStruct(s, d) for s, d in...]
    dot_general x18 -> x0, matrix products: 17.4 us -> none  [the longest x8 8.27 us: body(): jnp.dot(scaled, weight, preferred_element_type=jnp.float32)]
    all_to_all x1 -> x2, blocking collectives: 12.4 us -> 29.4 us  [exchange(): return lax.all_to_all(value, axis, split_axis=0, concat_axis=0, tiled=True)]
    all_to_all x1 -> x3, waiting for transfers between devices: 4.51 us -> 19.6 us  [exchange(): return lax.all_to_all(value, axis, split_axis=0, concat_axis=0, tiled=True)]
    all_to_all x1 -> x3, starting transfers between devices: 13.9 us -> 24.4 us  [exchange(): return lax.all_to_all(value, axis, split_axis=0, concat_axis=0, tiled=True)]
    slice x10 -> x1, local copies, waits for them, and re-layouts: 7.68 us -> 0.68 us  [body(): mixed[N - 2:]]
    unnamed x19 -> x14, local copies, waits for them, and re-layouts: 0.05 us -> 4.19 us
  transfers between devices with their start and end apart: 4 -> 4, of which waited for: 3 -> 3; matrix products, arithmetic and copies ran while one was open for 6% -> 1% of each run, Pallas kernels for 0% -> 7%
where the time goes in v1:
time: 134 us; the launch traced here: 132 us
  blocking collectives  58 us (43%)
  starting transfers between devices  27.8 us (21%)
  waiting for transfers between devices  20.3 us (15%)
  Pallas kernels  20.2 us (15%)
  local copies, waits for them, and re-layouts  5.41 us (4%)
    all_to_all x2, blocking collectives, exchange(): return lax.all_to_all(value, axis, split_axis=0, concat_axis=0, tiled=True)  29.4 us
    all_gather x1, blocking collectives, body(): tok = lax.all_gather(local, TP, axis=0, tiled=True)  28.5 us
    all_to_all x3, starting transfers between devices, exchange(): return lax.all_to_all(value, axis, split_axis=0, concat_axis=0, tiled=True)  24.4 us
    all_to_all x3, waiting for transfers between devices, exchange(): return lax.all_to_all(value, axis, split_axis=0, concat_axis=0, tiled=True)  19.6 us
    pallas_call x7, Pallas kernels, call(): pl.pallas_call(kernel, out_shape=[jax.ShapeDtypeStruct(s, d) for s, d in...  18.2 us
    unnamed x14, local copies, waits for them, and re-layouts  4.19 us
    ppermute x1, starting transfers between devices, body(): lax.ppermute(mixed[N - 2:], SP, [(i, i + 1) for i in range(count - 1)])  3.35 us
  transfers between devices with their start and end apart: 4, of which 3 were waited for; matrix products, arithmetic and copies ran while one was open for 1% of the time, Pallas kernels for 7%

profile of v1, /device:TPU:1, one launch (start us, length us, event | category | flops | bytes accessed | tf_op | source)
XLA Modules:
  0.0 132.3 jit_solution(13429595505940977744)
XLA Ops:
  0.0 1.2 copy.19.bias
  1.2 1.6 %prepare.1 = bf16[1,144,256]{2,1,0:T(8,128)(2,1)} custom-call(bf16[128,256]{1,0:T(8,128)(2,1)} %tok.1, bf16[1,256]{1,0:T(2,128)(2,1)} %gain.1), custom_call_target="tpu_custom_call" | custom-call | tf_op jit(solution)/shard_map/prepare/pallas_call | solution.py:25
  2.8 0.0 copy-start.3
  2.8 28.5 %all_gather.3.tok = bf16[8,144,256]{2,1,0:T(8,128)(2,1)} all-gather(bf16[1,144,256]{2,1,0:T(8,128)(2,1)} %prepare.1), channel_id=1, replica_groups=mesh['z'=16,'y'=8,'x'=4,'c'=2] {'x','c'}, dimensions={0}, use_global_device_ids=true | all-gather | bytes 663552 | tf_op jit(solution)/shard_map/all_gather | solution.py:305
  31.4 0.0 copy-done.3
  31.4 1.1 copy.18
  32.4 3.7 %states.1 = (bf16[8,80,128]{2,1,0:T(8,128)(2,1)}, bf16[128,256]{1,0:T(8,128)(2,1)}, bf16[128,256]{1,0:T(8,128)(2,1)}, f32[8,128]{1,0:T(8,128)}) custom-call(bf16[8,144,256]{2,1,0:T(8,128)(2,1)} %all_gather.3.tok, bf16[2048,256]{1,0:T(8,128)(2,1)} %kw.1, bf16[2048,256]{1,0:T(8,128)(2,1)} %vw.1, bf16[2048,2]{1,0:T(8,128)(2,1)} %bitcast.3, f32[2,1]{1,0:T(2,128)} %copy.19.bias), custom_call_target="tpu_custom_call" | custom-call | tf_op jit(solution)/shard_map/states/pallas_call | solution.py:25
  36.1 14.1 %all_to_all.25.arrived.row = bf16[8,80,128]{2,1,0:T(8,128)(2,1)} all-to-all(bf16[8,80,128]{2,1,0:T(8,128)(2,1)} %get-tuple-element.22), channel_id=1, replica_groups=mesh['z'=16,'y'=8,'x'=4,'c'=2] {'y'}, dimensions={0} | all-to-all | bytes 327680 | tf_op jit(solution)/shard_map/all_to_all | solution.py:296
  50.3 1.7 %row_total.1 = bf16[16,80,128]{2,1,0:T(8,128)(2,1)} custom-call(bf16[8,80,128]{2,1,0:T(8,128)(2,1)} %all_to_all.25.arrived.row), custom_call_target="tpu_custom_call" | custom-call | tf_op jit(solution)/shard_map/row_total/pallas_call | solution.py:25
  52.0 8.1 %all-to-all-start.2 = ((bf16[16,80,128]{2,1,0:T(8,128)(2,1)}), bf16[16,80,128]{2,1,0:T(8,128)(2,1)S(1)}, u32[]{:S(2)}, u32[]{:S(2)}) async-start(bf16[16,80,128]{2,1,0:T(8,128)(2,1)} %row_total.1), calls=%async_computation.2 | async-start | bytes 655360 | tf_op jit(solution)/shard_map/all_to_all | solution.py:296
  60.1 0.7 pad_add_fusion.place
  60.7 13.2 %all-to-all-done.2.column = bf16[16,80,128]{2,1,0:T(8,128)(2,1)S(1)} async-done(((bf16[16,80,128]{2,1,0:T(8,128)(2,1)}), bf16[16,80,128]{2,1,0:T(8,128)(2,1)S(1)}, u32[]{:S(2)}, u32[]{:S(2)}) %all-to-all-start.2) | async-done | bytes 327712 | tf_op jit(solution)/shard_map/all_to_all | solution.py:296
  73.9 0.0 copy-start.1
  73.9 0.7 copy-done.1
  74.6 2.0 %prefixes.1 = (bf16[8,64,128]{2,1,0:T(8,128)(2,1)}, f32[8,128]{1,0:T(8,128)}) custom-call(s32[2]{0:T(128)} %pad_add_fusion.place, bf16[8,80,128]{2,1,0:T(8,128)(2,1)} %all_to_all.25.arrived.row, bf16[16,80,128]{2,1,0:T(8,128)(2,1)} %copy-done.1), custom_call_target="tpu_custom_call" | custom-call | tf_op jit(solution)/shard_map/prefixes/pallas_call | solution.py:325
  76.6 0.0 copy-start.5
  76.6 3.9 %all-to-all-start.3 = ((bf16[8,64,128]{2,1,0:T(8,128)(2,1)}), bf16[8,64,128]{2,1,0:T(8,128)(2,1)S(1)}, u32[]{:S(2)}, u32[]{:S(2)}) async-start(bf16[8,64,128]{2,1,0:T(8,128)(2,1)} %get-tuple-element.23), calls=%async_computation.3 | async-start | bytes 262144 | tf_op jit(solution)/shard_map/all_to_all | solution.py:296
  80.5 0.0 copy-done.5
  80.6 0.5 broadcast_in_dim.3.gain
  81.1 4.0 %inside.1 = (bf16[128,256]{1,0:T(8,128)(2,1)}, f32[128,256]{1,0:T(8,128)}, f32[128,128]{1,0:T(8,128)}, f32[128,256]{1,0:T(8,128)}, bf16[128,128]{1,0:T(8,128)(2,1)}, /*index=5*/bf16[128,128]{1,0:T(8,128)(2,1)}) custom-call(bf16[8,144,256]{2,1,0:T(8,128)(2,1)} %all_gather.3.tok, f32[8,128]{1,0:T(8,128)} %get-tuple-element.17.aux, ...), custom_call_target="tpu_custom_call" | custom-call | tf_op jit(solution)/shard_map/inside/pallas_call | solution.py:25
  85.1 0.7 slice.3
  85.8 3.4 %collective-permute-start = (bf16[2,128]{1,0:T(2,128)(2,1)S(1)}, bf16[2,128]{1,0:T(2,128)(2,1)S(1)}, u32[]{:S(2)}, u32[]{:S(2)}) collective-permute-start(bf16[2,128]{1,0:T(2,128)(2,1)S(1)} %slice.3), channel_id=1, source_target_pairs={{0,8},{8,16},{16,24},{24,32},{32,40},{40,48},{48,56},{56,64},{64,7... | collective-permute-start | bytes 1544 | tf_op jit(solution)/shard_map/ppermute | solution.py:319
  89.2 0.7 collective-permute-done.halo
  89.9 0.0 copy-start.4
  89.9 0.5 copy-done.4
  90.4 2.2 %convolve.1 = bf16[8,16,2048]{2,1,0:T(8,128)(2,1)} custom-call(bf16[2,128]{1,0:T(2,128)(2,1)} %copy-done.4, bf16[128,128]{1,0:T(8,128)(2,1)} %get-tuple-element.20.mixed, bf16[128,128]{1,0:T(8,128)(2,1)} %get-tuple-element.21.gate_b, bf16[3,128]{1,0:T(4,128)(2,1)} %taps.1, bf16[128,2048]{1,0:T(8,128)(2,1)} %weight.2), custom_call_target="tpu_custom_call" | custom-call | tf_op jit(solution)/shard_map/convolve/pallas_call | solution.py:25
  92.6 0.0 all-to-all-done.3.arrived
  92.6 0.0 copy-start.2
  92.6 0.7 copy-done.2
  93.2 12.4 %all-to-all-start = ((bf16[8,16,2048]{2,1,0:T(8,128)(2,1)}), bf16[8,16,2048]{2,1,0:T(8,128)(2,1)S(1)}, u32[]{:S(2)}, u32[]{:S(2)}) async-start(bf16[8,16,2048]{2,1,0:T(8,128)(2,1)} %convolve.1), calls=%async_computation | async-start | bytes 1048576 | tf_op jit(solution)/shard_map/all_to_all | solution.py:296
  105.6 2.9 %finish.1 = bf16[8,16,2176]{2,1,0:T(8,128)(2,1)} custom-call(bf16[8,64,128]{2,1,0:T(8,128)(2,1)} %copy-done.2, f32[8,128]{1,0:T(8,128)} %get-tuple-element.24.own, bf16[128,256]{1,0:T(8,128)(2,1)} %get-tuple-element.25.queries, f32[128,256]{1,0:T(8,128)} %get-tuple-element.26.numer, f32[128,128]{1,0:T(8,128)} %get-tuple-element.27.cols, ...), custom_call_target="tpu_custom_call" | custom-call | tf_op jit(solution)/shard_map/finish/pallas_call | solution.py:25
  108.6 6.4 %all-to-all-done.conv = bf16[8,16,2048]{2,1,0:T(8,128)(2,1)S(1)} async-done(((bf16[8,16,2048]{2,1,0:T(8,128)(2,1)}), bf16[8,16,2048]{2,1,0:T(8,128)(2,1)S(1)}, u32[]{:S(2)}, u32[]{:S(2)}) %all-to-all-start) | async-done | bytes 524320 | tf_op jit(solution)/shard_map/all_to_all | solution.py:296
  115.0 0.0 copy-start
  115.0 15.3 %all_to_all.26.mem = bf16[8,16,2176]{2,1,0:T(8,128)(2,1)} all-to-all(bf16[8,16,2176]{2,1,0:T(8,128)(2,1)} %finish.1), channel_id=1, replica_groups=mesh['z'=16,'y'=8,'x'=4,'c'=2] {'x','c'}, dimensions={0} | all-to-all | bytes 1114112 | tf_op jit(solution)/shard_map/all_to_all | solution.py:296
  130.3 0.0 copy-done
  130.3 2.0 %gather_up.1 = bf16[16,2048]{1,0:T(8,128)(2,1)} custom-call(bf16[8,16,2048]{2,1,0:T(8,128)(2,1)} %copy-done, bf16[8,16,2176]{2,1,0:T(8,128)(2,1)} %all_to_all.26.mem), custom_call_target="tpu_custom_call" | custom-call | tf_op jit(solution)/shard_map/gather_up/pallas_call | solution.py:25
Async XLA Ops:
  2.8 28.5 %copy-start.3 = (bf16[2048,2,1]{0,1,2:T(2,128)(2,1)S(1)}, bf16[2048,2,1]{0,1,2:T(2,128)(2,1)}, u32[]{:S(2)}) copy-start(bf16[2048,2,1]{0,1,2:T(2,128)(2,1)} %param.25) | copy-start | bytes 24580
  52.0 21.9 %all-to-all-start.2 = ((bf16[16,80,128]{2,1,0:T(8,128)(2,1)}), bf16[16,80,128]{2,1,0:T(8,128)(2,1)S(1)}, u32[]{:S(2)}, u32[]{:S(2)}) async-start(bf16[16,80,128]{2,1,0:T(8,128)(2,1)} %row_total.1), calls=%async_computation.2 | async-start | bytes 655360 | tf_op jit(solution)/shard_map/all_to_all | solution.py:296
  73.9 0.7 copy-start.1
  76.6 3.9 %copy-start.5 = (bf16[256]{0:T(256)(128)(2,1)S(1)}, bf16[256]{0:T(256)(128)(2,1)}, u32[]{:S(2)}) copy-start(bf16[256]{0:T(256)(128)(2,1)} %param.27) | copy-start | bytes 1540
  76.6 16.0 %all-to-all-start.3 = ((bf16[8,64,128]{2,1,0:T(8,128)(2,1)}), bf16[8,64,128]{2,1,0:T(8,128)(2,1)S(1)}, u32[]{:S(2)}, u32[]{:S(2)}) async-start(bf16[8,64,128]{2,1,0:T(8,128)(2,1)} %get-tuple-element.23), calls=%async_computation.3 | async-start | bytes 262144 | tf_op jit(solution)/shard_map/all_to_all | solution.py:296
  85.8 4.1 %collective-permute-start = (bf16[2,128]{1,0:T(2,128)(2,1)S(1)}, bf16[2,128]{1,0:T(2,128)(2,1)S(1)}, u32[]{:S(2)}, u32[]{:S(2)}) collective-permute-start(bf16[2,128]{1,0:T(2,128)(2,1)S(1)} %slice.3), channel_id=1, source_target_pairs={{0,8},{8,16},{16,24},{24,32},{32,40},{40,48},{48,56},{56,64},{64,7... | collective-permute-start | bytes 1544 | tf_op jit(solution)/shard_map/ppermute | solution.py:319
  89.9 0.5 copy-start.4
  92.6 0.7 copy-start.2
  93.2 21.7 %all-to-all-start = ((bf16[8,16,2048]{2,1,0:T(8,128)(2,1)}), bf16[8,16,2048]{2,1,0:T(8,128)(2,1)S(1)}, u32[]{:S(2)}, u32[]{:S(2)}) async-start(bf16[8,16,2048]{2,1,0:T(8,128)(2,1)} %convolve.1), calls=%async_computation | async-start | bytes 1048576 | tf_op jit(solution)/shard_map/all_to_all | solution.py:296
  115.0 15.3 %copy-start = (bf16[8,16,2048]{2,1,0:T(8,128)(2,1)}, bf16[8,16,2048]{2,1,0:T(8,128)(2,1)S(1)}, u32[]{:S(2)}) copy-start(bf16[8,16,2048]{2,1,0:T(8,128)(2,1)S(1)} %all-to-all-done.conv) | copy-start | bytes 1572868

commit v2 on v1

v2 whole, which is shorter than its diff:
```python
import jax
import jax.numpy as jnp
from jax import lax
from jax.experimental import pallas as pl
from jax.experimental.pallas import tpu as pltpu
from jax.sharding import Mesh
from jax.sharding import PartitionSpec as P


N = 128
HD = 256
MDIM = 2048
EPS = 1e-06
LOWEST = -1e30
TP = "tp"
SP = "sp"
BF = jnp.bfloat16
F32 = jnp.float32
INTERPRET = False


def call(kernel, outs, *args, flops=0, scratch=(), specs=None, limit=16):
    options = {} if specs is None else {"in_specs": specs}
    return pl.pallas_call(
        kernel,
        out_shape=[jax.ShapeDtypeStruct(s, d) for s, d in outs],
        scratch_shapes=scratch,
        interpret=INTERPRET,
        compiler_params=pltpu.CompilerParams(vmem_limit_bytes=limit * 2**20),
        cost_estimate=pl.CostEstimate(flops=flops, bytes_accessed=flops // 1000, transcendentals=0) if flops else None,
        **options,
    )(*args)


def iota(dim):
    return lax.broadcasted_iota(jnp.int32, (N, N), dim)


def to_row(col):
    return jnp.sum(jnp.where(iota(0) == iota(1), col, 0.0), axis=0, keepdims=True)


def to_col(row):
    return jnp.sum(jnp.where(iota(0) == iota(1), row, 0.0), axis=1, keepdims=True)


def pieces(x):
    hi = x.astype(BF)
    rest = x - hi.astype(F32)
    mid = rest.astype(BF)
    low = (rest - mid.astype(F32)).astype(BF)
    return hi, mid, low


def dot(a, b):
    return jnp.dot(a, b, preferred_element_type=F32)


def dot_two(a, b):
    hi = a.astype(BF)
    return dot(hi, b) + dot((a - hi.astype(F32)).astype(BF), b)


def prepare(tok, gain, out):
    wide = tok[...].astype(F32)
    out[0, :N, :] = (wide * gain[...].astype(F32)).astype(BF)
    squares = to_row(jnp.sum(wide * wide, axis=1, keepdims=True))
    hi, mid, low = pieces(squares)
    zero = jnp.zeros((13, N), F32)
    tail = jnp.concatenate([hi.astype(F32), mid.astype(F32), low.astype(F32), zero], axis=0)
    out[0, N:, :N] = tail.astype(BF)
    out[0, N:, N:] = jnp.zeros((16, N), BF)


def log_sigmoid(x):
    e = jnp.exp(-jnp.abs(x))
    series = e * (1.0 - e * (0.5 - e * (1.0 / 3.0 - e * 0.25)))
    return -(jnp.maximum(-x, 0.0) + jnp.where(e < 0.01, series, jnp.log(1.0 + e)))


def states(tok, kw, vw, gw, bias, message, keys, values, aux, state):
    groups, _, part = tok.shape
    k_sum = jnp.zeros((N, HD), F32)
    v_sum = jnp.zeros((N, HD), F32)
    g_sum = jnp.zeros((N, 2), F32)
    sq = jnp.zeros((1, N), F32)
    for g in range(groups):
        piece = tok[g, :N, :]
        at = pl.ds(g * part, part)
        k_sum += dot(piece, kw[at, :])
        v_sum += dot(piece, vw[at, :])
        g_sum += lax.dot_general(piece, gw[:, at], (((1,), (1,)), ((), ())), preferred_element_type=F32)
        tail = tok[g, N:, :N].astype(F32)
        sq += tail[0:1] + tail[1:2] + tail[2:3]
    inv = lax.rsqrt(to_col(sq) / (groups * part) + EPS)
    k = (inv * k_sum).astype(BF)
    v = (inv * v_sum).astype(BF)
    keys[...] = k
    values[...] = v
    gates = inv * g_sum
    i_col = gates[:, 0:1] + bias[0:1, 0:1]
    lf_col = log_sigmoid(gates[:, 1:2] + bias[0:1, 1:2])
    lf_row = to_row(lf_col)
    i_row = to_row(i_col)
    lower = iota(1) <= iota(0)
    b_col = jnp.sum(jnp.where(lower, lf_row, 0.0), axis=1, keepdims=True)
    b_row = jnp.sum(jnp.where(iota(0) <= iota(1), lf_col, 0.0), axis=0, keepdims=True)
    b_all = jnp.sum(lf_col, axis=0, keepdims=True)
    after = jnp.sum(jnp.where(iota(1) > iota(0), lf_row, 0.0), axis=1, keepdims=True)
    weight = after + i_col
    top = jnp.max(weight, axis=0, keepdims=True)
    weight = jnp.exp(weight - top)
    kf = k.astype(F32) * HD**-0.5
    weighted = weight * kf
    hi = weighted.astype(BF)
    low = (weighted - hi.astype(F32)).astype(BF)
    across = (((0,), (0,)), ((), ()))
    memory = lax.dot_general(hi, v, across, preferred_element_type=F32)
    memory += lax.dot_general(low, v, across, preferred_element_type=F32)
    normer = jnp.sum(weighted, axis=0, keepdims=True)
    lane = lax.broadcasted_iota(jnp.int32, (1, N), 1)
    n_low = normer - normer.astype(BF).astype(F32)
    line = n_low[:, N:]
    for at, p in enumerate(pieces(b_all) + pieces(top)):
        line = jnp.where(lane == at, p.astype(F32), line)
    count, cut = message.shape[0], HD // message.shape[0]
    state[:, 0:cut, :] = memory[:, :N].reshape(count, cut, N)
    state[:, cut : 2 * cut, :] = memory[:, N:].reshape(count, cut, N)
    rest = jnp.concatenate([normer[:, :N], normer[:, N:], line, n_low[:, :N]], axis=0)
    state[:, 2 * cut :, :] = jnp.broadcast_to(rest[None], (count, 4, N))
    message[...] = state[...].astype(BF)
    aux[...] = jnp.concatenate([b_row, i_row, to_row(inv), jnp.zeros((5, N), F32)], axis=0)


def carry(place, arrived, message, own, state, back):
    count, rows, _ = arrived.shape
    slab = rows - 4
    state[...] = arrived[...].astype(F32)
    source = lax.broadcasted_iota(jnp.int32, (count, count), 1)
    target = lax.broadcasted_iota(jnp.int32, (count, count), 0)
    lines = state[:, slab + 2, :]
    tops = lines[:, 3:4] + lines[:, 4:5] + lines[:, 5:6]
    tops = jnp.sum(jnp.where(source == target, tops, 0.0), axis=0, keepdims=True)
    later = jnp.where(source < target, 1.0, 0.0)
    past = later.astype(BF)
    decay = jnp.zeros((count, count), F32)
    for p in range(3):
        decay += dot(past, (later * lines[:, p : p + 1]).astype(BF))
    logs = jnp.where(source < target, tops + decay, LOWEST)
    top = jnp.max(logs, axis=1, keepdims=True)
    weights = jnp.where(source < target, jnp.exp(logs - top), 0.0)
    hi = weights.astype(BF)
    low = (weights - hi.astype(F32)).astype(BF)
    mine = lax.broadcasted_iota(jnp.int32, (count, 1), 0) == place[0]
    pick = lambda a: jnp.sum(jnp.where(mine, a, 0.0), axis=0, keepdims=True)
    lines = []
    lane = lax.broadcasted_iota(jnp.int32, (1, N), 1)
    for r in range(rows):
        part = state[:, r, :]
        part = (jnp.where(lane < 6, 0.0, part) if r == slab + 2 else part).astype(BF)
        whole = dot(hi, part) + dot(low, part)
        if r < slab:
            back[:, r, :] = whole
        else:
            lines.append(pick(whole))
    message[...] = back[...].astype(BF)
    lines = [lines[0] + lines[3], lines[1] + lines[2], jnp.broadcast_to(pick(top), (1, N))]
    own[...] = jnp.concatenate(lines + [jnp.zeros((5, N), F32)], axis=0)


def inside(tok, aux, k_ref, v_ref, qw, ow, bw, cw, uw, gain, queries, numer, cols, gate, gate_b, mixed):
    groups, _, part = tok.shape
    sums = [jnp.zeros((N, w.shape[1]), F32) for w in (qw, ow, bw, cw, uw)]
    for g in range(groups):
        piece = tok[g, :N, :]
        at = pl.ds(g * part, part)
        sums = [s + dot(piece, w[at, :]) for s, w in zip(sums, (qw, ow, bw, cw, uw))]
    b_row, i_row = aux[0:1, :], aux[1:2, :]
    inv = to_col(aux[2:3, :])
    q, og, gb, gc, gu = [(inv * s).astype(BF) for s in sums]
    queries[...] = q
    gate_b[...] = gb
    mixed[...] = (gc.astype(F32) * gu.astype(F32)).astype(BF)
    gate[...] = jax.nn.sigmoid(og.astype(F32)) * gain[...].astype(F32).reshape(1, HD)
    b_col = to_col(b_row)
    causal = iota(1) <= iota(0)
    decays = jnp.where(causal, b_col - b_row + i_row, LOWEST)
    top = jnp.max(decays, axis=1, keepdims=True)
    weights = jnp.where(causal, jnp.exp(decays - top), 0.0)
    scores = lax.dot_general(q, k_ref[...], (((1,), (1,)), ((), ())), preferred_element_type=F32)
    scores = scores * HD**-0.5 * weights
    numer[...] = dot_two(scores, v_ref[...])
    denom = jnp.sum(scores, axis=1, keepdims=True)
    lane = iota(1)
    cols[...] = jnp.where(lane == 0, b_col, jnp.where(lane == 1, top, jnp.where(lane == 2, denom, 0.0)))


def convolve(halo, mixed, gate_b, taps, weight, out):
    now = mixed[...].astype(F32)
    prev = halo[...].astype(F32)
    row = iota(0)
    one = jnp.where(row == 0, prev[1:2], pltpu.roll(now, 1, 0))
    two = jnp.where(row == 0, prev[0:1], jnp.where(row == 1, prev[1:2], pltpu.roll(now, 2, 0)))
    t = taps[...].astype(F32)
    total = t[0:1] * two + t[1:2] * one + t[2:3] * now
    y = (gate_b[...].astype(F32) * total).astype(BF)
    count, rows, _ = out.shape
    done = dot(y, weight[...]).astype(BF)
    for g in range(count):
        out[g, :, :] = done[g * rows : (g + 1) * rows]


def finish(arrived, own, queries, numer, cols, gate, weight, out, state):
    _, rows, _ = arrived.shape
    half = rows // 2
    q = queries[...]
    state[...] = arrived[...].astype(F32)
    left = state[:, :half, :].reshape(HD, N).astype(BF)
    right = state[:, half:, :].reshape(HD, N).astype(BF)
    past = jnp.concatenate([dot(q, left), dot(q, right)], axis=1)
    qf = q.astype(F32)
    past_den = jnp.sum(qf[:, :N] * own[0:1, :] + qf[:, N:] * own[1:2, :], axis=1, keepdims=True)
    b_col, top, denom = cols[:, 0:1], cols[:, 1:2], cols[:, 2:3]
    inter = b_col + own[2:3, 0:1]
    most = jnp.maximum(inter, top)
    old, new = jnp.exp(inter - most), jnp.exp(top - most)
    den = old * past_den + new * denom
    raw = (old * past + new * numer[...]) / jnp.maximum(jnp.abs(den), jnp.exp(-most))
    squares = jnp.sum(raw * raw, axis=1, keepdims=True)
    y = (gate[...] * raw).astype(BF)
    done = dot(y, weight[...]).astype(BF)
    parts = [p.astype(F32) for p in pieces(squares)]
    lane = iota(1)
    tail = jnp.where(lane == 0, parts[0], jnp.where(lane == 1, parts[1], jnp.where(lane == 2, parts[2], 0.0)))
    tail = tail.astype(BF)
    groups, size, width = out.shape
    for g in range(groups):
        out[g, :, : width - N] = done[g * size : (g + 1) * size]
        out[g, :, width - N :] = tail[g * size : (g + 1) * size]


def gather_up(conv, mem, out):
    groups, _, width = conv.shape
    squares = jnp.zeros((conv.shape[1], 1), F32)
    for g in range(groups):
        tail = mem[g, :, width:].astype(F32)
        squares += tail[:, 0:1] + tail[:, 1:2] + tail[:, 2:3]
    scale = lax.rsqrt(squares / MDIM + EPS)
    c = jnp.zeros(conv.shape[1:], F32)
    m = jnp.zeros(conv.shape[1:], F32)
    for g in range(groups):
        c += conv[g].astype(F32)
        m += mem[g, :, :width].astype(F32)
    out[...] = (c + scale * m).astype(BF)


def exchange(value, axis):
    return lax.all_to_all(value, axis, split_axis=0, concat_axis=0, tiled=True)


def body(tokens, norm_gain, conv_b_w, conv_c_w, conv_u_w, conv_taps, query_w, key_w, value_w, outgate_w,
         gate_w, gate_bias, mem_gain, conv_out_w, mem_out_w):
    model = key_w.shape[0]
    count = lax.axis_size(SP)
    groups = lax.axis_size(TP)
    rows = 2 * HD // count
    (local,) = call(prepare, [((1, N + 16, tokens.shape[1]), BF)], tokens, norm_gain)
    tok = lax.all_gather(local, TP, axis=0, tiled=True)
    message, keys, values, aux = call(
        states,
        [((count, rows + 4, N), BF), ((N, HD), BF), ((N, HD), BF), ((8, N), F32)],
        tok, key_w, value_w, gate_w.reshape(model, 2).T, gate_bias.reshape(1, 2), flops=10**9,
        scratch=[pltpu.VMEM((count, rows + 4, N), F32)],
    )
    arrived = exchange(message, SP)
    queries, numer, cols, gate, gate_b, mixed = call(
        inside,
        [((N, HD), BF), ((N, HD), F32), ((N, N), F32), ((N, HD), F32), ((N, N), BF), ((N, N), BF)],
        tok, aux, keys, values, query_w, outgate_w, conv_b_w, conv_c_w, conv_u_w, mem_gain,
        flops=2 * 10**9,
    )
    halo = lax.ppermute(mixed[N - 2 :], SP, [(i, i + 1) for i in range(count - 1)])
    place = lax.axis_index(SP).reshape(1).astype(jnp.int32)
    vmem = pl.BlockSpec(memory_space=pltpu.VMEM)
    back, own = call(
        carry,
        [((count, rows, N), BF), ((8, N), F32)],
        place, arrived, flops=10**9,
        scratch=[pltpu.VMEM((count, rows + 4, N), F32), pltpu.VMEM((count, rows, N), F32)],
        specs=[pl.BlockSpec(memory_space=pltpu.SMEM), vmem],
    )
    state = exchange(back, SP)
    (conv,) = call(
        convolve, [((groups, N // groups, model), BF)], halo, mixed, gate_b, conv_taps, conv_out_w,
        flops=10**9,
    )
    conv = exchange(conv, TP)
    (mem,) = call(
        finish, [((groups, N // groups, model + N), BF)], state, own, queries, numer, cols, gate, mem_out_w,
        flops=10**9, scratch=[pltpu.VMEM((count, rows, N), F32)],
    )
    mem = exchange(mem, TP)
    (out,) = call(gather_up, [((N // groups, model), BF)], conv, mem)
    return out


def solution(mesh):
    sp = mesh.shape["sp"]
    finer = Mesh(mesh.devices.reshape(sp, mesh.shape["tp"]), ("sp", "tp"))
    cols = P(None, TP)
    in_specs = (
        P(SP, TP), cols, cols, cols, cols, cols, cols, cols, cols, cols,
        P(None, None, TP), cols, P(TP), P(TP, None), P(TP, None),
    )
    return jax.shard_map(body, mesh=finer, in_specs=in_specs, out_specs=P((SP, TP), None), check_vma=False)
```

time: 134 us -> 126 us (0.940)
  blocking collectives: 58 us -> 40.6 us
  Pallas kernels: 20.2 us -> 8.02 us
  waiting for transfers between devices: 20.3 us -> 31.3 us
  starting transfers between devices: 27.8 us -> 35.6 us
  local copies, waits for them, and re-layouts: 5.41 us -> 9.88 us
    all_to_all x2 -> x1, blocking collectives: 29.4 us -> 13.5 us  [exchange(): return lax.all_to_all(value, axis, split_axis=0, concat_axis=0, tiled=True)]
    all_to_all x3, waiting for transfers between devices: 19.6 us -> 30.6 us  [exchange(): return lax.all_to_all(value, axis, split_axis=0, concat_axis=0, tiled=True)]
    pallas_call x7, Pallas kernels: 18.2 us -> 8.02 us  [call(): pl.pallas_call(kernel, out_shape=[jax.ShapeDtypeStruct(s, d) for s, d in...]
    all_to_all x3, starting transfers between devices: 24.4 us -> 33 us  [exchange(): return lax.all_to_all(value, axis, split_axis=0, concat_axis=0, tiled=True)]
    unnamed x14 -> x38, local copies, waits for them, and re-layouts: 4.19 us -> 9.88 us
    pallas_call x1 -> x0, Pallas kernels: 2 us -> none  [body(): pl.pallas_call(prefixes, out_shape=[jax.ShapeDtypeStruct((ny, slices, N),...]
    all_gather x1, blocking collectives: 28.5 us -> 27.1 us  [body(): tok = lax.all_gather(local, TP, axis=0, tiled=True)]
  transfers between devices with their start and end apart: 4 -> 4, of which waited for: 3 -> 4; matrix products, arithmetic and copies ran while one was open for 1% -> 0% of each run, Pallas kernels for 7% -> 2%
where the time goes in v2:
time: 126 us
  blocking collectives  40.6 us (32%)
  starting transfers between devices  35.6 us (28%)
  waiting for transfers between devices  31.3 us (25%)
  local copies, waits for them, and re-layouts  9.88 us (8%)
  Pallas kernels  8.02 us (6%)
    all_to_all x3, starting transfers between devices, exchange(): return lax.all_to_all(value, axis, split_axis=0, concat_axis=0, tiled=True)  33 us
    all_to_all x3, waiting for transfers between devices, exchange(): return lax.all_to_all(value, axis, split_axis=0, concat_axis=0, tiled=True)  30.6 us
    all_gather x1, blocking collectives, body(): tok = lax.all_gather(local, TP, axis=0, tiled=True)  27.1 us
    all_to_all x1, blocking collectives, exchange(): return lax.all_to_all(value, axis, split_axis=0, concat_axis=0, tiled=True)  13.5 us
    unnamed x38, local copies, waits for them, and re-layouts  9.88 us
    pallas_call x7, Pallas kernels, call(): pl.pallas_call(kernel, out_shape=[jax.ShapeDtypeStruct(s, d) for s, d in...  8.02 us
    ppermute x1, starting transfers between devices, body(): lax.ppermute(mixed[N - 2:], SP, [(i, i + 1) for i in range(count - 1)])  2.61 us
  transfers between devices with their start and end apart: 4, of which 4 were waited for; matrix products, arithmetic and copies ran while one was open for 0% of the time, Pallas kernels for 2%

profile of v2, /device:TPU:1, one launch (start us, length us, event | category | flops | bytes accessed | tf_op | source)
XLA Modules:
  0.0 125.6 jit_solution(11625527116430736823)
XLA Ops:
  0.0 0.0 copy-start
  0.0 0.8 copy-done
  0.8 0.0 copy-start.1
  0.8 0.7 copy-done.1
  1.5 0.1 shard_map.145
  1.6 0.0 copy-start.11
  1.6 27.1 %all_gather.3.tok = bf16[8,144,256]{2,1,0:T(8,128)(2,1)S(1)} all-gather(bf16[1,144,256]{2,1,0:T(8,128)(2,1)S(1)} %shard_map.145), channel_id=1, replica_groups=mesh['sp'=128,'tp'=8] {'tp'}, dimensions={0}, use_global_device_ids=true | all-gather | bytes 663552 | tf_op jit(solution)/shard_map/all_gather | solution.py:268
  28.8 0.0 copy-done.11
  28.8 0.7 copy-done.13
  29.4 0.0 copy-start.2
  29.4 1.2 copy-done.2
  30.7 0.0 copy-start.3
  30.7 1.2 copy-done.3
  31.9 2.0 %shard_map.146 = (bf16[128,8,128]{2,1,0:T(8,128)(2,1)}, bf16[128,256]{1,0:T(8,128)(2,1)S(1)}, bf16[128,256]{1,0:T(8,128)(2,1)S(1)}, f32[8,128]{1,0:T(8,128)S(1)}) custom-call(bf16[8,144,256]{2,1,0:T(8,128)(2,1)S(1)} %all_gather.3.tok, bf16[2048,256]{1,0:T(8,128)(2,1)S(1)} %copy-done.2, bf16[2048,256]{1,0:T(8,128)(2,1)S(1)} %copy-done.3, ...), custom_call_target="tpu_custom_call" | custom-call | flops 1000000000 | bytes 1000000 | tf_op jit(solution)/shard_map/pallas_call | solution.py:24
  33.9 13.7 %all-to-all-start.1 = ((bf16[128,8,128]{2,1,0:T(8,128)(2,1)}), bf16[128,8,128]{2,1,0:T(8,128)(2,1)S(1)}, u32[]{:S(2)}, u32[]{:S(2)}) async-start(bf16[128,8,128]{2,1,0:T(8,128)(2,1)} %get-tuple-element.22), calls=%async_computation.1 | async-start | bytes 524288 | tf_op jit(solution)/shard_map/all_to_all | solution.py:258
  47.6 17.3 %all-to-all-done.1.arrived = bf16[128,8,128]{2,1,0:T(8,128)(2,1)S(1)} async-done(((bf16[128,8,128]{2,1,0:T(8,128)(2,1)}), bf16[128,8,128]{2,1,0:T(8,128)(2,1)S(1)}, u32[]{:S(2)}, u32[]{:S(2)}) %all-to-all-start.1) | async-done | bytes 262176 | tf_op jit(solution)/shard_map/all_to_all | solution.py:258
  64.9 0.0 copy-start.4
  64.9 0.0 copy-start.5
  64.9 2.2 %shard_map.149 = (bf16[128,4,128]{2,1,0:T(4,128)(2,1)}, f32[8,128]{1,0:T(8,128)S(1)}) custom-call(s32[1]{0:T(128)} %bitcast.3.place, bf16[128,8,128]{2,1,0:T(8,128)(2,1)S(1)} %all-to-all-done.1.arrived), custom_call_target="tpu_custom_call" | custom-call | flops 1000000000 | bytes 1000000 | tf_op jit(solution)/shard_map/pallas_call | solution.py:24
  67.1 12.4 %all-to-all-start.2 = ((bf16[128,4,128]{2,1,0:T(4,128)(2,1)}), bf16[128,4,128]{2,1,0:T(4,128)(2,1)S(1)}, u32[]{:S(2)}, u32[]{:S(2)}) async-start(bf16[128,4,128]{2,1,0:T(4,128)(2,1)} %get-tuple-element.23), calls=%async_computation.2 | async-start | bytes 262144 | tf_op jit(solution)/shard_map/all_to_all | solution.py:258
  79.5 0.0 copy-start.14
  79.5 0.0 copy-done.4
  79.5 0.0 copy-done.5
  79.5 0.6 copy-done.14
  80.2 0.0 copy-start.7
  80.2 1.0 copy-done.7
  81.2 0.0 copy-start.8
  81.2 1.0 copy-done.8
  82.2 1.0 copy-done.9
  83.3 1.1 shard_map.147
  84.4 0.0 copy-start.15
  84.4 0.6 copy-done.15
  85.1 2.6 %collective-permute-start = (bf16[2,128]{1,0:T(2,128)(2,1)S(1)}, bf16[2,128]{1,0:T(2,128)(2,1)S(1)}, u32[]{:S(2)}, u32[]{:S(2)}) collective-permute-start(bf16[2,128]{1,0:T(2,128)(2,1)S(1)} %slice.3), channel_id=1, source_target_pairs={{0,8},{8,16},{16,24},{24,32},{32,40},{40,48},{48,56},{56,64},{64,7... | collective-permute-start | bytes 1544 | tf_op jit(solution)/shard_map/ppermute | solution.py:282
  87.7 0.7 collective-permute-done.halo
  88.4 0.0 copy-done.10
  88.4 0.0 copy-done.12
  88.4 1.1 shard_map.148
  89.5 0.0 copy-done.17
  89.5 5.5 %all-to-all-done.2.arrived = bf16[128,4,128]{2,1,0:T(4,128)(2,1)S(1)} async-done(((bf16[128,4,128]{2,1,0:T(4,128)(2,1)}), bf16[128,4,128]{2,1,0:T(4,128)(2,1)S(1)}, u32[]{:S(2)}, u32[]{:S(2)}) %all-to-all-start.2) | async-done | bytes 131104 | tf_op jit(solution)/shard_map/all_to_all | solution.py:258
  95.0 6.9 %all-to-all-start = ((bf16[8,16,2048]{2,1,0:T(8,128)(2,1)}), bf16[8,16,2048]{2,1,0:T(8,128)(2,1)S(1)}, u32[]{:S(2)}, u32[]{:S(2)}) async-start(bf16[8,16,2048]{2,1,0:T(8,128)(2,1)} %shard_map.148), calls=%async_computation | async-start | bytes 1048576 | tf_op jit(solution)/shard_map/all_to_all | solution.py:258
  101.9 0.0 copy-done.16
  101.9 0.0 copy-done.6
  101.9 0.0 copy-start.18
  101.9 0.8 copy-done.18
  102.8 0.7 shard_map.150
  103.4 7.8 %all-to-all-done.conv = bf16[8,16,2048]{2,1,0:T(8,128)(2,1)S(1)} async-done(((bf16[8,16,2048]{2,1,0:T(8,128)(2,1)}), bf16[8,16,2048]{2,1,0:T(8,128)(2,1)S(1)}, u32[]{:S(2)}, u32[]{:S(2)}) %all-to-all-start) | async-done | bytes 524320 | tf_op jit(solution)/shard_map/all_to_all | solution.py:258
  111.3 13.5 %all_to_all.20.mem = bf16[8,16,2176]{2,1,0:T(8,128)(2,1)S(1)} all-to-all(bf16[8,16,2176]{2,1,0:T(8,128)(2,1)S(1)} %shard_map.150), channel_id=1, replica_groups=mesh['sp'=128,'tp'=8] {'tp'}, dimensions={0} | all-to-all | bytes 1114112 | tf_op jit(solution)/shard_map/all_to_all | solution.py:258
  124.8 0.8 shard_map.151
  (8 shorter events, 0.0 us)
Async XLA Ops:
  0.0 0.8 copy-start
  0.8 0.7 copy-start.1
  1.6 27.1 %copy-start.11 = (bf16[2048,2,1]{0,1,2:T(2,128)(2,1)S(1)}, bf16[2048,2,1]{0,1,2:T(2,128)(2,1)}, u32[]{:S(2)}) copy-start(bf16[2048,2,1]{0,1,2:T(2,128)(2,1)} %param.25) | copy-start | bytes 24580
  28.8 0.7 copy-start.13
  29.4 1.2 copy-start.2
  30.7 1.2 copy-start.3
  33.9 31.0 %all-to-all-start.1 = ((bf16[128,8,128]{2,1,0:T(8,128)(2,1)}), bf16[128,8,128]{2,1,0:T(8,128)(2,1)S(1)}, u32[]{:S(2)}, u32[]{:S(2)}) async-start(bf16[128,8,128]{2,1,0:T(8,128)(2,1)} %get-tuple-element.22), calls=%async_computation.1 | async-start | bytes 524288 | tf_op jit(solution)/shard_map/all_to_all | solution.py:258
  64.9 14.6 %copy-start.4 = (bf16[2048,256]{1,0:T(8,128)(2,1)S(1)}, bf16[2048,256]{1,0:T(8,128)(2,1)}, u32[]{:S(2)}) copy-start(bf16[2048,256]{1,0:T(8,128)(2,1)} %qw.1) | copy-start | bytes 3145732
  64.9 14.6 %copy-start.5 = (bf16[2048,256]{1,0:T(8,128)(2,1)S(1)}, bf16[2048,256]{1,0:T(8,128)(2,1)}, u32[]{:S(2)}) copy-start(bf16[2048,256]{1,0:T(8,128)(2,1)} %ow.1) | copy-start | bytes 3145732
  67.1 27.9 %all-to-all-start.2 = ((bf16[128,4,128]{2,1,0:T(4,128)(2,1)}), bf16[128,4,128]{2,1,0:T(4,128)(2,1)S(1)}, u32[]{:S(2)}, u32[]{:S(2)}) async-start(bf16[128,4,128]{2,1,0:T(4,128)(2,1)} %get-tuple-element.23), calls=%async_computation.2 | async-start | bytes 262144 | tf_op jit(solution)/shard_map/all_to_all | solution.py:258
  79.5 0.7 copy-start.14
  80.2 1.0 copy-start.7
  81.2 1.0 copy-start.8
  82.2 1.0 copy-start.9
  83.3 5.1 %copy-start.10 = (bf16[128,2048]{1,0:T(8,128)(2,1)S(1)}, bf16[128,2048]{1,0:T(8,128)(2,1)}, u32[]{:S(2)}) copy-start(bf16[128,2048]{1,0:T(8,128)(2,1)} %weight.2) | copy-start | bytes 1572868
  84.4 0.7 copy-start.15
  85.1 4.4 %copy-start.17 = (f32[128,128]{1,0:T(8,128)}, f32[128,128]{1,0:T(8,128)S(1)}, u32[]{:S(2)}) copy-start(f32[128,128]{1,0:T(8,128)S(1)} %get-tuple-element.27.cols) | copy-start | bytes 196612
  85.1 3.3 %copy-start.12 = (bf16[3,128]{1,0:T(4,128)(2,1)S(1)}, bf16[3,128]{1,0:T(4,128)(2,1)}, u32[]{:S(2)}) copy-start(bf16[3,128]{1,0:T(4,128)(2,1)} %taps.1) | copy-start | bytes 2308
  85.1 3.3 %collective-permute-start = (bf16[2,128]{1,0:T(2,128)(2,1)S(1)}, bf16[2,128]{1,0:T(2,128)(2,1)S(1)}, u32[]{:S(2)}, u32[]{:S(2)}) collective-permute-start(bf16[2,128]{1,0:T(2,128)(2,1)S(1)} %slice.3), channel_id=1, source_target_pairs={{0,8},{8,16},{16,24},{24,32},{32,40},{40,48},{48,56},{56,64},{64,7... | collective-permute-start | bytes 1544 | tf_op jit(solution)/shard_map/ppermute | solution.py:282
  88.4 13.5 %copy-start.16 = (f32[128,256]{1,0:T(8,128)S(1)}, f32[128,256]{1,0:T(8,128)}, u32[]{:S(2)}) copy-start(f32[128,256]{1,0:T(8,128)} %copy-done.15) | copy-start | bytes 393220
  89.5 12.4 %copy-start.6 = (bf16[256,2048]{1,0:T(8,128)(2,1)S(1)}, bf16[256,2048]{1,0:T(8,128)(2,1)}, u32[]{:S(2)}) copy-start(bf16[256,2048]{1,0:T(8,128)(2,1)} %weight.3) | copy-start | bytes 3145732
  95.0 16.3 %all-to-all-start = ((bf16[8,16,2048]{2,1,0:T(8,128)(2,1)}), bf16[8,16,2048]{2,1,0:T(8,128)(2,1)S(1)}, u32[]{:S(2)}, u32[]{:S(2)}) async-start(bf16[8,16,2048]{2,1,0:T(8,128)(2,1)} %shard_map.148), calls=%async_computation | async-start | bytes 1048576 | tf_op jit(solution)/shard_map/all_to_all | solution.py:258
  101.9 0.8 copy-start.18

commit v3 on v2

--- a/solution.py
+++ b/solution.py
@@ -11,6 +11,7 @@
 HD = 256
 MDIM = 2048
 EPS = 1e-06
+CHUNKS = 4
 LOWEST = -1e30
 TP = "tp"
 SP = "sp"
@@ -61,7 +62,16 @@
     return dot(hi, b) + dot((a - hi.astype(F32)).astype(BF), b)
 
 
-def prepare(tok, gain, out):
+def fetched(pairs, sems):
+    copies = [pltpu.make_async_copy(src, dst, sems.at[at]) for at, (src, dst) in enumerate(pairs)]
+    for c in copies:
+        c.start()
+    return copies
+
+
+def prepare(tok_hbm, gain_hbm, out, tok, gain, sems):
+    for c in fetched([(tok_hbm, tok), (gain_hbm, gain)], sems):
+        c.wait()
     wide = tok[...].astype(F32)
     out[0, :N, :] = (wide * gain[...].astype(F32)).astype(BF)
     squares = to_row(jnp.sum(wide * wide, axis=1, keepdims=True))
@@ -72,31 +82,43 @@
     out[0, N:, N:] = jnp.zeros((16, N), BF)
 
 
+def products(tok, sources, places, sems):
+    groups, _, part = tok.shape
+    step = groups * part // CHUNKS
+    cut = [pl.ds(c * step, step) for c in range(CHUNKS)]
+    copies = fetched([(s.at[at, :], p.at[at, :]) for at in cut for s, p in zip(sources, places)], sems)
+    sums = [jnp.zeros((N, p.shape[1]), F32) for p in places]
+    for c in range(CHUNKS):
+        for each in copies[c * len(places) : (c + 1) * len(places)]:
+            each.wait()
+        for g in range(c * groups // CHUNKS, (c + 1) * groups // CHUNKS):
+            piece = tok[g, :N, :]
+            at = pl.ds(g * part, part)
+            sums = [s + dot(piece, p[at, :]) for s, p in zip(sums, places)]
+    return sums
+
+
 def log_sigmoid(x):
     e = jnp.exp(-jnp.abs(x))
     series = e * (1.0 - e * (0.5 - e * (1.0 / 3.0 - e * 0.25)))
     return -(jnp.maximum(-x, 0.0) + jnp.where(e < 0.01, series, jnp.log(1.0 + e)))
 
 
-def states(tok, kw, vw, gw, bias, message, keys, values, aux, state):
+def states(tok, kw_hbm, vw_hbm, gw, bias, message, kv, aux, state, kw, vw, sems):
     groups, _, part = tok.shape
-    k_sum = jnp.zeros((N, HD), F32)
-    v_sum = jnp.zeros((N, HD), F32)
+    k_sum, v_sum = products(tok, (kw_hbm, vw_hbm), (kw, vw), sems)
     g_sum = jnp.zeros((N, 2), F32)
     sq = jnp.zeros((1, N), F32)
     for g in range(groups):
-        piece = tok[g, :N, :]
         at = pl.ds(g * part, part)
-        k_sum += dot(piece, kw[at, :])
-        v_sum += dot(piece, vw[at, :])
-        g_sum += lax.dot_general(piece, gw[:, at], (((1,), (1,)), ((), ())), preferred_element_type=F32)
+        g_sum += lax.dot_general(tok[g, :N, :], gw[:, at], (((1,), (1,)), ((), ())), preferred_element_type=F32)
         tail = tok[g, N:, :N].astype(F32)
         sq += tail[0:1] + tail[1:2] + tail[2:3]
     inv = lax.rsqrt(to_col(sq) / (groups * part) + EPS)
     k = (inv * k_sum).astype(BF)
     v = (inv * v_sum).astype(BF)
-    keys[...] = k
-    values[...] = v
+    kv[:, :HD] = k
+    kv[:, HD:] = v
     gates = inv * g_sum
     i_col = gates[:, 0:1] + bias[0:1, 0:1]
     lf_col = log_sigmoid(gates[:, 1:2] + bias[0:1, 1:2])
@@ -168,31 +190,26 @@
     own[...] = jnp.concatenate(lines + [jnp.zeros((5, N), F32)], axis=0)
 
 
-def inside(tok, aux, k_ref, v_ref, qw, ow, bw, cw, uw, gain, queries, numer, cols, gate, gate_b, mixed):
-    groups, _, part = tok.shape
-    sums = [jnp.zeros((N, w.shape[1]), F32) for w in (qw, ow, bw, cw, uw)]
-    for g in range(groups):
-        piece = tok[g, :N, :]
-        at = pl.ds(g * part, part)
-        sums = [s + dot(piece, w[at, :]) for s, w in zip(sums, (qw, ow, bw, cw, uw))]
+def inside(tok, aux, kv, qw_hbm, ow_hbm, bw_hbm, cw_hbm, uw_hbm, gain, pack, gate_b, mixed, qw, ow, bw, cw, uw, sems):
+    sums = products(tok, (qw_hbm, ow_hbm, bw_hbm, cw_hbm, uw_hbm), (qw, ow, bw, cw, uw), sems)
     b_row, i_row = aux[0:1, :], aux[1:2, :]
     inv = to_col(aux[2:3, :])
     q, og, gb, gc, gu = [(inv * s).astype(BF) for s in sums]
-    queries[...] = q
+    pack[:, :HD] = q.astype(F32)
     gate_b[...] = gb
     mixed[...] = (gc.astype(F32) * gu.astype(F32)).astype(BF)
-    gate[...] = jax.nn.sigmoid(og.astype(F32)) * gain[...].astype(F32).reshape(1, HD)
+    pack[:, 2 * HD : 3 * HD] = jax.nn.sigmoid(og.astype(F32)) * gain[...].astype(F32).reshape(1, HD)
     b_col = to_col(b_row)
     causal = iota(1) <= iota(0)
     decays = jnp.where(causal, b_col - b_row + i_row, LOWEST)
     top = jnp.max(decays, axis=1, keepdims=True)
     weights = jnp.where(causal, jnp.exp(decays - top), 0.0)
-    scores = lax.dot_general(q, k_ref[...], (((1,), (1,)), ((), ())), preferred_element_type=F32)
+    scores = lax.dot_general(q, kv[:, :HD], (((1,), (1,)), ((), ())), preferred_element_type=F32)
     scores = scores * HD**-0.5 * weights
-    numer[...] = dot_two(scores, v_ref[...])
+    pack[:, HD : 2 * HD] = dot_two(scores, kv[:, HD:])
     denom = jnp.sum(scores, axis=1, keepdims=True)
     lane = iota(1)
-    cols[...] = jnp.where(lane == 0, b_col, jnp.where(lane == 1, top, jnp.where(lane == 2, denom, 0.0)))
+    pack[:, 3 * HD :] = jnp.where(lane == 0, b_col, jnp.where(lane == 1, top, jnp.where(lane == 2, denom, 0.0)))
 
 
 def convolve(halo, mixed, gate_b, taps, weight, out):
@@ -204,53 +221,54 @@
     t = taps[...].astype(F32)
     total = t[0:1] * two + t[1:2] * one + t[2:3] * now
     y = (gate_b[...].astype(F32) * total).astype(BF)
-    count, rows, _ = out.shape
-    done = dot(y, weight[...]).astype(BF)
-    for g in range(count):
-        out[g, :, :] = done[g * rows : (g + 1) * rows]
-
-
-def finish(arrived, own, queries, numer, cols, gate, weight, out, state):
+    out[...] = dot(y, weight[...]).astype(BF)
+
+
+def finish(arrived, own, pack, conv, weight, out, state):
     _, rows, _ = arrived.shape
     half = rows // 2
-    q = queries[...]
+    q = pack[:, :HD].astype(BF)
     state[...] = arrived[...].astype(F32)
     left = state[:, :half, :].reshape(HD, N).astype(BF)
     right = state[:, half:, :].reshape(HD, N).astype(BF)
     past = jnp.concatenate([dot(q, left), dot(q, right)], axis=1)
-    qf = q.astype(F32)
-    past_den = jnp.sum(qf[:, :N] * own[0:1, :] + qf[:, N:] * own[1:2, :], axis=1, keepdims=True)
+    past_den = jnp.sum(pack[:, :N] * own[0:1, :] + pack[:, N:HD] * own[1:2, :], axis=1, keepdims=True)
+    cols = pack[:, 3 * HD :]
     b_col, top, denom = cols[:, 0:1], cols[:, 1:2], cols[:, 2:3]
     inter = b_col + own[2:3, 0:1]
     most = jnp.maximum(inter, top)
     old, new = jnp.exp(inter - most), jnp.exp(top - most)
     den = old * past_den + new * denom
-    raw = (old * past + new * numer[...]) / jnp.maximum(jnp.abs(den), jnp.exp(-most))
+    raw = (old * past + new * pack[:, HD : 2 * HD]) / jnp.maximum(jnp.abs(den), jnp.exp(-most))
     squares = jnp.sum(raw * raw, axis=1, keepdims=True)
-    y = (gate[...] * raw).astype(BF)
+    y = (pack[:, 2 * HD : 3 * HD] * raw).astype(BF)
     done = dot(y, weight[...]).astype(BF)
     parts = [p.astype(F32) for p in pieces(squares)]
     lane = iota(1)
     tail = jnp.where(lane == 0, parts[0], jnp.where(lane == 1, parts[1], jnp.where(lane == 2, parts[2], 0.0)))
     tail = tail.astype(BF)
-    groups, size, width = out.shape
+    groups, size, _ = out.shape
+    width = weight.shape[1]
     for g in range(groups):
-        out[g, :, : width - N] = done[g * size : (g + 1) * size]
-        out[g, :, width - N :] = tail[g * size : (g + 1) * size]
-
-
-def gather_up(conv, mem, out):
-    groups, _, width = conv.shape
-    squares = jnp.zeros((conv.shape[1], 1), F32)
+        at = slice(g * size, (g + 1) * size)
+        out[g, :, :width] = done[at]
+        out[g, :, width : 2 * width] = conv[at]
+        out[g, :, 2 * width :] = tail[at]
+
+
+def gather_up(arrived, out):
+    groups, size, width = arrived.shape
+    width = (width - N) // 2
+    squares = jnp.zeros((size, 1), F32)
     for g in range(groups):
-        tail = mem[g, :, width:].astype(F32)
+        tail = arrived[g, :, 2 * width :].astype(F32)
         squares += tail[:, 0:1] + tail[:, 1:2] + tail[:, 2:3]
     scale = lax.rsqrt(squares / MDIM + EPS)
-    c = jnp.zeros(conv.shape[1:], F32)
-    m = jnp.zeros(conv.shape[1:], F32)
+    c = jnp.zeros((size, width), F32)
+    m = jnp.zeros((size, width), F32)
     for g in range(groups):
-        c += conv[g].astype(F32)
-        m += mem[g, :, :width].astype(F32)
+        m += arrived[g, :, :width].astype(F32)
+        c += arrived[g, :, width : 2 * width].astype(F32)
     out[...] = (c + scale * m).astype(BF)
 
 
@@ -264,24 +282,32 @@
     count = lax.axis_size(SP)
     groups = lax.axis_size(TP)
     rows = 2 * HD // count
-    (local,) = call(prepare, [((1, N + 16, tokens.shape[1]), BF)], tokens, norm_gain)
+    vmem, hbm = pl.BlockSpec(memory_space=pltpu.VMEM), pl.BlockSpec(memory_space=pltpu.HBM)
+    room = lambda *arrays: [pltpu.VMEM(a.shape, a.dtype) for a in arrays]
+    sems = lambda n: [pltpu.SemaphoreType.DMA((n,))]
+    (local,) = call(
+        prepare, [((1, N + 16, tokens.shape[1]), BF)], tokens, norm_gain,
+        specs=[hbm, hbm], scratch=room(tokens, norm_gain) + sems(2),
+    )
     tok = lax.all_gather(local, TP, axis=0, tiled=True)
-    message, keys, values, aux = call(
+    message, kv, aux = call(
         states,
-        [((count, rows + 4, N), BF), ((N, HD), BF), ((N, HD), BF), ((8, N), F32)],
-        tok, key_w, value_w, gate_w.reshape(model, 2).T, gate_bias.reshape(1, 2), flops=10**9,
-        scratch=[pltpu.VMEM((count, rows + 4, N), F32)],
+        [((count, rows + 4, N), BF), ((N, 2 * HD), BF), ((8, N), F32)],
+        tok, key_w, value_w, gate_w.reshape(model, 2).T, gate_bias.reshape(1, 2), flops=10**9, limit=52,
+        scratch=[pltpu.VMEM((count, rows + 4, N), F32)] + room(key_w, value_w) + sems(2 * CHUNKS),
+        specs=[vmem, hbm, hbm, vmem, vmem],
     )
     arrived = exchange(message, SP)
-    queries, numer, cols, gate, gate_b, mixed = call(
+    others = (query_w, outgate_w, conv_b_w, conv_c_w, conv_u_w)
+    pack, gate_b, mixed = call(
         inside,
-        [((N, HD), BF), ((N, HD), F32), ((N, N), F32), ((N, HD), F32), ((N, N), BF), ((N, N), BF)],
-        tok, aux, keys, values, query_w, outgate_w, conv_b_w, conv_c_w, conv_u_w, mem_gain,
-        flops=2 * 10**9,
+        [((N, 3 * HD + N), F32), ((N, N), BF), ((N, N), BF)],
+        tok, aux, kv, *others, mem_gain, flops=2 * 10**9, limit=53,
+        scratch=room(*others) + sems(5 * CHUNKS), specs=[vmem] * 3 + [hbm] * 5 + [vmem],
     )
     halo = lax.ppermute(mixed[N - 2 :], SP, [(i, i + 1) for i in range(count - 1)])
+    (conv,) = call(convolve, [((N, model), BF)], halo, mixed, gate_b, conv_taps, conv_out_w, flops=10**9)
     place = lax.axis_index(SP).reshape(1).astype(jnp.int32)
-    vmem = pl.BlockSpec(memory_space=pltpu.VMEM)
     back, own = call(
         carry,
         [((count, rows, N), BF), ((8, N), F32)],
@@ -290,17 +316,12 @@
         specs=[pl.BlockSpec(memory_space=pltpu.SMEM), vmem],
     )
     state = exchange(back, SP)
-    (conv,) = call(
-        convolve, [((groups, N // groups, model), BF)], halo, mixed, gate_b, conv_taps, conv_out_w,
-        flops=10**9,
-    )
-    conv = exchange(conv, TP)
     (mem,) = call(
-        finish, [((groups, N // groups, model + N), BF)], state, own, queries, numer, cols, gate, mem_out_w,
+        finish, [((groups, N // groups, 2 * model + N), BF)], state, own, pack, conv, mem_out_w,
         flops=10**9, scratch=[pltpu.VMEM((count, rows, N), F32)],
     )
     mem = exchange(mem, TP)
-    (out,) = call(gather_up, [((N // groups, model), BF)], conv, mem)
+    (out,) = call(gather_up, [((N // groups, model), BF)], mem)
     return out
 
 

time: 126 us -> 119 us (0.944)
  blocking collectives: 40.6 us -> 49.6 us
  starting transfers between devices: 35.6 us -> 28.6 us
  local copies, waits for them, and re-layouts: 9.88 us -> 2.9 us
  waiting for transfers between devices: 31.3 us -> 25.9 us
  Pallas kernels: 8.02 us -> 11.7 us
    all_to_all x1, blocking collectives: 13.5 us -> 22.5 us  [exchange(): return lax.all_to_all(value, axis, split_axis=0, concat_axis=0, tiled=True)]
    unnamed x38 -> x18, local copies, waits for them, and re-layouts: 9.88 us -> 2.89 us
    all_to_all x3 -> x2, starting transfers between devices: 33 us -> 26.1 us  [exchange(): return lax.all_to_all(value, axis, split_axis=0, concat_axis=0, tiled=True)]
    all_to_all x3 -> x2, waiting for transfers between devices: 30.6 us -> 25.2 us  [exchange(): return lax.all_to_all(value, axis, split_axis=0, concat_axis=0, tiled=True)]
    pallas_call x7, Pallas kernels: 8.02 us -> 11.7 us  [call(): pl.pallas_call(kernel, out_shape=[jax.ShapeDtypeStruct(s, d) for s, d in...]
  transfers between devices with their start and end apart: 4 -> 3, of which waited for: 4 -> 3; matrix products, arithmetic and copies ran while one was open for 0% -> 0% of each run, Pallas kernels for 2% -> 4%
where the time goes in v3:
time: 119 us
  blocking collectives  49.6 us (42%)
  starting transfers between devices  28.6 us (24%)
  waiting for transfers between devices  25.9 us (22%)
  Pallas kernels  11.7 us (10%)
  local copies, waits for them, and re-layouts  2.9 us (2%)
    all_gather x1, blocking collectives, body(): tok = lax.all_gather(local, TP, axis=0, tiled=True)  27.1 us
    all_to_all x2, starting transfers between devices, exchange(): return lax.all_to_all(value, axis, split_axis=0, concat_axis=0, tiled=True)  26.1 us
    all_to_all x2, waiting for transfers between devices, exchange(): return lax.all_to_all(value, axis, split_axis=0, concat_axis=0, tiled=True)  25.2 us
    all_to_all x1, blocking collectives, exchange(): return lax.all_to_all(value, axis, split_axis=0, concat_axis=0, tiled=True)  22.5 us
    pallas_call x7, Pallas kernels, call(): pl.pallas_call(kernel, out_shape=[jax.ShapeDtypeStruct(s, d) for s, d in...  11.7 us
    unnamed x18, local copies, waits for them, and re-layouts  2.89 us
    ppermute x1, starting transfers between devices, body(): lax.ppermute(mixed[N - 2:], SP, [(i, i + 1) for i in range(count - 1)])  2.47 us
  transfers between devices with their start and end apart: 3, of which 3 were waited for; matrix products, arithmetic and copies ran while one was open for 0% of the time, Pallas kernels for 4%

profile of v3, /device:TPU:1, one launch (start us, length us, event | category | flops | bytes accessed | tf_op | source)
XLA Modules:
  0.0 118.7 jit_solution(11233920311352095758)
XLA Ops:
  0.0 0.0 copy-start.1
  0.0 0.8 copy-done.1
  0.8 0.0 copy-start.2
  0.8 0.7 copy-done.2
  1.5 0.2 shard_map.145
  1.7 27.1 %all_gather.3.tok = bf16[8,144,256]{2,1,0:T(8,128)(2,1)S(1)} all-gather(bf16[1,144,256]{2,1,0:T(8,128)(2,1)S(1)} %shard_map.145), channel_id=1, replica_groups=mesh['sp'=128,'tp'=8] {'tp'}, dimensions={0}, use_global_device_ids=true | all-gather | bytes 663552 | tf_op jit(solution)/shard_map/all_gather | solution.py:292
  28.8 0.0 copy-start
  28.8 0.0 copy-start.5
  28.8 0.7 copy-done.5
  29.5 0.0 copy-start.7
  29.5 0.7 copy-done.7
  30.2 3.5 %shard_map.146 = (bf16[128,8,128]{2,1,0:T(8,128)(2,1)}, bf16[128,512]{1,0:T(8,128)(2,1)S(1)}, f32[8,128]{1,0:T(8,128)S(1)}) custom-call(bf16[8,144,256]{2,1,0:T(8,128)(2,1)S(1)} %all_gather.3.tok, bf16[2048,256]{1,0:T(8,128)(2,1)} %kw_hbm.1, bf16[2048,256]{1,0:T(8,128)(2,1)} %vw_hbm.1, bf16[2,2048]{1,0:T(2,128)(2,1)S(1)} %bitcast.5, f32[1,2]{1,0:T(1,128)S(1)} %bitcast.6), custom_call_target="tpu_custom_call" | custom-call | flops 1000000000 | bytes 1000000 | tf_op jit(solution)/shard_map/pallas_call | solution.py:25
  33.7 0.0 copy-done
  33.7 13.7 %all-to-all-start = ((bf16[128,8,128]{2,1,0:T(8,128)(2,1)}), bf16[128,8,128]{2,1,0:T(8,128)(2,1)S(1)}, u32[]{:S(2)}, u32[]{:S(2)}) async-start(bf16[128,8,128]{2,1,0:T(8,128)(2,1)} %get-tuple-element.13), calls=%async_computation | async-start | bytes 524288 | tf_op jit(solution)/shard_map/all_to_all | solution.py:276
  47.4 17.3 %all-to-all-done.arrived = bf16[128,8,128]{2,1,0:T(8,128)(2,1)S(1)} async-done(((bf16[128,8,128]{2,1,0:T(8,128)(2,1)}), bf16[128,8,128]{2,1,0:T(8,128)(2,1)S(1)}, u32[]{:S(2)}, u32[]{:S(2)}) %all-to-all-start) | async-done | bytes 262176 | tf_op jit(solution)/shard_map/all_to_all | solution.py:276
  64.7 0.0 copy-start.8
  64.7 2.2 %shard_map.147 = (bf16[128,4,128]{2,1,0:T(4,128)(2,1)}, f32[8,128]{1,0:T(8,128)S(1)}) custom-call(s32[1]{0:T(128)} %bitcast.place, bf16[128,8,128]{2,1,0:T(8,128)(2,1)S(1)} %all-to-all-done.arrived), custom_call_target="tpu_custom_call" | custom-call | flops 1000000000 | bytes 1000000 | tf_op jit(solution)/shard_map/pallas_call | solution.py:25
  66.9 12.4 %all-to-all-start.1 = ((bf16[128,4,128]{2,1,0:T(4,128)(2,1)}), bf16[128,4,128]{2,1,0:T(4,128)(2,1)S(1)}, u32[]{:S(2)}, u32[]{:S(2)}) async-start(bf16[128,4,128]{2,1,0:T(4,128)(2,1)} %get-tuple-element.14), calls=%async_computation.1 | async-start | bytes 262144 | tf_op jit(solution)/shard_map/all_to_all | solution.py:276
  79.3 0.0 copy-done.8
  79.3 0.0 copy-start.4
  79.3 0.0 copy-start.6
  79.3 4.1 %shard_map.148 = (f32[128,896]{1,0:T(8,128)S(1)}, bf16[128,128]{1,0:T(8,128)(2,1)S(1)}, bf16[128,128]{1,0:T(8,128)(2,1)S(1)}) custom-call(bf16[8,144,256]{2,1,0:T(8,128)(2,1)} %copy-done, f32[8,128]{1,0:T(8,128)S(1)} %get-tuple-element.16.aux, bf16[128,512]{1,0:T(8,128)(2,1)S(1)} %get-tuple-element.17.kv, bf16[2048,256]{1,0:T(8,128)(2,1)} %qw_hbm.1, ...), custom_call_target="tpu_custom_call" | custom-call | flops 2000000000 | bytes 2000000 | tf_op jit(solution)/shard_map/pallas_call | solution.py:25
  83.4 2.5 %collective-permute-start = (bf16[2,128]{1,0:T(2,128)(2,1)S(1)}, bf16[2,128]{1,0:T(2,128)(2,1)S(1)}, u32[]{:S(2)}, u32[]{:S(2)}) collective-permute-start(bf16[2,128]{1,0:T(2,128)(2,1)S(1)} %slice.3), channel_id=1, source_target_pairs={{0,8},{8,16},{16,24},{24,32},{32,40},{40,48},{48,56},{56,64},{64,7... | collective-permute-start | bytes 1544 | tf_op jit(solution)/shard_map/ppermute | solution.py:308
  85.9 0.7 collective-permute-done.halo
  86.6 0.0 copy-done.4
  86.6 0.0 copy-done.6
  86.6 0.0 copy-start.3
  86.6 0.3 shard_map.149.conv
  86.9 7.9 %all-to-all-done.1.arrived = bf16[128,4,128]{2,1,0:T(4,128)(2,1)S(1)} async-done(((bf16[128,4,128]{2,1,0:T(4,128)(2,1)}), bf16[128,4,128]{2,1,0:T(4,128)(2,1)S(1)}, u32[]{:S(2)}, u32[]{:S(2)}) %all-to-all-start.1) | async-done | bytes 131104 | tf_op jit(solution)/shard_map/all_to_all | solution.py:276
  94.8 0.0 copy-done.3
  94.8 0.7 shard_map.150
  95.4 22.5 %all_to_all.15.arrived = bf16[8,16,4224]{2,1,0:T(8,128)(2,1)S(1)} all-to-all(bf16[8,16,4224]{2,1,0:T(8,128)(2,1)S(1)} %shard_map.150), channel_id=1, replica_groups=mesh['sp'=128,'tp'=8] {'tp'}, dimensions={0} | all-to-all | bytes 2162688 | tf_op jit(solution)/shard_map/all_to_all | solution.py:276
  117.9 0.8 shard_map.151
  (1 shorter events, 0.0 us)
Async XLA Ops:
  0.0 0.8 copy-start.1
  0.8 0.7 copy-start.2
  28.8 4.8 %copy-start = (bf16[8,144,256]{2,1,0:T(8,128)(2,1)}, bf16[8,144,256]{2,1,0:T(8,128)(2,1)S(1)}, u32[]{:S(2)}) copy-start(bf16[8,144,256]{2,1,0:T(8,128)(2,1)S(1)} %all_gather.3.tok) | copy-start | bytes 1769476
  28.8 0.7 copy-start.5
  29.5 0.7 copy-start.7
  33.7 31.0 %all-to-all-start = ((bf16[128,8,128]{2,1,0:T(8,128)(2,1)}), bf16[128,8,128]{2,1,0:T(8,128)(2,1)S(1)}, u32[]{:S(2)}, u32[]{:S(2)}) async-start(bf16[128,8,128]{2,1,0:T(8,128)(2,1)} %get-tuple-element.13), calls=%async_computation | async-start | bytes 524288 | tf_op jit(solution)/shard_map/all_to_all | solution.py:276
  64.7 14.6 %copy-start.8 = (bf16[256]{0:T(256)(128)(2,1)S(1)}, bf16[256]{0:T(256)(128)(2,1)}, u32[]{:S(2)}) copy-start(bf16[256]{0:T(256)(128)(2,1)} %gain.1) | copy-start | bytes 1540
  66.9 27.9 %all-to-all-start.1 = ((bf16[128,4,128]{2,1,0:T(4,128)(2,1)}), bf16[128,4,128]{2,1,0:T(4,128)(2,1)S(1)}, u32[]{:S(2)}, u32[]{:S(2)}) async-start(bf16[128,4,128]{2,1,0:T(4,128)(2,1)} %get-tuple-element.14), calls=%async_computation.1 | async-start | bytes 262144 | tf_op jit(solution)/shard_map/all_to_all | solution.py:276
  79.3 7.3 %copy-start.4 = (bf16[128,2048]{1,0:T(8,128)(2,1)S(1)}, bf16[128,2048]{1,0:T(8,128)(2,1)}, u32[]{:S(2)}) copy-start(bf16[128,2048]{1,0:T(8,128)(2,1)} %weight.2) | copy-start | bytes 1572868
  79.3 7.3 %copy-start.6 = (bf16[3,128]{1,0:T(4,128)(2,1)S(1)}, bf16[3,128]{1,0:T(4,128)(2,1)}, u32[]{:S(2)}) copy-start(bf16[3,128]{1,0:T(4,128)(2,1)} %taps.1) | copy-start | bytes 2308
  83.4 3.2 %collective-permute-start = (bf16[2,128]{1,0:T(2,128)(2,1)S(1)}, bf16[2,128]{1,0:T(2,128)(2,1)S(1)}, u32[]{:S(2)}, u32[]{:S(2)}) collective-permute-start(bf16[2,128]{1,0:T(2,128)(2,1)S(1)} %slice.3), channel_id=1, source_target_pairs={{0,8},{8,16},{16,24},{24,32},{32,40},{40,48},{48,56},{56,64},{64,7... | collective-permute-start | bytes 1544 | tf_op jit(solution)/shard_map/ppermute | solution.py:308
  86.6 8.2 %copy-start.3 = (bf16[256,2048]{1,0:T(8,128)(2,1)S(1)}, bf16[256,2048]{1,0:T(8,128)(2,1)}, u32[]{:S(2)}) copy-start(bf16[256,2048]{1,0:T(8,128)(2,1)} %weight.3) | copy-start | bytes 3145732

commit v4 on v3

--- a/solution.py
+++ b/solution.py
@@ -11,6 +11,7 @@
 HD = 256
 MDIM = 2048
 EPS = 1e-06
+OWN = 56
 CHUNKS = 4
 LOWEST = -1e30
 TP = "tp"
@@ -82,11 +83,14 @@
     out[0, N:, N:] = jnp.zeros((16, N), BF)
 
 
-def products(tok, sources, places, sems):
+def cuts(sources, places):
+    step = places[0].shape[0] // CHUNKS
+    cut = [pl.ds(c * step, step) for c in range(CHUNKS)]
+    return [(s.at[at, :], p.at[at, :]) for at in cut for s, p in zip(sources, places)]
+
+
+def products(tok, places, copies):
     groups, _, part = tok.shape
-    step = groups * part // CHUNKS
-    cut = [pl.ds(c * step, step) for c in range(CHUNKS)]
-    copies = fetched([(s.at[at, :], p.at[at, :]) for at in cut for s, p in zip(sources, places)], sems)
     sums = [jnp.zeros((N, p.shape[1]), F32) for p in places]
     for c in range(CHUNKS):
         for each in copies[c * len(places) : (c + 1) * len(places)]:
@@ -104,9 +108,12 @@
     return -(jnp.maximum(-x, 0.0) + jnp.where(e < 0.01, series, jnp.log(1.0 + e)))
 
 
-def states(tok, kw_hbm, vw_hbm, gw, bias, message, kv, aux, state, kw, vw, sems):
+def states(tok_hbm, kw_hbm, vw_hbm, gw_hbm, bias_hbm, message, kv, aux, state, tok, kw, vw, gw, bias, first, sems):
     groups, _, part = tok.shape
-    k_sum, v_sum = products(tok, (kw_hbm, vw_hbm), (kw, vw), sems)
+    small = fetched([(tok_hbm, tok), (gw_hbm, gw), (bias_hbm, bias)], first)
+    copies = fetched(cuts((kw_hbm, vw_hbm), (kw, vw)), sems)
+    for c in small:
+        c.wait()
     g_sum = jnp.zeros((N, 2), F32)
     sq = jnp.zeros((1, N), F32)
     for g in range(groups):
@@ -115,10 +122,6 @@
         tail = tok[g, N:, :N].astype(F32)
         sq += tail[0:1] + tail[1:2] + tail[2:3]
     inv = lax.rsqrt(to_col(sq) / (groups * part) + EPS)
-    k = (inv * k_sum).astype(BF)
-    v = (inv * v_sum).astype(BF)
-    kv[:, :HD] = k
-    kv[:, HD:] = v
     gates = inv * g_sum
     i_col = gates[:, 0:1] + bias[0:1, 0:1]
     lf_col = log_sigmoid(gates[:, 1:2] + bias[0:1, 1:2])
@@ -132,6 +135,11 @@
     weight = after + i_col
     top = jnp.max(weight, axis=0, keepdims=True)
     weight = jnp.exp(weight - top)
+    k_sum, v_sum = products(tok, (kw, vw), copies)
+    k = (inv * k_sum).astype(BF)
+    v = (inv * v_sum).astype(BF)
+    kv[:, :HD] = k
+    kv[:, HD:] = v
     kf = k.astype(F32) * HD**-0.5
     weighted = weight * kf
     hi = weighted.astype(BF)
@@ -190,14 +198,26 @@
     own[...] = jnp.concatenate(lines + [jnp.zeros((5, N), F32)], axis=0)
 
 
-def inside(tok, aux, kv, qw_hbm, ow_hbm, bw_hbm, cw_hbm, uw_hbm, gain, pack, gate_b, mixed, qw, ow, bw, cw, uw, sems):
-    sums = products(tok, (qw_hbm, ow_hbm, bw_hbm, cw_hbm, uw_hbm), (qw, ow, bw, cw, uw), sems)
+def mixing(tok_hbm, aux_hbm, bw_hbm, cw_hbm, uw_hbm, gate_b, mixed, tok, aux, bw, cw, uw, first, sems):
+    small = fetched([(tok_hbm, tok), (aux_hbm, aux)], first)
+    copies = fetched(cuts((bw_hbm, cw_hbm, uw_hbm), (bw, cw, uw)), sems)
+    for c in small:
+        c.wait()
+    inv = to_col(aux[2:3, :])
+    gb, gc, gu = [(inv * s).astype(BF) for s in products(tok, (bw, cw, uw), copies)]
+    gate_b[...] = gb
+    mixed[...] = (gc.astype(F32) * gu.astype(F32)).astype(BF)
+
+
+def inside(tok_hbm, aux_hbm, kv_hbm, qw_hbm, ow_hbm, gain_hbm, pack, tok, aux, kv, qw, ow, gain, first, sems):
+    small = fetched([(tok_hbm, tok), (aux_hbm, aux), (kv_hbm, kv), (gain_hbm, gain)], first)
+    copies = fetched(cuts((qw_hbm, ow_hbm), (qw, ow)), sems)
+    for c in small:
+        c.wait()
     b_row, i_row = aux[0:1, :], aux[1:2, :]
     inv = to_col(aux[2:3, :])
-    q, og, gb, gc, gu = [(inv * s).astype(BF) for s in sums]
+    q, og = [(inv * s).astype(BF) for s in products(tok, (qw, ow), copies)]
     pack[:, :HD] = q.astype(F32)
-    gate_b[...] = gb
-    mixed[...] = (gc.astype(F32) * gu.astype(F32)).astype(BF)
     pack[:, 2 * HD : 3 * HD] = jax.nn.sigmoid(og.astype(F32)) * gain[...].astype(F32).reshape(1, HD)
     b_col = to_col(b_row)
     causal = iota(1) <= iota(0)
@@ -212,7 +232,7 @@
     pack[:, 3 * HD :] = jnp.where(lane == 0, b_col, jnp.where(lane == 1, top, jnp.where(lane == 2, denom, 0.0)))
 
 
-def convolve(halo, mixed, gate_b, taps, weight, out):
+def convolve(place, halo, mixed, gate_b, taps, weight, keep, send):
     now = mixed[...].astype(F32)
     prev = halo[...].astype(F32)
     row = iota(0)
@@ -221,10 +241,15 @@
     t = taps[...].astype(F32)
     total = t[0:1] * two + t[1:2] * one + t[2:3] * now
     y = (gate_b[...].astype(F32) * total).astype(BF)
-    out[...] = dot(y, weight[...]).astype(BF)
-
-
-def finish(arrived, own, pack, conv, weight, out, state):
+    done = dot(y, weight[...]).astype(BF)
+    half = done.shape[1] // 2
+    left, right = done[:, :half], done[:, half:]
+    first = place[0] % 2 == 0
+    keep[...] = jnp.where(first, left, right)
+    send[...] = jnp.where(first, right, left)
+
+
+def finish(arrived, own, pack, keep, other, weight, out, state):
     _, rows, _ = arrived.shape
     half = rows // 2
     q = pack[:, :HD].astype(BF)
@@ -249,27 +274,31 @@
     tail = tail.astype(BF)
     groups, size, _ = out.shape
     width = weight.shape[1]
+    conv = (keep[...].astype(F32) + other[...].astype(F32)).astype(BF)
     for g in range(groups):
         at = slice(g * size, (g + 1) * size)
         out[g, :, :width] = done[at]
-        out[g, :, width : 2 * width] = conv[at]
-        out[g, :, 2 * width :] = tail[at]
+        out[g, :, width : width + width // 2] = conv[at]
+        out[g, :, width + width // 2 :] = tail[at]
 
 
 def gather_up(arrived, out):
     groups, size, width = arrived.shape
-    width = (width - N) // 2
+    half = (width - N) // 3
     squares = jnp.zeros((size, 1), F32)
     for g in range(groups):
-        tail = arrived[g, :, 2 * width :].astype(F32)
+        tail = arrived[g, :, 3 * half :].astype(F32)
         squares += tail[:, 0:1] + tail[:, 1:2] + tail[:, 2:3]
     scale = lax.rsqrt(squares / MDIM + EPS)
-    c = jnp.zeros((size, width), F32)
-    m = jnp.zeros((size, width), F32)
-    for g in range(groups):
-        m += arrived[g, :, :width].astype(F32)
-        c += arrived[g, :, width : 2 * width].astype(F32)
-    out[...] = (c + scale * m).astype(BF)
+    for side in range(2):
+        at = slice(side * half, (side + 1) * half)
+        m = jnp.zeros((size, half), F32)
+        c = jnp.zeros((size, half), F32)
+        for g in range(groups):
+            m += arrived[g, :, at].astype(F32)
+        for g in range(side, groups, 2):
+            c += arrived[g, :, 2 * half : 3 * half].astype(F32)
+        out[:, at] = (c + scale * m).astype(BF)
 
 
 def exchange(value, axis):
@@ -285,39 +314,50 @@
     vmem, hbm = pl.BlockSpec(memory_space=pltpu.VMEM), pl.BlockSpec(memory_space=pltpu.HBM)
     room = lambda *arrays: [pltpu.VMEM(a.shape, a.dtype) for a in arrays]
     sems = lambda n: [pltpu.SemaphoreType.DMA((n,))]
+    vmem, hbm, smem = [pl.BlockSpec(memory_space=m) for m in (pltpu.VMEM, pltpu.HBM, pltpu.SMEM)]
+    room = lambda *arrays: [pltpu.VMEM(a.shape, a.dtype) for a in arrays]
+    sems = lambda *ns: [pltpu.SemaphoreType.DMA((n,)) for n in ns]
     (local,) = call(
         prepare, [((1, N + 16, tokens.shape[1]), BF)], tokens, norm_gain,
-        specs=[hbm, hbm], scratch=room(tokens, norm_gain) + sems(2),
+        specs=[hbm] * 2, scratch=room(tokens, norm_gain) + sems(2), limit=OWN,
     )
     tok = lax.all_gather(local, TP, axis=0, tiled=True)
+    taken = (tok, key_w, value_w, gate_w.reshape(model, 2).T, gate_bias.reshape(1, 2))
     message, kv, aux = call(
         states,
         [((count, rows + 4, N), BF), ((N, 2 * HD), BF), ((8, N), F32)],
-        tok, key_w, value_w, gate_w.reshape(model, 2).T, gate_bias.reshape(1, 2), flops=10**9, limit=52,
-        scratch=[pltpu.VMEM((count, rows + 4, N), F32)] + room(key_w, value_w) + sems(2 * CHUNKS),
-        specs=[vmem, hbm, hbm, vmem, vmem],
+        *taken, flops=10**9, specs=[hbm] * 5, limit=OWN,
+        scratch=[pltpu.VMEM((count, rows + 4, N), F32)] + room(*taken) + sems(3, 2 * CHUNKS),
     )
     arrived = exchange(message, SP)
-    others = (query_w, outgate_w, conv_b_w, conv_c_w, conv_u_w)
-    pack, gate_b, mixed = call(
-        inside,
-        [((N, 3 * HD + N), F32), ((N, N), BF), ((N, N), BF)],
-        tok, aux, kv, *others, mem_gain, flops=2 * 10**9, limit=53,
-        scratch=room(*others) + sems(5 * CHUNKS), specs=[vmem] * 3 + [hbm] * 5 + [vmem],
+    taken = (tok, aux, conv_b_w, conv_c_w, conv_u_w)
+    gate_b, mixed = call(
+        mixing, [((N, N), BF), ((N, N), BF)], *taken, flops=10**9, specs=[hbm] * 5, limit=OWN,
+        scratch=room(*taken) + sems(2, 3 * CHUNKS),
     )
     halo = lax.ppermute(mixed[N - 2 :], SP, [(i, i + 1) for i in range(count - 1)])
-    (conv,) = call(convolve, [((N, model), BF)], halo, mixed, gate_b, conv_taps, conv_out_w, flops=10**9)
+    taken = (tok, aux, kv, query_w, outgate_w, mem_gain)
+    (pack,) = call(
+        inside, [((N, 3 * HD + N), F32)], *taken, flops=10**9, specs=[hbm] * 6, limit=OWN,
+        scratch=room(*taken) + sems(4, 2 * CHUNKS),
+    )
+    core = lax.axis_index(TP).reshape(1).astype(jnp.int32)
+    keep, send = call(
+        convolve, [((N, model // 2), BF), ((N, model // 2), BF)], core, halo, mixed, gate_b, conv_taps, conv_out_w,
+        flops=10**9, specs=[smem] + [vmem] * 5,
+    )
+    other = lax.ppermute(send, TP, [(i, i ^ 1) for i in range(groups)])
     place = lax.axis_index(SP).reshape(1).astype(jnp.int32)
     back, own = call(
         carry,
         [((count, rows, N), BF), ((8, N), F32)],
         place, arrived, flops=10**9,
         scratch=[pltpu.VMEM((count, rows + 4, N), F32), pltpu.VMEM((count, rows, N), F32)],
-        specs=[pl.BlockSpec(memory_space=pltpu.SMEM), vmem],
+        specs=[smem, vmem],
     )
     state = exchange(back, SP)
     (mem,) = call(
-        finish, [((groups, N // groups, 2 * model + N), BF)], state, own, pack, conv, mem_out_w,
+        finish, [((groups, N // groups, 3 * model // 2 + N), BF)], state, own, pack, keep, other, mem_out_w,
         flops=10**9, scratch=[pltpu.VMEM((count, rows, N), F32)],
     )
     mem = exchange(mem, TP)

time: 119 us -> 118 us (level)
  waiting for transfers between devices: 25.9 us -> 18 us
  Pallas kernels: 11.7 us -> 16.7 us
  starting transfers between devices: 28.6 us -> 32.7 us
  blocking collectives: 49.6 us -> 46.1 us
    all_to_all x2, waiting for transfers between devices: 25.2 us -> 17.3 us  [exchange(): return lax.all_to_all(value, axis, split_axis=0, concat_axis=0, tiled=True)]
    pallas_call x7 -> x8, Pallas kernels: 11.7 us -> 16.7 us  [call(): pl.pallas_call(kernel, out_shape=[jax.ShapeDtypeStruct(s, d) for s, d in...]
    all_to_all x1, blocking collectives: 22.5 us -> 17.6 us  [exchange(): return lax.all_to_all(value, axis, split_axis=0, concat_axis=0, tiled=True)]
    ppermute x0 -> x1, starting transfers between devices: none -> 4.17 us  [body(): other = lax.ppermute(send, TP, [(i, i ^ 1) for i in range(groups)])]
    all_gather x1, blocking collectives: 27.1 us -> 28.4 us  [body(): tok = lax.all_gather(local, TP, axis=0, tiled=True)]
    unnamed x18 -> x12, local copies, waits for them, and re-layouts: 2.89 us -> 3.21 us
  transfers between devices with their start and end apart: 3 -> 4, of which waited for: 3 -> 2; matrix products, arithmetic and copies ran while one was open for 0% -> 1% of each run, Pallas kernels for 4% -> 6%
where the time goes in v4:
time: 118 us; the launch traced here: 117 us
  blocking collectives  46.1 us (39%)
  starting transfers between devices  32.7 us (28%)
  waiting for transfers between devices  18 us (15%)
  Pallas kernels  16.7 us (14%)
  local copies, waits for them, and re-layouts  3.88 us (3%)
    all_gather x1, blocking collectives, body(): tok = lax.all_gather(local, TP, axis=0, tiled=True)  28.4 us
    all_to_all x2, starting transfers between devices, exchange(): return lax.all_to_all(value, axis, split_axis=0, concat_axis=0, tiled=True)  26.1 us
    all_to_all x1, blocking collectives, exchange(): return lax.all_to_all(value, axis, split_axis=0, concat_axis=0, tiled=True)  17.6 us
    all_to_all x2, waiting for transfers between devices, exchange(): return lax.all_to_all(value, axis, split_axis=0, concat_axis=0, tiled=True)  17.3 us
    pallas_call x8, Pallas kernels, call(): pl.pallas_call(kernel, out_shape=[jax.ShapeDtypeStruct(s, d) for s, d in...  16.7 us
    ppermute x1, starting transfers between devices, body(): other = lax.ppermute(send, TP, [(i, i ^ 1) for i in range(groups)])  4.17 us
    unnamed x12, local copies, waits for them, and re-layouts  3.21 us
    ppermute x1, starting transfers between devices, body(): lax.ppermute(mixed[N - 2:], SP, [(i, i + 1) for i in range(count - 1)])  2.47 us
  transfers between devices with their start and end apart: 4, of which 2 were waited for; matrix products, arithmetic and copies ran while one was open for 1% of the time, Pallas kernels for 6%

profile of v4, /device:TPU:1, one launch (start us, length us, event | category | flops | bytes accessed | tf_op | source)
XLA Modules:
  0.0 117.5 jit_solution(8447966568802699506)
XLA Ops:
  0.0 1.6 %shard_map.145 = bf16[1,144,256]{2,1,0:T(8,128)(2,1)} custom-call(bf16[128,256]{1,0:T(8,128)(2,1)} %tok_hbm.1, bf16[1,256]{1,0:T(2,128)(2,1)} %gain_hbm.2), custom_call_target="tpu_custom_call" | custom-call | tf_op jit(solution)/shard_map/pallas_call | solution.py:26
  1.6 28.4 %all_gather.3.tok_hbm = bf16[8,144,256]{2,1,0:T(8,128)(2,1)} all-gather(bf16[1,144,256]{2,1,0:T(8,128)(2,1)} %shard_map.145), channel_id=1, replica_groups=mesh['sp'=128,'tp'=8] {'tp'}, dimensions={0}, use_global_device_ids=true | all-gather | bytes 663552 | tf_op jit(solution)/shard_map/all_gather | solution.py:324
  30.0 4.1 %shard_map.146 = (bf16[128,8,128]{2,1,0:T(8,128)(2,1)}, bf16[128,512]{1,0:T(8,128)(2,1)}, f32[8,128]{1,0:T(8,128)}) custom-call(bf16[8,144,256]{2,1,0:T(8,128)(2,1)} %all_gather.3.tok_hbm, bf16[2048,256]{1,0:T(8,128)(2,1)} %kw_hbm.1, bf16[2048,256]{1,0:T(8,128)(2,1)} %vw_hbm.1, bf16[2,2048]{1,0:T(2,128)(2,1)} %bitcast.6, f32[1,2]{1,0:T(1,128)} %bitcast.7), custom_call_target="tpu_custom_call" | custom-call | flops 1000000000 | bytes 1000000 | tf_op jit(solution)/shard_map/pallas_call | solution.py:26
  34.1 13.7 %all-to-all-start = ((bf16[128,8,128]{2,1,0:T(8,128)(2,1)}), bf16[128,8,128]{2,1,0:T(8,128)(2,1)S(1)}, u32[]{:S(2)}, u32[]{:S(2)}) async-start(bf16[128,8,128]{2,1,0:T(8,128)(2,1)} %get-tuple-element.14), calls=%async_computation | async-start | bytes 524288 | tf_op jit(solution)/shard_map/all_to_all | solution.py:305
  47.9 17.3 %all-to-all-done.arrived = bf16[128,8,128]{2,1,0:T(8,128)(2,1)S(1)} async-done(((bf16[128,8,128]{2,1,0:T(8,128)(2,1)}), bf16[128,8,128]{2,1,0:T(8,128)(2,1)S(1)}, u32[]{:S(2)}, u32[]{:S(2)}) %all-to-all-start) | async-done | bytes 262176 | tf_op jit(solution)/shard_map/all_to_all | solution.py:305
  65.2 2.2 %shard_map.147 = (bf16[128,4,128]{2,1,0:T(4,128)(2,1)}, f32[8,128]{1,0:T(8,128)S(1)}) custom-call(s32[1]{0:T(128)} %bitcast.place, bf16[128,8,128]{2,1,0:T(8,128)(2,1)S(1)} %all-to-all-done.arrived), custom_call_target="tpu_custom_call" | custom-call | flops 1000000000 | bytes 1000000 | tf_op jit(solution)/shard_map/pallas_call | solution.py:26
  67.3 12.4 %all-to-all-start.1 = ((bf16[128,4,128]{2,1,0:T(4,128)(2,1)}), bf16[128,4,128]{2,1,0:T(4,128)(2,1)S(1)}, u32[]{:S(2)}, u32[]{:S(2)}) async-start(bf16[128,4,128]{2,1,0:T(4,128)(2,1)} %get-tuple-element.15), calls=%async_computation.1 | async-start | bytes 262144 | tf_op jit(solution)/shard_map/all_to_all | solution.py:305
  79.7 0.0 copy-start.1
  79.7 3.5 %shard_map.149 = (bf16[128,128]{1,0:T(8,128)(2,1)}, bf16[128,128]{1,0:T(8,128)(2,1)}) custom-call(bf16[8,144,256]{2,1,0:T(8,128)(2,1)} %all_gather.3.tok_hbm, f32[8,128]{1,0:T(8,128)} %get-tuple-element.17.aux_hbm, bf16[2048,128]{1,0:T(8,128)(2,1)} %bw_hbm.1, bf16[2048,128]{1,0:T(8,128)(2,1)} %cw_hbm.1, bf16[2048,128]{1,0:T(8,128)(2,1)} %uw_hbm.1), custom_call_target="tpu_custom_call" | custom-call | flops 1000000000 | bytes 1000000 | tf_op jit(solution)/shard_map/pallas_call | solution.py:26
  83.2 0.7 slice.3
  83.9 2.5 %collective-permute-start = (bf16[2,128]{1,0:T(2,128)(2,1)S(1)}, bf16[2,128]{1,0:T(2,128)(2,1)S(1)}, u32[]{:S(2)}, u32[]{:S(2)}) collective-permute-start(bf16[2,128]{1,0:T(2,128)(2,1)S(1)} %slice.3), channel_id=1, source_target_pairs={{0,8},{8,16},{16,24},{24,32},{32,40},{40,48},{48,56},{56,64},{64,7... | collective-permute-start | bytes 1544 | tf_op jit(solution)/shard_map/ppermute | solution.py:338
  86.4 0.7 collective-permute-done.halo
  87.1 0.0 copy-start.2
  87.1 0.0 copy-done.1
  87.1 0.7 copy-done.2
  87.7 0.0 copy-start.3
  87.8 0.8 copy-done.3
  88.5 0.0 copy-start.5
  88.5 0.8 copy-done.5
  89.3 0.3 shard_map.150
  89.6 4.2 %collective-permute-start.1 = (bf16[128,1024]{1,0:T(8,128)(2,1)S(1)}, bf16[128,1024]{1,0:T(8,128)(2,1)S(1)}, u32[]{:S(2)}, u32[]{:S(2)}) collective-permute-start(bf16[128,1024]{1,0:T(8,128)(2,1)S(1)} %get-tuple-element.22), channel_id=1, source_target_pairs={{0,1},{1,0},{2,3},{3,2},{4,5},{5,4},{6,7},{7,6},{8,9},{9,8},{10,11... | collective-permute-start | bytes 786440 | tf_op jit(solution)/shard_map/ppermute | solution.py:349
  93.7 0.0 copy-start
  93.7 3.5 %shard_map.148.pack = f32[128,896]{1,0:T(8,128)} custom-call(bf16[8,144,256]{2,1,0:T(8,128)(2,1)} %all_gather.3.tok_hbm, f32[8,128]{1,0:T(8,128)} %get-tuple-element.17.aux_hbm, bf16[128,512]{1,0:T(8,128)(2,1)} %get-tuple-element.18.kv_hbm, bf16[2048,256]{1,0:T(8,128)(2,1)} %qw_hbm.1, bf16[2048,256]{1,0:T(8,128)(2,1)} %ow_hbm.1, bf16[256]{0:T(256)(128)(2,1)} %gain_hbm.3), custom_call_target="tpu_custom_call" | custom-call | flops 1000000000 | bytes 1000000 | tf_op jit(solution)/shard_map/pallas_call | solution.py:26
  97.2 0.0 collective-permute-done.1.other
  97.3 0.0 all-to-all-done.1.arrived
  97.3 0.0 copy-done
  97.3 0.0 copy-start.4
  97.3 1.0 copy-done.4
  98.3 0.7 shard_map.151
  99.0 17.6 %all_to_all.15.arrived = bf16[8,16,3200]{2,1,0:T(8,128)(2,1)S(1)} all-to-all(bf16[8,16,3200]{2,1,0:T(8,128)(2,1)S(1)} %shard_map.151), channel_id=1, replica_groups=mesh['sp'=128,'tp'=8] {'tp'}, dimensions={0} | all-to-all | bytes 1638400 | tf_op jit(solution)/shard_map/all_to_all | solution.py:305
  116.7 0.8 shard_map.152
Async XLA Ops:
  34.1 31.0 %all-to-all-start = ((bf16[128,8,128]{2,1,0:T(8,128)(2,1)}), bf16[128,8,128]{2,1,0:T(8,128)(2,1)S(1)}, u32[]{:S(2)}, u32[]{:S(2)}) async-start(bf16[128,8,128]{2,1,0:T(8,128)(2,1)} %get-tuple-element.14), calls=%async_computation | async-start | bytes 524288 | tf_op jit(solution)/shard_map/all_to_all | solution.py:305
  67.3 29.9 %all-to-all-start.1 = ((bf16[128,4,128]{2,1,0:T(4,128)(2,1)}), bf16[128,4,128]{2,1,0:T(4,128)(2,1)S(1)}, u32[]{:S(2)}, u32[]{:S(2)}) async-start(bf16[128,4,128]{2,1,0:T(4,128)(2,1)} %get-tuple-element.15), calls=%async_computation.1 | async-start | bytes 262144 | tf_op jit(solution)/shard_map/all_to_all | solution.py:305
  79.7 7.3 %copy-start.1 = (bf16[128,2048]{1,0:T(8,128)(2,1)S(1)}, bf16[128,2048]{1,0:T(8,128)(2,1)}, u32[]{:S(2)}) copy-start(bf16[128,2048]{1,0:T(8,128)(2,1)} %weight.2) | copy-start | bytes 1572868
  83.9 3.2 %collective-permute-start = (bf16[2,128]{1,0:T(2,128)(2,1)S(1)}, bf16[2,128]{1,0:T(2,128)(2,1)S(1)}, u32[]{:S(2)}, u32[]{:S(2)}) collective-permute-start(bf16[2,128]{1,0:T(2,128)(2,1)S(1)} %slice.3), channel_id=1, source_target_pairs={{0,8},{8,16},{16,24},{24,32},{32,40},{40,48},{48,56},{56,64},{64,7... | collective-permute-start | bytes 1544 | tf_op jit(solution)/shard_map/ppermute | solution.py:338
  87.1 0.7 copy-start.2
  87.7 0.8 copy-start.3
  88.5 0.8 copy-start.5
  89.6 7.7 %collective-permute-start.1 = (bf16[128,1024]{1,0:T(8,128)(2,1)S(1)}, bf16[128,1024]{1,0:T(8,128)(2,1)S(1)}, u32[]{:S(2)}, u32[]{:S(2)}) collective-permute-start(bf16[128,1024]{1,0:T(8,128)(2,1)S(1)} %get-tuple-element.22), channel_id=1, source_target_pairs={{0,1},{1,0},{2,3},{3,2},{4,5},{5,4},{6,7},{7,6},{8,9},{9,8},{10,11... | collective-permute-start | bytes 786440 | tf_op jit(solution)/shard_map/ppermute | solution.py:349
  93.7 3.5 %copy-start = (bf16[256,2048]{1,0:T(8,128)(2,1)S(1)}, bf16[256,2048]{1,0:T(8,128)(2,1)}, u32[]{:S(2)}) copy-start(bf16[256,2048]{1,0:T(8,128)(2,1)} %weight.3) | copy-start | bytes 3145732
  97.3 1.0 copy-start.4

commit v5 on v4

--- a/solution.py
+++ b/solution.py
@@ -21,16 +21,22 @@
 INTERPRET = False
 
 
-def call(kernel, outs, *args, flops=0, scratch=(), specs=None, limit=16):
-    options = {} if specs is None else {"in_specs": specs}
+V, H, S, A = pltpu.VMEM, pltpu.HBM, pltpu.SMEM, None
+
+
+def call(kernel, outs, *args, flops=0, scratch=(), places, limit=OWN):
+    if not INTERPRET:
+        args = [a if p in (S, A) else pltpu.with_memory_space_constraint(a, p) for a, p in zip(args, places)]
+    outs = [jax.ShapeDtypeStruct(s, d) if p is A or INTERPRET else p(s, d) for s, d, p in outs]
     return pl.pallas_call(
         kernel,
-        out_shape=[jax.ShapeDtypeStruct(s, d) for s, d in outs],
+        out_shape=outs,
+        in_specs=[pl.BlockSpec(memory_space=V if p is A else p) for p in places],
+        out_specs=[pl.BlockSpec(memory_space=V) for _ in outs],
         scratch_shapes=scratch,
         interpret=INTERPRET,
         compiler_params=pltpu.CompilerParams(vmem_limit_bytes=limit * 2**20),
         cost_estimate=pl.CostEstimate(flops=flops, bytes_accessed=flops // 1000, transcendentals=0) if flops else None,
-        **options,
     )(*args)
 
 
@@ -108,9 +114,9 @@
     return -(jnp.maximum(-x, 0.0) + jnp.where(e < 0.01, series, jnp.log(1.0 + e)))
 
 
-def states(tok_hbm, kw_hbm, vw_hbm, gw_hbm, bias_hbm, message, kv, aux, state, tok, kw, vw, gw, bias, first, sems):
+def states(tok, kw_hbm, vw_hbm, gw_hbm, bias_hbm, message, kv, aux, state, kw, vw, gw, bias, first, sems):
     groups, _, part = tok.shape
-    small = fetched([(tok_hbm, tok), (gw_hbm, gw), (bias_hbm, bias)], first)
+    small = fetched([(gw_hbm, gw), (bias_hbm, bias)], first)
     copies = fetched(cuts((kw_hbm, vw_hbm), (kw, vw)), sems)
     for c in small:
         c.wait()
@@ -198,22 +204,18 @@
     own[...] = jnp.concatenate(lines + [jnp.zeros((5, N), F32)], axis=0)
 
 
-def mixing(tok_hbm, aux_hbm, bw_hbm, cw_hbm, uw_hbm, gate_b, mixed, tok, aux, bw, cw, uw, first, sems):
-    small = fetched([(tok_hbm, tok), (aux_hbm, aux)], first)
+def mixing(tok, aux, bw_hbm, cw_hbm, uw_hbm, gate_b, mixed, edge, bw, cw, uw, sems):
     copies = fetched(cuts((bw_hbm, cw_hbm, uw_hbm), (bw, cw, uw)), sems)
-    for c in small:
-        c.wait()
     inv = to_col(aux[2:3, :])
     gb, gc, gu = [(inv * s).astype(BF) for s in products(tok, (bw, cw, uw), copies)]
     gate_b[...] = gb
-    mixed[...] = (gc.astype(F32) * gu.astype(F32)).astype(BF)
-
-
-def inside(tok_hbm, aux_hbm, kv_hbm, qw_hbm, ow_hbm, gain_hbm, pack, tok, aux, kv, qw, ow, gain, first, sems):
-    small = fetched([(tok_hbm, tok), (aux_hbm, aux), (kv_hbm, kv), (gain_hbm, gain)], first)
+    mix = (gc.astype(F32) * gu.astype(F32)).astype(BF)
+    mixed[...] = mix
+    edge[...] = mix[N - 16 :]
+
+
+def inside(tok, aux, kv, qw_hbm, ow_hbm, gain, pack, qw, ow, sems):
     copies = fetched(cuts((qw_hbm, ow_hbm), (qw, ow)), sems)
-    for c in small:
-        c.wait()
     b_row, i_row = aux[0:1, :], aux[1:2, :]
     inv = to_col(aux[2:3, :])
     q, og = [(inv * s).astype(BF) for s in products(tok, (qw, ow), copies)]
@@ -234,7 +236,7 @@
 
 def convolve(place, halo, mixed, gate_b, taps, weight, keep, send):
     now = mixed[...].astype(F32)
-    prev = halo[...].astype(F32)
+    prev = halo[...].astype(F32)[14:]
     row = iota(0)
     one = jnp.where(row == 0, prev[1:2], pltpu.roll(now, 1, 0))
     two = jnp.where(row == 0, prev[0:1], jnp.where(row == 1, prev[1:2], pltpu.roll(now, 2, 0)))
@@ -314,54 +316,52 @@
     vmem, hbm = pl.BlockSpec(memory_space=pltpu.VMEM), pl.BlockSpec(memory_space=pltpu.HBM)
     room = lambda *arrays: [pltpu.VMEM(a.shape, a.dtype) for a in arrays]
     sems = lambda n: [pltpu.SemaphoreType.DMA((n,))]
-    vmem, hbm, smem = [pl.BlockSpec(memory_space=m) for m in (pltpu.VMEM, pltpu.HBM, pltpu.SMEM)]
     room = lambda *arrays: [pltpu.VMEM(a.shape, a.dtype) for a in arrays]
     sems = lambda *ns: [pltpu.SemaphoreType.DMA((n,)) for n in ns]
     (local,) = call(
-        prepare, [((1, N + 16, tokens.shape[1]), BF)], tokens, norm_gain,
-        specs=[hbm] * 2, scratch=room(tokens, norm_gain) + sems(2), limit=OWN,
+        prepare, [((1, N + 16, tokens.shape[1]), BF, V)], tokens, norm_gain, places=[H, H],
+        scratch=room(tokens, norm_gain) + sems(2),
     )
     tok = lax.all_gather(local, TP, axis=0, tiled=True)
-    taken = (tok, key_w, value_w, gate_w.reshape(model, 2).T, gate_bias.reshape(1, 2))
+    taken = (key_w, value_w, gate_w.reshape(model, 2).T, gate_bias.reshape(1, 2))
     message, kv, aux = call(
         states,
-        [((count, rows + 4, N), BF), ((N, 2 * HD), BF), ((8, N), F32)],
-        *taken, flops=10**9, specs=[hbm] * 5, limit=OWN,
-        scratch=[pltpu.VMEM((count, rows + 4, N), F32)] + room(*taken) + sems(3, 2 * CHUNKS),
+        [((count, rows + 4, N), BF, A), ((N, 2 * HD), BF, A), ((8, N), F32, A)],
+        tok, *taken, flops=10**9, places=[V, H, H, H, H],
+        scratch=[pltpu.VMEM((count, rows + 4, N), F32)] + room(*taken) + sems(2, 2 * CHUNKS),
     )
     arrived = exchange(message, SP)
-    taken = (tok, aux, conv_b_w, conv_c_w, conv_u_w)
-    gate_b, mixed = call(
-        mixing, [((N, N), BF), ((N, N), BF)], *taken, flops=10**9, specs=[hbm] * 5, limit=OWN,
-        scratch=room(*taken) + sems(2, 3 * CHUNKS),
-    )
-    halo = lax.ppermute(mixed[N - 2 :], SP, [(i, i + 1) for i in range(count - 1)])
-    taken = (tok, aux, kv, query_w, outgate_w, mem_gain)
+    taken = (conv_b_w, conv_c_w, conv_u_w)
+    gate_b, mixed, edge = call(
+        mixing, [((N, N), BF, V), ((N, N), BF, V), ((16, N), BF, V)], tok, aux, *taken, flops=10**9,
+        places=[V, A, H, H, H], scratch=room(*taken) + sems(3 * CHUNKS),
+    )
+    halo = lax.ppermute(edge, SP, [(i, i + 1) for i in range(count - 1)])
     (pack,) = call(
-        inside, [((N, 3 * HD + N), F32)], *taken, flops=10**9, specs=[hbm] * 6, limit=OWN,
-        scratch=room(*taken) + sems(4, 2 * CHUNKS),
+        inside, [((N, 3 * HD + N), F32, A)], tok, aux, kv, query_w, outgate_w, mem_gain, flops=10**9,
+        places=[V, A, A, H, H, A], scratch=room(query_w, outgate_w) + sems(2 * CHUNKS),
     )
     core = lax.axis_index(TP).reshape(1).astype(jnp.int32)
     keep, send = call(
-        convolve, [((N, model // 2), BF), ((N, model // 2), BF)], core, halo, mixed, gate_b, conv_taps, conv_out_w,
-        flops=10**9, specs=[smem] + [vmem] * 5,
+        convolve, [((N, model // 2), BF, V), ((N, model // 2), BF, V)],
+        core, halo, mixed, gate_b, conv_taps, conv_out_w,
+        flops=10**9, places=[S, V, V, V, A, V], limit=16,
     )
     other = lax.ppermute(send, TP, [(i, i ^ 1) for i in range(groups)])
     place = lax.axis_index(SP).reshape(1).astype(jnp.int32)
     back, own = call(
         carry,
-        [((count, rows, N), BF), ((8, N), F32)],
-        place, arrived, flops=10**9,
+        [((count, rows, N), BF, V), ((8, N), F32, V)],
+        place, arrived, flops=10**9, places=[S, V], limit=16,
         scratch=[pltpu.VMEM((count, rows + 4, N), F32), pltpu.VMEM((count, rows, N), F32)],
-        specs=[smem, vmem],
     )
     state = exchange(back, SP)
     (mem,) = call(
-        finish, [((groups, N // groups, 3 * model // 2 + N), BF)], state, own, pack, keep, other, mem_out_w,
-        flops=10**9, scratch=[pltpu.VMEM((count, rows, N), F32)],
+        finish, [((groups, N // groups, 3 * model // 2 + N), BF, V)], state, own, pack, keep, other, mem_out_w,
+        flops=10**9, scratch=[pltpu.VMEM((count, rows, N), F32)], places=[V] * 6, limit=16,
     )
     mem = exchange(mem, TP)
-    (out,) = call(gather_up, [((N // groups, model), BF)], mem)
+    (out,) = call(gather_up, [((N // groups, model), BF, A)], mem, places=[V], limit=16)
     return out
 
 

time: 118 us -> 116 us (0.983)
  local copies, waits for them, and re-layouts: 3.88 us -> 1.71 us
    all_to_all x1, blocking collectives: 17.6 us -> 19.7 us  [exchange(): return lax.all_to_all(value, axis, split_axis=0, concat_axis=0, tiled=True)]
    unnamed x12 -> x8, local copies, waits for them, and re-layouts: 3.21 us -> 1.71 us
    all_gather x1, blocking collectives: 28.4 us -> 27.1 us  [body(): tok = lax.all_gather(local, TP, axis=0, tiled=True)]
  transfers between devices with their start and end apart: 4 -> 4, of which waited for: 2 -> 3; matrix products, arithmetic and copies ran while one was open for 1% -> 0% of each run, Pallas kernels for 6% -> 6%
where the time goes in v5:
time: 116 us; the launch traced here: 115 us
  blocking collectives  46.8 us (40%)
  starting transfers between devices  32.7 us (28%)
  waiting for transfers between devices  18.3 us (16%)
  Pallas kernels  15.6 us (13%)
  local copies, waits for them, and re-layouts  1.71 us (1%)
    all_gather x1, blocking collectives, body(): tok = lax.all_gather(local, TP, axis=0, tiled=True)  27.1 us
    all_to_all x2, starting transfers between devices, exchange(): return lax.all_to_all(value, axis, split_axis=0, concat_axis=0, tiled=True)  26.1 us
    all_to_all x1, blocking collectives, exchange(): return lax.all_to_all(value, axis, split_axis=0, concat_axis=0, tiled=True)  19.7 us
    all_to_all x2, waiting for transfers between devices, exchange(): return lax.all_to_all(value, axis, split_axis=0, concat_axis=0, tiled=True)  17.6 us
    pallas_call x8, Pallas kernels, call(): pl.pallas_call(kernel, out_shape=outs, in_specs=[pl.BlockSpec(memory_spac...  15.6 us
    ppermute x1, starting transfers between devices, body(): other = lax.ppermute(send, TP, [(i, i ^ 1) for i in range(groups)])  4.17 us
    ppermute x1, starting transfers between devices, body(): halo = lax.ppermute(edge, SP, [(i, i + 1) for i in range(count - 1)])  2.48 us
  transfers between devices with their start and end apart: 4, of which 3 were waited for; matrix products, arithmetic and copies ran while one was open for 0% of the time, Pallas kernels for 6%

profile of v5, /device:TPU:1, one launch (start us, length us, event | category | flops | bytes accessed | tf_op | source)
XLA Modules:
  0.0 115.3 jit_solution(3752096291449370848)
XLA Ops:
  0.0 1.0 shard_map.145
  1.0 27.1 %all_gather.3.tok = bf16[8,144,256]{2,1,0:T(8,128)(2,1)S(1)} all-gather(bf16[1,144,256]{2,1,0:T(8,128)(2,1)S(1)} %shard_map.145), channel_id=1, replica_groups=mesh['sp'=128,'tp'=8] {'tp'}, dimensions={0}, use_global_device_ids=true | all-gather | bytes 663552 | tf_op jit(solution)/shard_map/all_gather | solution.py:325
  28.1 3.8 %shard_map.146 = (bf16[128,8,128]{2,1,0:T(8,128)(2,1)}, bf16[128,512]{1,0:T(8,128)(2,1)}, f32[8,128]{1,0:T(8,128)}) custom-call(bf16[8,144,256]{2,1,0:T(8,128)(2,1)S(1)} %all_gather.3.tok, bf16[2048,256]{1,0:T(8,128)(2,1)} %kw_hbm.1, bf16[2048,256]{1,0:T(8,128)(2,1)} %vw_hbm.1, bf16[2,2048]{1,0:T(2,128)(2,1)} %bitcast.6, f32[1,2]{1,0:T(1,128)} %bitcast.7), custom_call_target="tpu_custom_call" | custom-call | flops 1000000000 | bytes 1000000 | tf_op jit(solution)/shard_map/pallas_call | solution.py:31
  32.0 13.7 %all-to-all-start = ((bf16[128,8,128]{2,1,0:T(8,128)(2,1)}), bf16[128,8,128]{2,1,0:T(8,128)(2,1)S(1)}, u32[]{:S(2)}, u32[]{:S(2)}) async-start(bf16[128,8,128]{2,1,0:T(8,128)(2,1)} %get-tuple-element.15), calls=%async_computation | async-start | bytes 524288 | tf_op jit(solution)/shard_map/all_to_all | solution.py:307
  45.7 17.3 %all-to-all-done.arrived = bf16[128,8,128]{2,1,0:T(8,128)(2,1)S(1)} async-done(((bf16[128,8,128]{2,1,0:T(8,128)(2,1)}), bf16[128,8,128]{2,1,0:T(8,128)(2,1)S(1)}, u32[]{:S(2)}, u32[]{:S(2)}) %all-to-all-start) | async-done | bytes 262176 | tf_op jit(solution)/shard_map/all_to_all | solution.py:307
  63.0 2.2 %shard_map.147 = (bf16[128,4,128]{2,1,0:T(4,128)(2,1)}, f32[8,128]{1,0:T(8,128)S(1)}) custom-call(s32[1]{0:T(128)} %bitcast.place, bf16[128,8,128]{2,1,0:T(8,128)(2,1)S(1)} %all-to-all-done.arrived), custom_call_target="tpu_custom_call" | custom-call | flops 1000000000 | bytes 1000000 | tf_op jit(solution)/shard_map/pallas_call | solution.py:31
  65.2 12.4 %all-to-all-start.1 = ((bf16[128,4,128]{2,1,0:T(4,128)(2,1)}), bf16[128,4,128]{2,1,0:T(4,128)(2,1)S(1)}, u32[]{:S(2)}, u32[]{:S(2)}) async-start(bf16[128,4,128]{2,1,0:T(4,128)(2,1)} %get-tuple-element.16), calls=%async_computation.1 | async-start | bytes 262144 | tf_op jit(solution)/shard_map/all_to_all | solution.py:307
  77.6 0.0 copy-start.1
  77.6 2.9 %shard_map.149 = (bf16[128,128]{1,0:T(8,128)(2,1)S(1)}, bf16[128,128]{1,0:T(8,128)(2,1)S(1)}, bf16[16,128]{1,0:T(8,128)(2,1)S(1)}) custom-call(bf16[8,144,256]{2,1,0:T(8,128)(2,1)S(1)} %all_gather.3.tok, f32[8,128]{1,0:T(8,128)} %get-tuple-element.18.aux, bf16[2048,128]{1,0:T(8,128)(2,1)} %bw_hbm.1, bf16[2048,128]{1,0:T(8,128)(2,1)} %cw_hbm.1, ...), custom_call_target="tpu_custom_call" | custom-call | flops 1000000000 | bytes 1000000 | tf_op jit(solution)/shard_map/pallas_call | solution.py:31
  80.5 2.5 %collective-permute-start = (bf16[16,128]{1,0:T(8,128)(2,1)S(1)}, bf16[16,128]{1,0:T(8,128)(2,1)S(1)}, u32[]{:S(2)}, u32[]{:S(2)}) collective-permute-start(bf16[16,128]{1,0:T(8,128)(2,1)S(1)} %get-tuple-element.20), channel_id=1, source_target_pairs={{0,8},{8,16},{16,24},{24,32},{32,40},{40,48},{48,56},{56,64},{64,7... | collective-permute-start | bytes 12296 | tf_op jit(solution)/shard_map/ppermute | solution.py:339
  83.0 0.7 collective-permute-done.halo
  83.7 0.0 copy-start.2
  83.7 0.0 copy-done.1
  83.7 0.7 copy-done.2
  84.4 0.3 shard_map.150
  84.7 4.2 %collective-permute-start.1 = (bf16[128,1024]{1,0:T(8,128)(2,1)S(1)}, bf16[128,1024]{1,0:T(8,128)(2,1)S(1)}, u32[]{:S(2)}, u32[]{:S(2)}) collective-permute-start(bf16[128,1024]{1,0:T(8,128)(2,1)S(1)} %get-tuple-element.24), channel_id=1, source_target_pairs={{0,1},{1,0},{2,3},{3,2},{4,5},{5,4},{6,7},{7,6},{8,9},{9,8},{10,11... | collective-permute-start | bytes 786440 | tf_op jit(solution)/shard_map/ppermute | solution.py:350
  88.9 0.0 copy-start
  88.9 3.8 %shard_map.148.pack = f32[128,896]{1,0:T(8,128)} custom-call(bf16[8,144,256]{2,1,0:T(8,128)(2,1)S(1)} %all_gather.3.tok, f32[8,128]{1,0:T(8,128)} %get-tuple-element.18.aux, bf16[128,512]{1,0:T(8,128)(2,1)} %get-tuple-element.19.kv, bf16[2048,256]{1,0:T(8,128)(2,1)} %qw_hbm.1, bf16[2048,256]{1,0:T(8,128)(2,1)} %ow_hbm.1, bf16[256]{0:T(256)(128)(2,1)} %gain.1), custom_call_target="tpu_custom_call" | custom-call | flops 1000000000 | bytes 1000000 | tf_op jit(solution)/shard_map/pallas_call | solution.py:31
  92.7 0.0 collective-permute-done.1.other
  92.7 0.3 all-to-all-done.1.arrived
  93.1 0.0 copy-done
  93.1 0.0 copy-start.3
  93.1 1.0 copy-done.3
  94.1 0.7 shard_map.151
  94.8 19.7 %all_to_all.15.arrived = bf16[8,16,3200]{2,1,0:T(8,128)(2,1)S(1)} all-to-all(bf16[8,16,3200]{2,1,0:T(8,128)(2,1)S(1)} %shard_map.151), channel_id=1, replica_groups=mesh['sp'=128,'tp'=8] {'tp'}, dimensions={0} | all-to-all | bytes 1638400 | tf_op jit(solution)/shard_map/all_to_all | solution.py:307
  114.5 0.8 shard_map.152
Async XLA Ops:
  32.0 31.0 %all-to-all-start = ((bf16[128,8,128]{2,1,0:T(8,128)(2,1)}), bf16[128,8,128]{2,1,0:T(8,128)(2,1)S(1)}, u32[]{:S(2)}, u32[]{:S(2)}) async-start(bf16[128,8,128]{2,1,0:T(8,128)(2,1)} %get-tuple-element.15), calls=%async_computation | async-start | bytes 524288 | tf_op jit(solution)/shard_map/all_to_all | solution.py:307
  65.2 27.9 %all-to-all-start.1 = ((bf16[128,4,128]{2,1,0:T(4,128)(2,1)}), bf16[128,4,128]{2,1,0:T(4,128)(2,1)S(1)}, u32[]{:S(2)}, u32[]{:S(2)}) async-start(bf16[128,4,128]{2,1,0:T(4,128)(2,1)} %get-tuple-element.16), calls=%async_computation.1 | async-start | bytes 262144 | tf_op jit(solution)/shard_map/all_to_all | solution.py:307
  77.6 6.2 %copy-start.1 = (bf16[128,2048]{1,0:T(8,128)(2,1)S(1)}, bf16[128,2048]{1,0:T(8,128)(2,1)}, u32[]{:S(2)}) copy-start(bf16[128,2048]{1,0:T(8,128)(2,1)} %weight.2) | copy-start | bytes 1572868
  80.5 3.2 %collective-permute-start = (bf16[16,128]{1,0:T(8,128)(2,1)S(1)}, bf16[16,128]{1,0:T(8,128)(2,1)S(1)}, u32[]{:S(2)}, u32[]{:S(2)}) collective-permute-start(bf16[16,128]{1,0:T(8,128)(2,1)S(1)} %get-tuple-element.20), channel_id=1, source_target_pairs={{0,8},{8,16},{16,24},{24,32},{32,40},{40,48},{48,56},{56,64},{64,7... | collective-permute-start | bytes 12296 | tf_op jit(solution)/shard_map/ppermute | solution.py:339
  83.7 0.7 copy-start.2
  84.7 8.0 %collective-permute-start.1 = (bf16[128,1024]{1,0:T(8,128)(2,1)S(1)}, bf16[128,1024]{1,0:T(8,128)(2,1)S(1)}, u32[]{:S(2)}, u32[]{:S(2)}) collective-permute-start(bf16[128,1024]{1,0:T(8,128)(2,1)S(1)} %get-tuple-element.24), channel_id=1, source_target_pairs={{0,1},{1,0},{2,3},{3,2},{4,5},{5,4},{6,7},{7,6},{8,9},{9,8},{10,11... | collective-permute-start | bytes 786440 | tf_op jit(solution)/shard_map/ppermute | solution.py:350
  88.9 4.2 %copy-start = (bf16[256,2048]{1,0:T(8,128)(2,1)S(1)}, bf16[256,2048]{1,0:T(8,128)(2,1)}, u32[]{:S(2)}) copy-start(bf16[256,2048]{1,0:T(8,128)(2,1)} %weight.3) | copy-start | bytes 3145732
  93.1 1.0 copy-start.3

commit v6 on v5

--- a/solution.py
+++ b/solution.py
@@ -76,8 +76,8 @@
     return copies
 
 
-def prepare(tok_hbm, gain_hbm, out, tok, gain, sems):
-    for c in fetched([(tok_hbm, tok), (gain_hbm, gain)], sems):
+def prepare(tok_hbm, gain_hbm, gw_hbm, bias_hbm, taps_hbm, out, gw, bias, taps, tok, gain, sems):
+    for c in fetched([(tok_hbm, tok), (gain_hbm, gain), (gw_hbm, gw), (bias_hbm, bias), (taps_hbm, taps)], sems):
         c.wait()
     wide = tok[...].astype(F32)
     out[0, :N, :] = (wide * gain[...].astype(F32)).astype(BF)
@@ -95,7 +95,7 @@
     return [(s.at[at, :], p.at[at, :]) for at in cut for s, p in zip(sources, places)]
 
 
-def products(tok, places, copies):
+def products(tok, places, copies=()):
     groups, _, part = tok.shape
     sums = [jnp.zeros((N, p.shape[1]), F32) for p in places]
     for c in range(CHUNKS):
@@ -114,12 +114,9 @@
     return -(jnp.maximum(-x, 0.0) + jnp.where(e < 0.01, series, jnp.log(1.0 + e)))
 
 
-def states(tok, kw_hbm, vw_hbm, gw_hbm, bias_hbm, message, kv, aux, state, kw, vw, gw, bias, first, sems):
+def states(tok, gw, bias, kw_hbm, vw_hbm, message, kv, aux, state, kw, vw, sems):
     groups, _, part = tok.shape
-    small = fetched([(gw_hbm, gw), (bias_hbm, bias)], first)
     copies = fetched(cuts((kw_hbm, vw_hbm), (kw, vw)), sems)
-    for c in small:
-        c.wait()
     g_sum = jnp.zeros((N, 2), F32)
     sq = jnp.zeros((1, N), F32)
     for g in range(groups):
@@ -168,7 +165,7 @@
     aux[...] = jnp.concatenate([b_row, i_row, to_row(inv), jnp.zeros((5, N), F32)], axis=0)
 
 
-def carry(place, arrived, message, own, state, back):
+def carry(place, arrived, _, message, own, state, back):
     count, rows, _ = arrived.shape
     slab = rows - 4
     state[...] = arrived[...].astype(F32)
@@ -189,25 +186,23 @@
     low = (weights - hi.astype(F32)).astype(BF)
     mine = lax.broadcasted_iota(jnp.int32, (count, 1), 0) == place[0]
     pick = lambda a: jnp.sum(jnp.where(mine, a, 0.0), axis=0, keepdims=True)
-    lines = []
     lane = lax.broadcasted_iota(jnp.int32, (1, N), 1)
-    for r in range(rows):
-        part = state[:, r, :]
-        part = (jnp.where(lane < 6, 0.0, part) if r == slab + 2 else part).astype(BF)
-        whole = dot(hi, part) + dot(low, part)
-        if r < slab:
-            back[:, r, :] = whole
-        else:
-            lines.append(pick(whole))
+    parts = [state[:, r, :] for r in range(rows)]
+    parts[slab + 2] = jnp.where(lane < 6, 0.0, parts[slab + 2])
+    wide = jnp.concatenate([p.astype(BF) for p in parts], axis=1)
+    whole = dot(jnp.concatenate([hi, low], axis=1), jnp.concatenate([wide, wide], axis=0))
+    whole = [whole[:, r * N : (r + 1) * N] for r in range(rows)]
+    for r in range(slab):
+        back[:, r, :] = whole[r]
     message[...] = back[...].astype(BF)
+    lines = [pick(w) for w in whole[slab:]]
     lines = [lines[0] + lines[3], lines[1] + lines[2], jnp.broadcast_to(pick(top), (1, N))]
     own[...] = jnp.concatenate(lines + [jnp.zeros((5, N), F32)], axis=0)
 
 
-def mixing(tok, aux, bw_hbm, cw_hbm, uw_hbm, gate_b, mixed, edge, bw, cw, uw, sems):
-    copies = fetched(cuts((bw_hbm, cw_hbm, uw_hbm), (bw, cw, uw)), sems)
+def mixing(tok, aux, bw, cw, uw, gate_b, mixed, edge):
     inv = to_col(aux[2:3, :])
-    gb, gc, gu = [(inv * s).astype(BF) for s in products(tok, (bw, cw, uw), copies)]
+    gb, gc, gu = [(inv * s).astype(BF) for s in products(tok, (bw, cw, uw))]
     gate_b[...] = gb
     mix = (gc.astype(F32) * gu.astype(F32)).astype(BF)
     mixed[...] = mix
@@ -318,41 +313,41 @@
     sems = lambda n: [pltpu.SemaphoreType.DMA((n,))]
     room = lambda *arrays: [pltpu.VMEM(a.shape, a.dtype) for a in arrays]
     sems = lambda *ns: [pltpu.SemaphoreType.DMA((n,)) for n in ns]
-    (local,) = call(
-        prepare, [((1, N + 16, tokens.shape[1]), BF, V)], tokens, norm_gain, places=[H, H],
-        scratch=room(tokens, norm_gain) + sems(2),
+    small = (gate_w.reshape(model, 2).T, gate_bias.reshape(1, 2), conv_taps)
+    local, gate_wt, biases, taps = call(
+        prepare,
+        [((1, N + 16, tokens.shape[1]), BF, V)] + [(a.shape, a.dtype, V) for a in small],
+        tokens, norm_gain, *small, places=[H] * 5, scratch=room(tokens, norm_gain) + sems(5),
     )
     tok = lax.all_gather(local, TP, axis=0, tiled=True)
-    taken = (key_w, value_w, gate_w.reshape(model, 2).T, gate_bias.reshape(1, 2))
     message, kv, aux = call(
         states,
-        [((count, rows + 4, N), BF, A), ((N, 2 * HD), BF, A), ((8, N), F32, A)],
-        tok, *taken, flops=10**9, places=[V, H, H, H, H],
-        scratch=[pltpu.VMEM((count, rows + 4, N), F32)] + room(*taken) + sems(2, 2 * CHUNKS),
+        [((count, rows + 4, N), BF, A), ((N, 2 * HD), BF, A), ((8, N), F32, V)],
+        tok, gate_wt, biases, key_w, value_w, flops=10**9, places=[V, V, V, H, H],
+        scratch=[pltpu.VMEM((count, rows + 4, N), F32)] + room(key_w, value_w) + sems(2 * CHUNKS),
     )
     arrived = exchange(message, SP)
-    taken = (conv_b_w, conv_c_w, conv_u_w)
     gate_b, mixed, edge = call(
-        mixing, [((N, N), BF, V), ((N, N), BF, V), ((16, N), BF, V)], tok, aux, *taken, flops=10**9,
-        places=[V, A, H, H, H], scratch=room(*taken) + sems(3 * CHUNKS),
+        mixing, [((N, N), BF, V), ((N, N), BF, V), ((16, N), BF, V)], tok, aux, conv_b_w, conv_c_w,
+        conv_u_w, flops=10**9, places=[V] * 5, limit=16,
     )
     halo = lax.ppermute(edge, SP, [(i, i + 1) for i in range(count - 1)])
     (pack,) = call(
         inside, [((N, 3 * HD + N), F32, A)], tok, aux, kv, query_w, outgate_w, mem_gain, flops=10**9,
-        places=[V, A, A, H, H, A], scratch=room(query_w, outgate_w) + sems(2 * CHUNKS),
+        places=[V, V, A, H, H, A], scratch=room(query_w, outgate_w) + sems(2 * CHUNKS),
     )
     core = lax.axis_index(TP).reshape(1).astype(jnp.int32)
     keep, send = call(
         convolve, [((N, model // 2), BF, V), ((N, model // 2), BF, V)],
-        core, halo, mixed, gate_b, conv_taps, conv_out_w,
-        flops=10**9, places=[S, V, V, V, A, V], limit=16,
+        core, halo, mixed, gate_b, taps, conv_out_w,
+        flops=10**9, places=[S] + [V] * 5, limit=16,
     )
     other = lax.ppermute(send, TP, [(i, i ^ 1) for i in range(groups)])
     place = lax.axis_index(SP).reshape(1).astype(jnp.int32)
     back, own = call(
         carry,
         [((count, rows, N), BF, V), ((8, N), F32, V)],
-        place, arrived, flops=10**9, places=[S, V], limit=16,
+        place, arrived, other, flops=10**9, places=[S, V, V], limit=16,
         scratch=[pltpu.VMEM((count, rows + 4, N), F32), pltpu.VMEM((count, rows, N), F32)],
     )
     state = exchange(back, SP)

time: 116 us -> 117 us (level)
  waiting for transfers between devices: 18.3 us -> 22 us
  Pallas kernels: 15.6 us -> 12.7 us
    pallas_call x8, Pallas kernels: 15.6 us -> 12.7 us  [call(): pl.pallas_call(kernel, out_shape=outs, in_specs=[pl.BlockSpec(memory_spac...]
    all_to_all x2, waiting for transfers between devices: 17.6 us -> 20.2 us  [exchange(): return lax.all_to_all(value, axis, split_axis=0, concat_axis=0, tiled=True)]
    all_to_all x2, starting transfers between devices: 26.1 us -> 27.6 us  [exchange(): return lax.all_to_all(value, axis, split_axis=0, concat_axis=0, tiled=True)]
  transfers between devices with their start and end apart: 4 -> 4, of which waited for: 3 -> 4; matrix products, arithmetic and copies ran while one was open for 0% -> 0% of each run, Pallas kernels for 6% -> 4%
where the time goes in v6:
time: 117 us; the launch traced here: 116 us
  blocking collectives  46.7 us (40%)
  starting transfers between devices  33.6 us (29%)
  waiting for transfers between devices  22 us (19%)
  Pallas kernels  12.7 us (11%)
    all_to_all x2, starting transfers between devices, exchange(): return lax.all_to_all(value, axis, split_axis=0, concat_axis=0, tiled=True)  27.6 us
    all_gather x1, blocking collectives, body(): tok = lax.all_gather(local, TP, axis=0, tiled=True)  27.1 us
    all_to_all x2, waiting for transfers between devices, exchange(): return lax.all_to_all(value, axis, split_axis=0, concat_axis=0, tiled=True)  20.2 us
    all_to_all x1, blocking collectives, exchange(): return lax.all_to_all(value, axis, split_axis=0, concat_axis=0, tiled=True)  19.5 us
    pallas_call x8, Pallas kernels, call(): pl.pallas_call(kernel, out_shape=outs, in_specs=[pl.BlockSpec(memory_spac...  12.7 us
    ppermute x1, starting transfers between devices, body(): other = lax.ppermute(send, TP, [(i, i ^ 1) for i in range(groups)])  3.48 us
    ppermute x1, starting transfers between devices, body(): halo = lax.ppermute(edge, SP, [(i, i + 1) for i in range(count - 1)])  2.48 us
  transfers between devices with their start and end apart: 4, of which 4 were waited for; matrix products, arithmetic and copies ran while one was open for 0% of the time, Pallas kernels for 4%

profile of v6, /device:TPU:1, one launch (start us, length us, event | category | flops | bytes accessed | tf_op | source)
XLA Modules:
  0.0 116.2 jit_solution(11699118611128600838)
XLA Ops:
  0.0 1.0 shard_map.145
  1.0 27.1 %all_gather.3.tok = bf16[8,144,256]{2,1,0:T(8,128)(2,1)S(1)} all-gather(bf16[1,144,256]{2,1,0:T(8,128)(2,1)S(1)} %get-tuple-element.19), channel_id=1, replica_groups=mesh['sp'=128,'tp'=8] {'tp'}, dimensions={0}, use_global_device_ids=true | all-gather | bytes 663552 | tf_op jit(solution)/shard_map/all_gather | solution.py:322
  28.1 0.0 copy-start.2
  28.1 0.0 copy-start.3
  28.1 3.3 %shard_map.146 = (bf16[128,8,128]{2,1,0:T(8,128)(2,1)}, bf16[128,512]{1,0:T(8,128)(2,1)}, f32[8,128]{1,0:T(8,128)S(1)}) custom-call(bf16[8,144,256]{2,1,0:T(8,128)(2,1)S(1)} %all_gather.3.tok, bf16[2,2048]{1,0:T(2,128)(2,1)S(1)} %get-tuple-element.20.gw, f32[1,2]{1,0:T(1,128)S(1)} %get-tuple-element.21.bias, bf16[2048,256]{1,0:T(8,128)(2,1)} %kw_hbm.1, ...), custom_call_target="tpu_custom_call" | custom-call | flops 1000000000 | bytes 1000000 | tf_op jit(solution)/shard_map/pallas_call | solution.py:31
  31.5 0.0 copy-start.1
  31.5 13.8 %all-to-all-start = ((bf16[128,8,128]{2,1,0:T(8,128)(2,1)}), bf16[128,8,128]{2,1,0:T(8,128)(2,1)S(1)}, u32[]{:S(2)}, u32[]{:S(2)}) async-start(bf16[128,8,128]{2,1,0:T(8,128)(2,1)} %get-tuple-element.22), calls=%async_computation | async-start | bytes 524288 | tf_op jit(solution)/shard_map/all_to_all | solution.py:302
  45.3 0.0 copy-done.2
  45.3 0.0 copy-done.3
  45.3 0.0 copy-done.1
  45.3 0.0 copy-start.4
  45.4 0.6 shard_map.147
  45.9 2.5 %collective-permute-start = (bf16[16,128]{1,0:T(8,128)(2,1)S(1)}, bf16[16,128]{1,0:T(8,128)(2,1)S(1)}, u32[]{:S(2)}, u32[]{:S(2)}) collective-permute-start(bf16[16,128]{1,0:T(8,128)(2,1)S(1)} %get-tuple-element.24), channel_id=1, source_target_pairs={{0,8},{8,16},{16,24},{24,32},{32,40},{40,48},{48,56},{56,64},{64,7... | collective-permute-start | bytes 12296 | tf_op jit(solution)/shard_map/ppermute | solution.py:334
  48.4 0.7 collective-permute-done.halo
  49.2 0.0 copy-done.4
  49.2 0.3 shard_map.148
  49.5 3.5 %collective-permute-start.1 = (bf16[128,1024]{1,0:T(8,128)(2,1)S(1)}, bf16[128,1024]{1,0:T(8,128)(2,1)S(1)}, u32[]{:S(2)}, u32[]{:S(2)}) collective-permute-start(bf16[128,1024]{1,0:T(8,128)(2,1)S(1)} %get-tuple-element.28), channel_id=1, source_target_pairs={{0,1},{1,0},{2,3},{3,2},{4,5},{5,4},{6,7},{7,6},{8,9},{9,8},{10,11... | collective-permute-start | bytes 786440 | tf_op jit(solution)/shard_map/ppermute | solution.py:345
  53.0 1.1 collective-permute-done.1._.other
  54.1 8.5 %all-to-all-done.arrived = bf16[128,8,128]{2,1,0:T(8,128)(2,1)S(1)} async-done(((bf16[128,8,128]{2,1,0:T(8,128)(2,1)}), bf16[128,8,128]{2,1,0:T(8,128)(2,1)S(1)}, u32[]{:S(2)}, u32[]{:S(2)}) %all-to-all-start) | async-done | bytes 262176 | tf_op jit(solution)/shard_map/all_to_all | solution.py:302
  62.6 2.2 %shard_map.149 = (bf16[128,4,128]{2,1,0:T(4,128)(2,1)}, f32[8,128]{1,0:T(8,128)S(1)}) custom-call(s32[1]{0:T(128)} %bitcast.place, bf16[128,8,128]{2,1,0:T(8,128)(2,1)S(1)} %all-to-all-done.arrived, bf16[128,1024]{1,0:T(8,128)(2,1)S(1)} %collective-permute-done.1._.other), custom_call_target="tpu_custom_call" | custom-call | flops 1000000000 | bytes 1000000 | tf_op jit(solution)/shard_map/pallas_call | solution.py:31
  64.8 13.8 %all-to-all-start.1 = ((bf16[128,4,128]{2,1,0:T(4,128)(2,1)}), bf16[128,4,128]{2,1,0:T(4,128)(2,1)S(1)}, u32[]{:S(2)}, u32[]{:S(2)}) async-start(bf16[128,4,128]{2,1,0:T(4,128)(2,1)} %get-tuple-element.29), calls=%async_computation.1 | async-start | bytes 262144 | tf_op jit(solution)/shard_map/all_to_all | solution.py:302
  78.6 0.0 copy-start
  78.6 3.8 %shard_map.150.pack = f32[128,896]{1,0:T(8,128)} custom-call(bf16[8,144,256]{2,1,0:T(8,128)(2,1)S(1)} %all_gather.3.tok, f32[8,128]{1,0:T(8,128)S(1)} %get-tuple-element.23.aux, bf16[128,512]{1,0:T(8,128)(2,1)} %get-tuple-element.31.kv, bf16[2048,256]{1,0:T(8,128)(2,1)} %qw_hbm.1, bf16[2048,256]{1,0:T(8,128)(2,1)} %ow_hbm.1, bf16[256]{0:T(256)(128)(2,1)} %gain.1), custom_call_target="tpu_custom_call" | custom-call | flops 1000000000 | bytes 1000000 | tf_op jit(solution)/shard_map/pallas_call | solution.py:31
  82.4 11.6 %all-to-all-done.1.arrived = bf16[128,4,128]{2,1,0:T(4,128)(2,1)S(1)} async-done(((bf16[128,4,128]{2,1,0:T(4,128)(2,1)}), bf16[128,4,128]{2,1,0:T(4,128)(2,1)S(1)}, u32[]{:S(2)}, u32[]{:S(2)}) %all-to-all-start.1) | async-done | bytes 131104 | tf_op jit(solution)/shard_map/all_to_all | solution.py:302
  94.1 0.0 copy-done
  94.1 0.0 copy-start.5
  94.1 1.0 copy-done.5
  95.1 0.7 shard_map.151
  95.8 19.5 %all_to_all.15.arrived = bf16[8,16,3200]{2,1,0:T(8,128)(2,1)S(1)} all-to-all(bf16[8,16,3200]{2,1,0:T(8,128)(2,1)S(1)} %shard_map.151), channel_id=1, replica_groups=mesh['sp'=128,'tp'=8] {'tp'}, dimensions={0} | all-to-all | bytes 1638400 | tf_op jit(solution)/shard_map/all_to_all | solution.py:302
  115.4 0.8 shard_map.152
Async XLA Ops:
  28.1 17.2 %copy-start.2 = (bf16[2048,128]{1,0:T(8,128)(2,1)S(1)}, bf16[2048,128]{1,0:T(8,128)(2,1)}, u32[]{:S(2)}) copy-start(bf16[2048,128]{1,0:T(8,128)(2,1)} %cw.1) | copy-start | bytes 1572868
  28.1 17.2 %copy-start.3 = (bf16[2048,128]{1,0:T(8,128)(2,1)S(1)}, bf16[2048,128]{1,0:T(8,128)(2,1)}, u32[]{:S(2)}) copy-start(bf16[2048,128]{1,0:T(8,128)(2,1)} %uw.1) | copy-start | bytes 1572868
  31.5 13.9 %copy-start.1 = (bf16[2048,128]{1,0:T(8,128)(2,1)S(1)}, bf16[2048,128]{1,0:T(8,128)(2,1)}, u32[]{:S(2)}) copy-start(bf16[2048,128]{1,0:T(8,128)(2,1)} %bw.1) | copy-start | bytes 1572868
  31.5 31.2 %all-to-all-start = ((bf16[128,8,128]{2,1,0:T(8,128)(2,1)}), bf16[128,8,128]{2,1,0:T(8,128)(2,1)S(1)}, u32[]{:S(2)}, u32[]{:S(2)}) async-start(bf16[128,8,128]{2,1,0:T(8,128)(2,1)} %get-tuple-element.22), calls=%async_computation | async-start | bytes 524288 | tf_op jit(solution)/shard_map/all_to_all | solution.py:302
  45.3 3.8 %copy-start.4 = (bf16[128,2048]{1,0:T(8,128)(2,1)S(1)}, bf16[128,2048]{1,0:T(8,128)(2,1)}, u32[]{:S(2)}) copy-start(bf16[128,2048]{1,0:T(8,128)(2,1)} %weight.2) | copy-start | bytes 1572868
  45.9 3.2 %collective-permute-start = (bf16[16,128]{1,0:T(8,128)(2,1)S(1)}, bf16[16,128]{1,0:T(8,128)(2,1)S(1)}, u32[]{:S(2)}, u32[]{:S(2)}) collective-permute-start(bf16[16,128]{1,0:T(8,128)(2,1)S(1)} %get-tuple-element.24), channel_id=1, source_target_pairs={{0,8},{8,16},{16,24},{24,32},{32,40},{40,48},{48,56},{56,64},{64,7... | collective-permute-start | bytes 12296 | tf_op jit(solution)/shard_map/ppermute | solution.py:334
  49.5 4.6 %collective-permute-start.1 = (bf16[128,1024]{1,0:T(8,128)(2,1)S(1)}, bf16[128,1024]{1,0:T(8,128)(2,1)S(1)}, u32[]{:S(2)}, u32[]{:S(2)}) collective-permute-start(bf16[128,1024]{1,0:T(8,128)(2,1)S(1)} %get-tuple-element.28), channel_id=1, source_target_pairs={{0,1},{1,0},{2,3},{3,2},{4,5},{5,4},{6,7},{7,6},{8,9},{9,8},{10,11... | collective-permute-start | bytes 786440 | tf_op jit(solution)/shard_map/ppermute | solution.py:345
  64.8 29.3 %all-to-all-start.1 = ((bf16[128,4,128]{2,1,0:T(4,128)(2,1)}), bf16[128,4,128]{2,1,0:T(4,128)(2,1)S(1)}, u32[]{:S(2)}, u32[]{:S(2)}) async-start(bf16[128,4,128]{2,1,0:T(4,128)(2,1)} %get-tuple-element.29), calls=%async_computation.1 | async-start | bytes 262144 | tf_op jit(solution)/shard_map/all_to_all | solution.py:302
  78.6 15.5 %copy-start = (bf16[256,2048]{1,0:T(8,128)(2,1)S(1)}, bf16[256,2048]{1,0:T(8,128)(2,1)}, u32[]{:S(2)}) copy-start(bf16[256,2048]{1,0:T(8,128)(2,1)} %weight.3) | copy-start | bytes 3145732
  94.1 1.0 copy-start.5

commit v7 on v6

--- a/solution.py
+++ b/solution.py
@@ -76,9 +76,12 @@
     return copies
 
 
-def prepare(tok_hbm, gain_hbm, gw_hbm, bias_hbm, taps_hbm, out, gw, bias, taps, tok, gain, sems):
-    for c in fetched([(tok_hbm, tok), (gain_hbm, gain), (gw_hbm, gw), (bias_hbm, bias), (taps_hbm, taps)], sems):
-        c.wait()
+def prepare(tok_hbm, gain_hbm, *rest):
+    count = (len(rest) - 4) // 2
+    sources, out, places, (tok, gain, sems) = rest[:count], rest[count], rest[count + 1 : -3], rest[-3:]
+    copies = fetched([(tok_hbm, tok), (gain_hbm, gain), *zip(sources, places)], sems)
+    copies[0].wait()
+    copies[1].wait()
     wide = tok[...].astype(F32)
     out[0, :N, :] = (wide * gain[...].astype(F32)).astype(BF)
     squares = to_row(jnp.sum(wide * wide, axis=1, keepdims=True))
@@ -87,6 +90,8 @@
     tail = jnp.concatenate([hi.astype(F32), mid.astype(F32), low.astype(F32), zero], axis=0)
     out[0, N:, :N] = tail.astype(BF)
     out[0, N:, N:] = jnp.zeros((16, N), BF)
+    for c in copies[2:]:
+        c.wait()
 
 
 def cuts(sources, places):
@@ -114,9 +119,8 @@
     return -(jnp.maximum(-x, 0.0) + jnp.where(e < 0.01, series, jnp.log(1.0 + e)))
 
 
-def states(tok, gw, bias, kw_hbm, vw_hbm, message, kv, aux, state, kw, vw, sems):
+def states(tok, gw, bias, kw, vw, message, kv, aux, state):
     groups, _, part = tok.shape
-    copies = fetched(cuts((kw_hbm, vw_hbm), (kw, vw)), sems)
     g_sum = jnp.zeros((N, 2), F32)
     sq = jnp.zeros((1, N), F32)
     for g in range(groups):
@@ -138,7 +142,7 @@
     weight = after + i_col
     top = jnp.max(weight, axis=0, keepdims=True)
     weight = jnp.exp(weight - top)
-    k_sum, v_sum = products(tok, (kw, vw), copies)
+    k_sum, v_sum = products(tok, (kw, vw))
     k = (inv * k_sum).astype(BF)
     v = (inv * v_sum).astype(BF)
     kv[:, :HD] = k
@@ -165,7 +169,7 @@
     aux[...] = jnp.concatenate([b_row, i_row, to_row(inv), jnp.zeros((5, N), F32)], axis=0)
 
 
-def carry(place, arrived, _, message, own, state, back):
+def carry(place, arrived, message, own, state, back):
     count, rows, _ = arrived.shape
     slab = rows - 4
     state[...] = arrived[...].astype(F32)
@@ -313,18 +317,18 @@
     sems = lambda n: [pltpu.SemaphoreType.DMA((n,))]
     room = lambda *arrays: [pltpu.VMEM(a.shape, a.dtype) for a in arrays]
     sems = lambda *ns: [pltpu.SemaphoreType.DMA((n,)) for n in ns]
-    small = (gate_w.reshape(model, 2).T, gate_bias.reshape(1, 2), conv_taps)
-    local, gate_wt, biases, taps = call(
+    small = (gate_w.reshape(model, 2).T, gate_bias.reshape(1, 2), conv_taps, key_w, value_w)
+    local, gate_wt, biases, taps, key_v, value_v = call(
         prepare,
         [((1, N + 16, tokens.shape[1]), BF, V)] + [(a.shape, a.dtype, V) for a in small],
-        tokens, norm_gain, *small, places=[H] * 5, scratch=room(tokens, norm_gain) + sems(5),
+        tokens, norm_gain, *small, places=[H] * 7, scratch=room(tokens, norm_gain) + sems(7),
     )
     tok = lax.all_gather(local, TP, axis=0, tiled=True)
     message, kv, aux = call(
         states,
         [((count, rows + 4, N), BF, A), ((N, 2 * HD), BF, A), ((8, N), F32, V)],
-        tok, gate_wt, biases, key_w, value_w, flops=10**9, places=[V, V, V, H, H],
-        scratch=[pltpu.VMEM((count, rows + 4, N), F32)] + room(key_w, value_w) + sems(2 * CHUNKS),
+        tok, gate_wt, biases, key_v, value_v, flops=10**9, places=[V] * 5,
+        scratch=[pltpu.VMEM((count, rows + 4, N), F32)],
     )
     arrived = exchange(message, SP)
     gate_b, mixed, edge = call(
@@ -347,7 +351,7 @@
     back, own = call(
         carry,
         [((count, rows, N), BF, V), ((8, N), F32, V)],
-        place, arrived, other, flops=10**9, places=[S, V, V], limit=16,
+        place, arrived, flops=10**9, places=[S, V], limit=16,
         scratch=[pltpu.VMEM((count, rows + 4, N), F32), pltpu.VMEM((count, rows, N), F32)],
     )
     state = exchange(back, SP)

time: 117 us -> 114 us (0.974)
    all_to_all x2, starting transfers between devices: 27.6 us -> 26.1 us  [exchange(): return lax.all_to_all(value, axis, split_axis=0, concat_axis=0, tiled=True)]
  transfers between devices with their start and end apart: 4 -> 4, of which waited for: 4 -> 3; matrix products, arithmetic and copies ran while one was open for 0% -> 0% of each run, Pallas kernels for 4% -> 4%
where the time goes in v7:
time: 114 us
  blocking collectives  46.8 us (41%)
  starting transfers between devices  32.7 us (29%)
  waiting for transfers between devices  21.3 us (19%)
  Pallas kernels  11.9 us (10%)
    all_gather x1, blocking collectives, body(): tok = lax.all_gather(local, TP, axis=0, tiled=True)  27.1 us
    all_to_all x2, starting transfers between devices, exchange(): return lax.all_to_all(value, axis, split_axis=0, concat_axis=0, tiled=True)  26.1 us
    all_to_all x2, waiting for transfers between devices, exchange(): return lax.all_to_all(value, axis, split_axis=0, concat_axis=0, tiled=True)  20.6 us
    all_to_all x1, blocking collectives, exchange(): return lax.all_to_all(value, axis, split_axis=0, concat_axis=0, tiled=True)  19.7 us
    pallas_call x8, Pallas kernels, call(): pl.pallas_call(kernel, out_shape=outs, in_specs=[pl.BlockSpec(memory_spac...  11.9 us
    ppermute x1, starting transfers between devices, body(): other = lax.ppermute(send, TP, [(i, i ^ 1) for i in range(groups)])  4.18 us
    ppermute x1, starting transfers between devices, body(): halo = lax.ppermute(edge, SP, [(i, i + 1) for i in range(count - 1)])  2.48 us
  transfers between devices with their start and end apart: 4, of which 3 were waited for; matrix products, arithmetic and copies ran while one was open for 0% of the time, Pallas kernels for 4%

profile of v7, /device:TPU:1, one launch (start us, length us, event | category | flops | bytes accessed | tf_op | source)
XLA Modules:
  0.0 114.0 jit_solution(11325170060329905584)
XLA Ops:
  0.0 1.7 %shard_map.145 = (bf16[1,144,256]{2,1,0:T(8,128)(2,1)S(1)}, bf16[2,2048]{1,0:T(2,128)(2,1)S(1)}, f32[1,2]{1,0:T(1,128)S(1)}, bf16[3,128]{1,0:T(4,128)(2,1)S(1)},...) custom-call(bf16[128,256]{1,0:T(8,128)(2,1)} %tok_hbm.1, bf16[1,256]{1,0:T(2,128)(2,1)} %gain_hbm.1, ...), custom_call_target="tpu_custom_call" | custom-call | tf_op jit(solution)/shard_map/pallas_call | solution.py:31
  1.7 27.1 %all_gather.3.tok = bf16[8,144,256]{2,1,0:T(8,128)(2,1)S(1)} all-gather(bf16[1,144,256]{2,1,0:T(8,128)(2,1)S(1)} %get-tuple-element.21), channel_id=1, replica_groups=mesh['sp'=128,'tp'=8] {'tp'}, dimensions={0}, use_global_device_ids=true | all-gather | bytes 663552 | tf_op jit(solution)/shard_map/all_gather | solution.py:326
  28.8 1.8 %shard_map.146 = (bf16[128,8,128]{2,1,0:T(8,128)(2,1)}, bf16[128,512]{1,0:T(8,128)(2,1)}, f32[8,128]{1,0:T(8,128)S(1)}) custom-call(bf16[8,144,256]{2,1,0:T(8,128)(2,1)S(1)} %all_gather.3.tok, bf16[2,2048]{1,0:T(2,128)(2,1)S(1)} %get-tuple-element.22.gw, f32[1,2]{1,0:T(1,128)S(1)} %get-tuple-element.23.bias, bf16[2048,256]{1,0:T(8,128)(2,1)S(1)} %get-tuple-element.24.kw, ...), custom_call_target="tpu_custom_call" | custom-call | flops 1000000000 | bytes 1000000 | tf_op jit(solution)/shard_map/pallas_call | solution.py:31
  30.6 13.7 %all-to-all-start = ((bf16[128,8,128]{2,1,0:T(8,128)(2,1)}), bf16[128,8,128]{2,1,0:T(8,128)(2,1)S(1)}, u32[]{:S(2)}, u32[]{:S(2)}) async-start(bf16[128,8,128]{2,1,0:T(8,128)(2,1)} %get-tuple-element.26), calls=%async_computation | async-start | bytes 524288 | tf_op jit(solution)/shard_map/all_to_all | solution.py:306
  44.4 17.3 %all-to-all-done.arrived = bf16[128,8,128]{2,1,0:T(8,128)(2,1)S(1)} async-done(((bf16[128,8,128]{2,1,0:T(8,128)(2,1)}), bf16[128,8,128]{2,1,0:T(8,128)(2,1)S(1)}, u32[]{:S(2)}, u32[]{:S(2)}) %all-to-all-start) | async-done | bytes 262176 | tf_op jit(solution)/shard_map/all_to_all | solution.py:306
  61.7 0.0 copy-start.1
  61.7 0.0 copy-start.2
  61.7 0.0 copy-start.3
  61.7 2.2 %shard_map.147 = (bf16[128,4,128]{2,1,0:T(4,128)(2,1)}, f32[8,128]{1,0:T(8,128)S(1)}) custom-call(s32[1]{0:T(128)} %bitcast.place, bf16[128,8,128]{2,1,0:T(8,128)(2,1)S(1)} %all-to-all-done.arrived), custom_call_target="tpu_custom_call" | custom-call | flops 1000000000 | bytes 1000000 | tf_op jit(solution)/shard_map/pallas_call | solution.py:31
  63.8 12.4 %all-to-all-start.1 = ((bf16[128,4,128]{2,1,0:T(4,128)(2,1)}), bf16[128,4,128]{2,1,0:T(4,128)(2,1)S(1)}, u32[]{:S(2)}, u32[]{:S(2)}) async-start(bf16[128,4,128]{2,1,0:T(4,128)(2,1)} %get-tuple-element.27), calls=%async_computation.1 | async-start | bytes 262144 | tf_op jit(solution)/shard_map/all_to_all | solution.py:306
  76.2 0.0 copy-done.1
  76.2 0.0 copy-done.2
  76.2 0.0 copy-done.3
  76.2 0.0 copy-start.4
  76.3 0.6 shard_map.149
  76.8 2.5 %collective-permute-start = (bf16[16,128]{1,0:T(8,128)(2,1)S(1)}, bf16[16,128]{1,0:T(8,128)(2,1)S(1)}, u32[]{:S(2)}, u32[]{:S(2)}) collective-permute-start(bf16[16,128]{1,0:T(8,128)(2,1)S(1)} %get-tuple-element.31), channel_id=1, source_target_pairs={{0,8},{8,16},{16,24},{24,32},{32,40},{40,48},{48,56},{56,64},{64,7... | collective-permute-start | bytes 12296 | tf_op jit(solution)/shard_map/ppermute | solution.py:338
  79.3 0.7 collective-permute-done.halo
  80.1 0.0 copy-done.4
  80.1 0.3 shard_map.150
  80.4 4.2 %collective-permute-start.1 = (bf16[128,1024]{1,0:T(8,128)(2,1)S(1)}, bf16[128,1024]{1,0:T(8,128)(2,1)S(1)}, u32[]{:S(2)}, u32[]{:S(2)}) collective-permute-start(bf16[128,1024]{1,0:T(8,128)(2,1)S(1)} %get-tuple-element.36), channel_id=1, source_target_pairs={{0,1},{1,0},{2,3},{3,2},{4,5},{5,4},{6,7},{7,6},{8,9},{9,8},{10,11... | collective-permute-start | bytes 786440 | tf_op jit(solution)/shard_map/ppermute | solution.py:349
  84.5 0.0 copy-start
  84.6 3.8 %shard_map.148.pack = f32[128,896]{1,0:T(8,128)} custom-call(bf16[8,144,256]{2,1,0:T(8,128)(2,1)S(1)} %all_gather.3.tok, f32[8,128]{1,0:T(8,128)S(1)} %get-tuple-element.29.aux, bf16[128,512]{1,0:T(8,128)(2,1)} %get-tuple-element.30.kv, bf16[2048,256]{1,0:T(8,128)(2,1)} %qw_hbm.1, bf16[2048,256]{1,0:T(8,128)(2,1)} %ow_hbm.1, bf16[256]{0:T(256)(128)(2,1)} %gain.1), custom_call_target="tpu_custom_call" | custom-call | flops 1000000000 | bytes 1000000 | tf_op jit(solution)/shard_map/pallas_call | solution.py:31
  88.4 0.0 collective-permute-done.1.other
  88.4 3.3 %all-to-all-done.1.arrived = bf16[128,4,128]{2,1,0:T(4,128)(2,1)S(1)} async-done(((bf16[128,4,128]{2,1,0:T(4,128)(2,1)}), bf16[128,4,128]{2,1,0:T(4,128)(2,1)S(1)}, u32[]{:S(2)}, u32[]{:S(2)}) %all-to-all-start.1) | async-done | bytes 131104 | tf_op jit(solution)/shard_map/all_to_all | solution.py:306
  91.7 0.0 copy-done
  91.7 0.0 copy-start.5
  91.7 1.0 copy-done.5
  92.7 0.7 shard_map.151
  93.5 19.7 %all_to_all.15.arrived = bf16[8,16,3200]{2,1,0:T(8,128)(2,1)S(1)} all-to-all(bf16[8,16,3200]{2,1,0:T(8,128)(2,1)S(1)} %shard_map.151), channel_id=1, replica_groups=mesh['sp'=128,'tp'=8] {'tp'}, dimensions={0} | all-to-all | bytes 1638400 | tf_op jit(solution)/shard_map/all_to_all | solution.py:306
  113.1 0.8 shard_map.152
Async XLA Ops:
  30.6 31.0 %all-to-all-start = ((bf16[128,8,128]{2,1,0:T(8,128)(2,1)}), bf16[128,8,128]{2,1,0:T(8,128)(2,1)S(1)}, u32[]{:S(2)}, u32[]{:S(2)}) async-start(bf16[128,8,128]{2,1,0:T(8,128)(2,1)} %get-tuple-element.26), calls=%async_computation | async-start | bytes 524288 | tf_op jit(solution)/shard_map/all_to_all | solution.py:306
  61.7 14.6 %copy-start.1 = (bf16[2048,128]{1,0:T(8,128)(2,1)S(1)}, bf16[2048,128]{1,0:T(8,128)(2,1)}, u32[]{:S(2)}) copy-start(bf16[2048,128]{1,0:T(8,128)(2,1)} %bw.1) | copy-start | bytes 1572868
  61.7 14.6 %copy-start.2 = (bf16[2048,128]{1,0:T(8,128)(2,1)S(1)}, bf16[2048,128]{1,0:T(8,128)(2,1)}, u32[]{:S(2)}) copy-start(bf16[2048,128]{1,0:T(8,128)(2,1)} %cw.1) | copy-start | bytes 1572868
  61.7 14.6 %copy-start.3 = (bf16[2048,128]{1,0:T(8,128)(2,1)S(1)}, bf16[2048,128]{1,0:T(8,128)(2,1)}, u32[]{:S(2)}) copy-start(bf16[2048,128]{1,0:T(8,128)(2,1)} %uw.1) | copy-start | bytes 1572868
  63.8 27.9 %all-to-all-start.1 = ((bf16[128,4,128]{2,1,0:T(4,128)(2,1)}), bf16[128,4,128]{2,1,0:T(4,128)(2,1)S(1)}, u32[]{:S(2)}, u32[]{:S(2)}) async-start(bf16[128,4,128]{2,1,0:T(4,128)(2,1)} %get-tuple-element.27), calls=%async_computation.1 | async-start | bytes 262144 | tf_op jit(solution)/shard_map/all_to_all | solution.py:306
  76.2 3.8 %copy-start.4 = (bf16[128,2048]{1,0:T(8,128)(2,1)S(1)}, bf16[128,2048]{1,0:T(8,128)(2,1)}, u32[]{:S(2)}) copy-start(bf16[128,2048]{1,0:T(8,128)(2,1)} %weight.2) | copy-start | bytes 1572868
  76.8 3.2 %collective-permute-start = (bf16[16,128]{1,0:T(8,128)(2,1)S(1)}, bf16[16,128]{1,0:T(8,128)(2,1)S(1)}, u32[]{:S(2)}, u32[]{:S(2)}) collective-permute-start(bf16[16,128]{1,0:T(8,128)(2,1)S(1)} %get-tuple-element.31), channel_id=1, source_target_pairs={{0,8},{8,16},{16,24},{24,32},{32,40},{40,48},{48,56},{56,64},{64,7... | collective-permute-start | bytes 12296 | tf_op jit(solution)/shard_map/ppermute | solution.py:338
  80.4 8.0 %collective-permute-start.1 = (bf16[128,1024]{1,0:T(8,128)(2,1)S(1)}, bf16[128,1024]{1,0:T(8,128)(2,1)S(1)}, u32[]{:S(2)}, u32[]{:S(2)}) collective-permute-start(bf16[128,1024]{1,0:T(8,128)(2,1)S(1)} %get-tuple-element.36), channel_id=1, source_target_pairs={{0,1},{1,0},{2,3},{3,2},{4,5},{5,4},{6,7},{7,6},{8,9},{9,8},{10,11... | collective-permute-start | bytes 786440 | tf_op jit(solution)/shard_map/ppermute | solution.py:349
  84.5 7.2 %copy-start = (bf16[256,2048]{1,0:T(8,128)(2,1)S(1)}, bf16[256,2048]{1,0:T(8,128)(2,1)}, u32[]{:S(2)}) copy-start(bf16[256,2048]{1,0:T(8,128)(2,1)} %weight.3) | copy-start | bytes 3145732
  91.7 1.0 copy-start.5

commit v8 on v7

--- a/solution.py
+++ b/solution.py
@@ -12,6 +12,7 @@
 MDIM = 2048
 EPS = 1e-06
 OWN = 56
+FIRST = 84
 CHUNKS = 4
 LOWEST = -1e30
 TP = "tp"
@@ -173,11 +174,12 @@
     count, rows, _ = arrived.shape
     slab = rows - 4
     state[...] = arrived[...].astype(F32)
-    source = lax.broadcasted_iota(jnp.int32, (count, count), 1)
-    target = lax.broadcasted_iota(jnp.int32, (count, count), 0)
+    column = lax.broadcasted_iota(jnp.int32, (count, count), 1)
+    line = lax.broadcasted_iota(jnp.int32, (count, count), 0)
+    source, target = (column + FIRST) % count, (line + FIRST) % count
     lines = state[:, slab + 2, :]
     tops = lines[:, 3:4] + lines[:, 4:5] + lines[:, 5:6]
-    tops = jnp.sum(jnp.where(source == target, tops, 0.0), axis=0, keepdims=True)
+    tops = jnp.sum(jnp.where(column == line, tops, 0.0), axis=0, keepdims=True)
     later = jnp.where(source < target, 1.0, 0.0)
     past = later.astype(BF)
     decay = jnp.zeros((count, count), F32)
@@ -188,7 +190,7 @@
     weights = jnp.where(source < target, jnp.exp(logs - top), 0.0)
     hi = weights.astype(BF)
     low = (weights - hi.astype(F32)).astype(BF)
-    mine = lax.broadcasted_iota(jnp.int32, (count, 1), 0) == place[0]
+    mine = (lax.broadcasted_iota(jnp.int32, (count, 1), 0) + FIRST) % count == place[0]
     pick = lambda a: jnp.sum(jnp.where(mine, a, 0.0), axis=0, keepdims=True)
     lane = lax.broadcasted_iota(jnp.int32, (1, N), 1)
     parts = [state[:, r, :] for r in range(rows)]
@@ -302,8 +304,10 @@
         out[:, at] = (c + scale * m).astype(BF)
 
 
-def exchange(value, axis):
-    return lax.all_to_all(value, axis, split_axis=0, concat_axis=0, tiled=True)
+def exchange(value, axis, first=0):
+    count = lax.axis_size(axis)
+    order = [[(i + first) % count for i in range(count)]] if first else None
+    return lax.all_to_all(value, axis, split_axis=0, concat_axis=0, tiled=True, axis_index_groups=order)
 
 
 def body(tokens, norm_gain, conv_b_w, conv_c_w, conv_u_w, conv_taps, query_w, key_w, value_w, outgate_w,
@@ -330,7 +334,7 @@
         tok, gate_wt, biases, key_v, value_v, flops=10**9, places=[V] * 5,
         scratch=[pltpu.VMEM((count, rows + 4, N), F32)],
     )
-    arrived = exchange(message, SP)
+    arrived = exchange(message, SP, FIRST % count)
     gate_b, mixed, edge = call(
         mixing, [((N, N), BF, V), ((N, N), BF, V), ((16, N), BF, V)], tok, aux, conv_b_w, conv_c_w,
         conv_u_w, flops=10**9, places=[V] * 5, limit=16,
@@ -354,7 +358,7 @@
         place, arrived, flops=10**9, places=[S, V], limit=16,
         scratch=[pltpu.VMEM((count, rows + 4, N), F32), pltpu.VMEM((count, rows, N), F32)],
     )
-    state = exchange(back, SP)
+    state = exchange(back, SP, FIRST % count)
     (mem,) = call(
         finish, [((groups, N // groups, 3 * model // 2 + N), BF, V)], state, own, pack, keep, other, mem_out_w,
         flops=10**9, scratch=[pltpu.VMEM((count, rows, N), F32)], places=[V] * 6, limit=16,

time: 114 us -> 115 us (level)
  the two profiles are of different devices: /device:TPU:1 before, /device:TPU:65 now
where the time goes in v8:
time: 115 us
  starting transfers between devices  53.8 us (47%)
  blocking collectives  30.6 us (27%)
  waiting for transfers between devices  17.2 us (15%)
  Pallas kernels  11.9 us (10%)
    all_to_all x2, starting transfers between devices, exchange(): lax.all_to_all(value, axis, split_axis=0, concat_axis=0, tiled=True, axis...  46.7 us
    all_to_all x1, blocking collectives, exchange(): lax.all_to_all(value, axis, split_axis=0, concat_axis=0, tiled=True, axis...  16.5 us
    all_gather x1, blocking collectives, body(): tok = lax.all_gather(local, TP, axis=0, tiled=True)  14 us
    all_to_all x2, waiting for transfers between devices, exchange(): lax.all_to_all(value, axis, split_axis=0, concat_axis=0, tiled=True, axis...  12.7 us
    pallas_call x8, Pallas kernels, call(): pl.pallas_call(kernel, out_shape=outs, in_specs=[pl.BlockSpec(memory_spac...  11.9 us
    ppermute x1, starting transfers between devices, body(): other = lax.ppermute(send, TP, [(i, i ^ 1) for i in range(groups)])  4.92 us
    ppermute x1, waiting for transfers between devices, body(): halo = lax.ppermute(edge, SP, [(i, i + 1) for i in range(count - 1)])  4.54 us
  transfers between devices with their start and end apart: 4, of which 2 were waited for; matrix products, arithmetic and copies ran while one was open for 0% of the time, Pallas kernels for 4%

profile of v8, /device:TPU:65, one launch (start us, length us, event | category | flops | bytes accessed | tf_op | source)
XLA Modules:
  0.0 114.7 jit_solution(2126132544370774111)
XLA Ops:
  0.0 1.7 %shard_map.145 = (bf16[1,144,256]{2,1,0:T(8,128)(2,1)S(1)}, bf16[2,2048]{1,0:T(2,128)(2,1)S(1)}, f32[1,2]{1,0:T(1,128)S(1)}, bf16[3,128]{1,0:T(4,128)(2,1)S(1)},...) custom-call(bf16[128,256]{1,0:T(8,128)(2,1)} %tok_hbm.1, bf16[1,256]{1,0:T(2,128)(2,1)} %gain_hbm.1, ...), custom_call_target="tpu_custom_call" | custom-call | tf_op jit(solution)/shard_map/pallas_call | solution.py:32
  1.7 14.0 %all_gather.3.tok = bf16[8,144,256]{2,1,0:T(8,128)(2,1)S(1)} all-gather(bf16[1,144,256]{2,1,0:T(8,128)(2,1)S(1)} %get-tuple-element.21), channel_id=1, replica_groups=mesh['sp'=128,'tp'=8] {'tp'}, dimensions={0}, use_global_device_ids=true | all-gather | bytes 663552 | tf_op jit(solution)/shard_map/all_gather | solution.py:330
  15.8 1.8 %shard_map.146 = (bf16[128,8,128]{2,1,0:T(8,128)(2,1)}, bf16[128,512]{1,0:T(8,128)(2,1)}, f32[8,128]{1,0:T(8,128)S(1)}) custom-call(bf16[8,144,256]{2,1,0:T(8,128)(2,1)S(1)} %all_gather.3.tok, bf16[2,2048]{1,0:T(2,128)(2,1)S(1)} %get-tuple-element.22.gw, f32[1,2]{1,0:T(1,128)S(1)} %get-tuple-element.23.bias, bf16[2048,256]{1,0:T(8,128)(2,1)S(1)} %get-tuple-element.24.kw, ...), custom_call_target="tpu_custom_call" | custom-call | flops 1000000000 | bytes 1000000 | tf_op jit(solution)/shard_map/pallas_call | solution.py:32
  17.6 29.6 %all-to-all-start = ((bf16[128,8,128]{2,1,0:T(8,128)(2,1)}), bf16[128,8,128]{2,1,0:T(8,128)(2,1)S(1)}, u32[]{:S(2)}, u32[]{:S(2)}) async-start(bf16[128,8,128]{2,1,0:T(8,128)(2,1)} %get-tuple-element.26), calls=%async_computation | async-start | bytes 524288 | tf_op jit(solution)/shard_map/all_to_all | solution.py:310
  47.1 12.7 %all-to-all-done.arrived = bf16[128,8,128]{2,1,0:T(8,128)(2,1)S(1)} async-done(((bf16[128,8,128]{2,1,0:T(8,128)(2,1)}), bf16[128,8,128]{2,1,0:T(8,128)(2,1)S(1)}, u32[]{:S(2)}, u32[]{:S(2)}) %all-to-all-start) | async-done | bytes 262176 | tf_op jit(solution)/shard_map/all_to_all | solution.py:310
  59.8 0.0 copy-start.1
  59.8 0.0 copy-start.2
  59.8 0.0 copy-start.3
  59.8 2.2 %shard_map.147 = (bf16[128,4,128]{2,1,0:T(4,128)(2,1)}, f32[8,128]{1,0:T(8,128)S(1)}) custom-call(s32[1]{0:T(128)} %bitcast.place, bf16[128,8,128]{2,1,0:T(8,128)(2,1)S(1)} %all-to-all-done.arrived), custom_call_target="tpu_custom_call" | custom-call | flops 1000000000 | bytes 1000000 | tf_op jit(solution)/shard_map/pallas_call | solution.py:32
  62.0 17.1 %all-to-all-start.1 = ((bf16[128,4,128]{2,1,0:T(4,128)(2,1)}), bf16[128,4,128]{2,1,0:T(4,128)(2,1)S(1)}, u32[]{:S(2)}, u32[]{:S(2)}) async-start(bf16[128,4,128]{2,1,0:T(4,128)(2,1)} %get-tuple-element.27), calls=%async_computation.1 | async-start | bytes 262144 | tf_op jit(solution)/shard_map/all_to_all | solution.py:310
  79.1 0.0 copy-done.1
  79.1 0.0 copy-done.2
  79.1 0.0 copy-done.3
  79.1 0.0 copy-start.4
  79.1 0.6 shard_map.149
  79.7 2.2 %collective-permute-start = (bf16[16,128]{1,0:T(8,128)(2,1)S(1)}, bf16[16,128]{1,0:T(8,128)(2,1)S(1)}, u32[]{:S(2)}, u32[]{:S(2)}) collective-permute-start(bf16[16,128]{1,0:T(8,128)(2,1)S(1)} %get-tuple-element.31), channel_id=1, source_target_pairs={{0,8},{8,16},{16,24},{24,32},{32,40},{40,48},{48,56},{56,64},{64,7... | collective-permute-start | bytes 12296 | tf_op jit(solution)/shard_map/ppermute | solution.py:342
  81.9 4.5 %collective-permute-done.halo = bf16[16,128]{1,0:T(8,128)(2,1)S(1)} collective-permute-done((bf16[16,128]{1,0:T(8,128)(2,1)S(1)}, bf16[16,128]{1,0:T(8,128)(2,1)S(1)}, u32[]{:S(2)}, u32[]{:S(2)}) %collective-permute-start) | collective-permute-done | bytes 4128 | tf_op jit(solution)/shard_map/ppermute | solution.py:342
  86.5 0.0 copy-done.4
  86.5 0.3 shard_map.150
  86.8 4.9 %collective-permute-start.1 = (bf16[128,1024]{1,0:T(8,128)(2,1)S(1)}, bf16[128,1024]{1,0:T(8,128)(2,1)S(1)}, u32[]{:S(2)}, u32[]{:S(2)}) collective-permute-start(bf16[128,1024]{1,0:T(8,128)(2,1)S(1)} %get-tuple-element.36), channel_id=1, source_target_pairs={{0,1},{1,0},{2,3},{3,2},{4,5},{5,4},{6,7},{7,6},{8,9},{9,8},{10,11... | collective-permute-start | bytes 786440 | tf_op jit(solution)/shard_map/ppermute | solution.py:353
  91.7 0.0 copy-start
  91.7 3.8 %shard_map.148.pack = f32[128,896]{1,0:T(8,128)} custom-call(bf16[8,144,256]{2,1,0:T(8,128)(2,1)S(1)} %all_gather.3.tok, f32[8,128]{1,0:T(8,128)S(1)} %get-tuple-element.29.aux, bf16[128,512]{1,0:T(8,128)(2,1)} %get-tuple-element.30.kv, bf16[2048,256]{1,0:T(8,128)(2,1)} %qw_hbm.1, bf16[2048,256]{1,0:T(8,128)(2,1)} %ow_hbm.1, bf16[256]{0:T(256)(128)(2,1)} %gain.1), custom_call_target="tpu_custom_call" | custom-call | flops 1000000000 | bytes 1000000 | tf_op jit(solution)/shard_map/pallas_call | solution.py:32
  95.6 0.0 collective-permute-done.1.other
  95.6 0.0 all-to-all-done.1.arrived
  95.6 0.0 copy-done
  95.6 0.0 copy-start.5
  95.6 1.0 copy-done.5
  96.6 0.7 shard_map.151
  97.3 16.5 %all_to_all.15.arrived = bf16[8,16,3200]{2,1,0:T(8,128)(2,1)S(1)} all-to-all(bf16[8,16,3200]{2,1,0:T(8,128)(2,1)S(1)} %shard_map.151), channel_id=1, replica_groups=mesh['sp'=128,'tp'=8] {'tp'}, dimensions={0} | all-to-all | bytes 1638400 | tf_op jit(solution)/shard_map/all_to_all | solution.py:310
  113.9 0.8 shard_map.152
Async XLA Ops:
  17.6 42.2 %all-to-all-start = ((bf16[128,8,128]{2,1,0:T(8,128)(2,1)}), bf16[128,8,128]{2,1,0:T(8,128)(2,1)S(1)}, u32[]{:S(2)}, u32[]{:S(2)}) async-start(bf16[128,8,128]{2,1,0:T(8,128)(2,1)} %get-tuple-element.26), calls=%async_computation | async-start | bytes 524288 | tf_op jit(solution)/shard_map/all_to_all | solution.py:310
  59.8 19.3 %copy-start.1 = (bf16[2048,128]{1,0:T(8,128)(2,1)S(1)}, bf16[2048,128]{1,0:T(8,128)(2,1)}, u32[]{:S(2)}) copy-start(bf16[2048,128]{1,0:T(8,128)(2,1)} %bw.1) | copy-start | bytes 1572868
  59.8 19.3 %copy-start.2 = (bf16[2048,128]{1,0:T(8,128)(2,1)S(1)}, bf16[2048,128]{1,0:T(8,128)(2,1)}, u32[]{:S(2)}) copy-start(bf16[2048,128]{1,0:T(8,128)(2,1)} %cw.1) | copy-start | bytes 1572868
  59.8 19.3 %copy-start.3 = (bf16[2048,128]{1,0:T(8,128)(2,1)S(1)}, bf16[2048,128]{1,0:T(8,128)(2,1)}, u32[]{:S(2)}) copy-start(bf16[2048,128]{1,0:T(8,128)(2,1)} %uw.1) | copy-start | bytes 1572868
  62.0 33.6 %all-to-all-start.1 = ((bf16[128,4,128]{2,1,0:T(4,128)(2,1)}), bf16[128,4,128]{2,1,0:T(4,128)(2,1)S(1)}, u32[]{:S(2)}, u32[]{:S(2)}) async-start(bf16[128,4,128]{2,1,0:T(4,128)(2,1)} %get-tuple-element.27), calls=%async_computation.1 | async-start | bytes 262144 | tf_op jit(solution)/shard_map/all_to_all | solution.py:310
  79.1 7.4 %copy-start.4 = (bf16[128,2048]{1,0:T(8,128)(2,1)S(1)}, bf16[128,2048]{1,0:T(8,128)(2,1)}, u32[]{:S(2)}) copy-start(bf16[128,2048]{1,0:T(8,128)(2,1)} %weight.2) | copy-start | bytes 1572868
  79.7 6.8 %collective-permute-start = (bf16[16,128]{1,0:T(8,128)(2,1)S(1)}, bf16[16,128]{1,0:T(8,128)(2,1)S(1)}, u32[]{:S(2)}, u32[]{:S(2)}) collective-permute-start(bf16[16,128]{1,0:T(8,128)(2,1)S(1)} %get-tuple-element.31), channel_id=1, source_target_pairs={{0,8},{8,16},{16,24},{24,32},{32,40},{40,48},{48,56},{56,64},{64,7... | collective-permute-start | bytes 12296 | tf_op jit(solution)/shard_map/ppermute | solution.py:342
  86.8 8.8 %collective-permute-start.1 = (bf16[128,1024]{1,0:T(8,128)(2,1)S(1)}, bf16[128,1024]{1,0:T(8,128)(2,1)S(1)}, u32[]{:S(2)}, u32[]{:S(2)}) collective-permute-start(bf16[128,1024]{1,0:T(8,128)(2,1)S(1)} %get-tuple-element.36), channel_id=1, source_target_pairs={{0,1},{1,0},{2,3},{3,2},{4,5},{5,4},{6,7},{7,6},{8,9},{9,8},{10,11... | collective-permute-start | bytes 786440 | tf_op jit(solution)/shard_map/ppermute | solution.py:353
  91.7 3.9 %copy-start = (bf16[256,2048]{1,0:T(8,128)(2,1)S(1)}, bf16[256,2048]{1,0:T(8,128)(2,1)}, u32[]{:S(2)}) copy-start(bf16[256,2048]{1,0:T(8,128)(2,1)} %weight.3) | copy-start | bytes 3145732
  95.6 1.0 copy-start.5

commit v9 on v8

--- a/solution.py
+++ b/solution.py
@@ -12,7 +12,8 @@
 MDIM = 2048
 EPS = 1e-06
 OWN = 56
-FIRST = 84
+FIRST = 76
+TP_FIRST = 6
 CHUNKS = 4
 LOWEST = -1e30
 TP = "tp"
@@ -77,12 +78,13 @@
     return copies
 
 
-def prepare(tok_hbm, gain_hbm, *rest):
-    count = (len(rest) - 4) // 2
-    sources, out, places, (tok, gain, sems) = rest[:count], rest[count], rest[count + 1 : -3], rest[-3:]
-    copies = fetched([(tok_hbm, tok), (gain_hbm, gain), *zip(sources, places)], sems)
-    copies[0].wait()
-    copies[1].wait()
+def prepare(tok_hbm, gain_hbm, gw_hbm, bias_hbm, taps_hbm, kw_hbm, vw_hbm,
+            out, gw, bias, taps, kw, vw, tok, gain, first, sems):
+    mine = fetched([(tok_hbm, tok), (gain_hbm, gain)], first)
+    small = [(gw_hbm, gw), (bias_hbm, bias), (taps_hbm, taps)]
+    others = fetched(small + cuts((kw_hbm, vw_hbm), (kw, vw)), sems)
+    for c in mine:
+        c.wait()
     wide = tok[...].astype(F32)
     out[0, :N, :] = (wide * gain[...].astype(F32)).astype(BF)
     squares = to_row(jnp.sum(wide * wide, axis=1, keepdims=True))
@@ -91,7 +93,7 @@
     tail = jnp.concatenate([hi.astype(F32), mid.astype(F32), low.astype(F32), zero], axis=0)
     out[0, N:, :N] = tail.astype(BF)
     out[0, N:, N:] = jnp.zeros((16, N), BF)
-    for c in copies[2:]:
+    for c in others:
         c.wait()
 
 
@@ -280,9 +282,10 @@
     conv = (keep[...].astype(F32) + other[...].astype(F32)).astype(BF)
     for g in range(groups):
         at = slice(g * size, (g + 1) * size)
-        out[g, :, :width] = done[at]
-        out[g, :, width : width + width // 2] = conv[at]
-        out[g, :, width + width // 2 :] = tail[at]
+        to = (g - TP_FIRST) % groups
+        out[to, :, :width] = done[at]
+        out[to, :, width : width + width // 2] = conv[at]
+        out[to, :, width + width // 2 :] = tail[at]
 
 
 def gather_up(arrived, out):
@@ -299,7 +302,7 @@
         c = jnp.zeros((size, half), F32)
         for g in range(groups):
             m += arrived[g, :, at].astype(F32)
-        for g in range(side, groups, 2):
+        for g in range((side - TP_FIRST) % 2, groups, 2):
             c += arrived[g, :, 2 * half : 3 * half].astype(F32)
         out[:, at] = (c + scale * m).astype(BF)
 
@@ -325,7 +328,8 @@
     local, gate_wt, biases, taps, key_v, value_v = call(
         prepare,
         [((1, N + 16, tokens.shape[1]), BF, V)] + [(a.shape, a.dtype, V) for a in small],
-        tokens, norm_gain, *small, places=[H] * 7, scratch=room(tokens, norm_gain) + sems(7),
+        tokens, norm_gain, *small, places=[H] * 7,
+        scratch=room(tokens, norm_gain) + sems(2, 3 + 2 * CHUNKS),
     )
     tok = lax.all_gather(local, TP, axis=0, tiled=True)
     message, kv, aux = call(
@@ -363,7 +367,7 @@
         finish, [((groups, N // groups, 3 * model // 2 + N), BF, V)], state, own, pack, keep, other, mem_out_w,
         flops=10**9, scratch=[pltpu.VMEM((count, rows, N), F32)], places=[V] * 6, limit=16,
     )
-    mem = exchange(mem, TP)
+    mem = exchange(mem, TP, TP_FIRST)
     (out,) = call(gather_up, [((N // groups, model), BF, A)], mem, places=[V], limit=16)
     return out
 

time: 115 us -> 115 us (level)
  starting transfers between devices: 53.8 us -> 55.6 us
    all_to_all x2, starting transfers between devices: 46.7 us -> 48.4 us  [exchange(): lax.all_to_all(value, axis, split_axis=0, concat_axis=0, tiled=True, axis...]
where the time goes in v9:
time: 115 us
  starting transfers between devices  55.6 us (48%)
  blocking collectives  30 us (26%)
  waiting for transfers between devices  16.1 us (14%)
  Pallas kernels  11.9 us (10%)
    all_to_all x2, starting transfers between devices, exchange(): lax.all_to_all(value, axis, split_axis=0, concat_axis=0, tiled=True, axis...  48.4 us
    all_to_all x1, blocking collectives, exchange(): lax.all_to_all(value, axis, split_axis=0, concat_axis=0, tiled=True, axis...  16 us
    all_gather x1, blocking collectives, body(): tok = lax.all_gather(local, TP, axis=0, tiled=True)  14 us
    pallas_call x8, Pallas kernels, call(): pl.pallas_call(kernel, out_shape=outs, in_specs=[pl.BlockSpec(memory_spac...  11.9 us
    all_to_all x2, waiting for transfers between devices, exchange(): lax.all_to_all(value, axis, split_axis=0, concat_axis=0, tiled=True, axis...  11.8 us
    ppermute x1, starting transfers between devices, body(): other = lax.ppermute(send, TP, [(i, i ^ 1) for i in range(groups)])  5.03 us
    ppermute x1, waiting for transfers between devices, body(): halo = lax.ppermute(edge, SP, [(i, i + 1) for i in range(count - 1)])  4.25 us
  transfers between devices with their start and end apart: 4, of which 2 were waited for; matrix products, arithmetic and copies ran while one was open for 0% of the time, Pallas kernels for 4%

profile of v9, /device:TPU:65, one launch (start us, length us, event | category | flops | bytes accessed | tf_op | source)
XLA Modules:
  0.0 114.8 jit_solution(15136311580403713362)
XLA Ops:
  0.0 1.7 %shard_map.145 = (bf16[1,144,256]{2,1,0:T(8,128)(2,1)S(1)}, bf16[2,2048]{1,0:T(2,128)(2,1)S(1)}, f32[1,2]{1,0:T(1,128)S(1)}, bf16[3,128]{1,0:T(4,128)(2,1)S(1)},...) custom-call(bf16[128,256]{1,0:T(8,128)(2,1)} %tok_hbm.1, bf16[1,256]{1,0:T(2,128)(2,1)} %gain_hbm.1, ...), custom_call_target="tpu_custom_call" | custom-call | tf_op jit(solution)/shard_map/pallas_call | solution.py:33
  1.7 14.0 %all_gather.3.tok = bf16[8,144,256]{2,1,0:T(8,128)(2,1)S(1)} all-gather(bf16[1,144,256]{2,1,0:T(8,128)(2,1)S(1)} %get-tuple-element.21), channel_id=1, replica_groups=mesh['sp'=128,'tp'=8] {'tp'}, dimensions={0}, use_global_device_ids=true | all-gather | bytes 663552 | tf_op jit(solution)/shard_map/all_gather | solution.py:334
  15.7 1.8 %shard_map.146 = (bf16[128,8,128]{2,1,0:T(8,128)(2,1)}, bf16[128,512]{1,0:T(8,128)(2,1)}, f32[8,128]{1,0:T(8,128)S(1)}) custom-call(bf16[8,144,256]{2,1,0:T(8,128)(2,1)S(1)} %all_gather.3.tok, bf16[2,2048]{1,0:T(2,128)(2,1)S(1)} %get-tuple-element.22.gw, f32[1,2]{1,0:T(1,128)S(1)} %get-tuple-element.23.bias, bf16[2048,256]{1,0:T(8,128)(2,1)S(1)} %get-tuple-element.24.kw, ...), custom_call_target="tpu_custom_call" | custom-call | flops 1000000000 | bytes 1000000 | tf_op jit(solution)/shard_map/pallas_call | solution.py:33
  17.5 30.5 %all-to-all-start = ((bf16[128,8,128]{2,1,0:T(8,128)(2,1)}), bf16[128,8,128]{2,1,0:T(8,128)(2,1)S(1)}, u32[]{:S(2)}, u32[]{:S(2)}) async-start(bf16[128,8,128]{2,1,0:T(8,128)(2,1)} %get-tuple-element.26), calls=%async_computation | async-start | bytes 524288 | tf_op jit(solution)/shard_map/all_to_all | solution.py:313
  48.1 11.8 %all-to-all-done.arrived = bf16[128,8,128]{2,1,0:T(8,128)(2,1)S(1)} async-done(((bf16[128,8,128]{2,1,0:T(8,128)(2,1)}), bf16[128,8,128]{2,1,0:T(8,128)(2,1)S(1)}, u32[]{:S(2)}, u32[]{:S(2)}) %all-to-all-start) | async-done | bytes 262176 | tf_op jit(solution)/shard_map/all_to_all | solution.py:313
  59.9 0.0 copy-start.1
  59.9 0.0 copy-start.2
  59.9 0.0 copy-start.3
  59.9 2.2 %shard_map.147 = (bf16[128,4,128]{2,1,0:T(4,128)(2,1)}, f32[8,128]{1,0:T(8,128)S(1)}) custom-call(s32[1]{0:T(128)} %bitcast.place, bf16[128,8,128]{2,1,0:T(8,128)(2,1)S(1)} %all-to-all-done.arrived), custom_call_target="tpu_custom_call" | custom-call | flops 1000000000 | bytes 1000000 | tf_op jit(solution)/shard_map/pallas_call | solution.py:33
  62.1 17.9 %all-to-all-start.1 = ((bf16[128,4,128]{2,1,0:T(4,128)(2,1)}), bf16[128,4,128]{2,1,0:T(4,128)(2,1)S(1)}, u32[]{:S(2)}, u32[]{:S(2)}) async-start(bf16[128,4,128]{2,1,0:T(4,128)(2,1)} %get-tuple-element.27), calls=%async_computation.1 | async-start | bytes 262144 | tf_op jit(solution)/shard_map/all_to_all | solution.py:313
  80.0 0.0 copy-done.1
  80.0 0.0 copy-done.2
  80.0 0.0 copy-done.3
  80.0 0.0 copy-start.4
  80.0 0.6 shard_map.149
  80.6 2.2 %collective-permute-start = (bf16[16,128]{1,0:T(8,128)(2,1)S(1)}, bf16[16,128]{1,0:T(8,128)(2,1)S(1)}, u32[]{:S(2)}, u32[]{:S(2)}) collective-permute-start(bf16[16,128]{1,0:T(8,128)(2,1)S(1)} %get-tuple-element.31), channel_id=1, source_target_pairs={{0,8},{8,16},{16,24},{24,32},{32,40},{40,48},{48,56},{56,64},{64,7... | collective-permute-start | bytes 12296 | tf_op jit(solution)/shard_map/ppermute | solution.py:346
  82.8 4.3 %collective-permute-done.halo = bf16[16,128]{1,0:T(8,128)(2,1)S(1)} collective-permute-done((bf16[16,128]{1,0:T(8,128)(2,1)S(1)}, bf16[16,128]{1,0:T(8,128)(2,1)S(1)}, u32[]{:S(2)}, u32[]{:S(2)}) %collective-permute-start) | collective-permute-done | bytes 4128 | tf_op jit(solution)/shard_map/ppermute | solution.py:346
  87.1 0.0 copy-done.4
  87.1 0.3 shard_map.150
  87.4 5.0 %collective-permute-start.1 = (bf16[128,1024]{1,0:T(8,128)(2,1)S(1)}, bf16[128,1024]{1,0:T(8,128)(2,1)S(1)}, u32[]{:S(2)}, u32[]{:S(2)}) collective-permute-start(bf16[128,1024]{1,0:T(8,128)(2,1)S(1)} %get-tuple-element.36), channel_id=1, source_target_pairs={{0,1},{1,0},{2,3},{3,2},{4,5},{5,4},{6,7},{7,6},{8,9},{9,8},{10,11... | collective-permute-start | bytes 786440 | tf_op jit(solution)/shard_map/ppermute | solution.py:357
  92.4 0.0 copy-start
  92.4 3.8 %shard_map.148.pack = f32[128,896]{1,0:T(8,128)} custom-call(bf16[8,144,256]{2,1,0:T(8,128)(2,1)S(1)} %all_gather.3.tok, f32[8,128]{1,0:T(8,128)S(1)} %get-tuple-element.29.aux, bf16[128,512]{1,0:T(8,128)(2,1)} %get-tuple-element.30.kv, bf16[2048,256]{1,0:T(8,128)(2,1)} %qw_hbm.1, bf16[2048,256]{1,0:T(8,128)(2,1)} %ow_hbm.1, bf16[256]{0:T(256)(128)(2,1)} %gain.1), custom_call_target="tpu_custom_call" | custom-call | flops 1000000000 | bytes 1000000 | tf_op jit(solution)/shard_map/pallas_call | solution.py:33
  96.3 0.0 collective-permute-done.1.other
  96.3 0.0 all-to-all-done.1.arrived
  96.3 0.0 copy-done
  96.3 0.0 copy-start.5
  96.3 1.0 copy-done.5
  97.3 0.7 shard_map.151
  98.0 16.0 %all_to_all.15.arrived = bf16[8,16,3200]{2,1,0:T(8,128)(2,1)S(1)} all-to-all(bf16[8,16,3200]{2,1,0:T(8,128)(2,1)S(1)} %shard_map.151), channel_id=1, replica_groups={{6,7,0,1,2,3,4,5},{14,15,8,9,10,11,12,13},{22,23,16,17,18,19,20,21},{30..., dimensions={0} | all-to-all | bytes 1638400 | tf_op jit(solution)/shard_map/all_to_all | solution.py:313
  114.0 0.8 shard_map.152
Async XLA Ops:
  17.5 42.4 %all-to-all-start = ((bf16[128,8,128]{2,1,0:T(8,128)(2,1)}), bf16[128,8,128]{2,1,0:T(8,128)(2,1)S(1)}, u32[]{:S(2)}, u32[]{:S(2)}) async-start(bf16[128,8,128]{2,1,0:T(8,128)(2,1)} %get-tuple-element.26), calls=%async_computation | async-start | bytes 524288 | tf_op jit(solution)/shard_map/all_to_all | solution.py:313
  59.9 20.1 %copy-start.1 = (bf16[2048,128]{1,0:T(8,128)(2,1)S(1)}, bf16[2048,128]{1,0:T(8,128)(2,1)}, u32[]{:S(2)}) copy-start(bf16[2048,128]{1,0:T(8,128)(2,1)} %bw.1) | copy-start | bytes 1572868
  59.9 20.1 %copy-start.2 = (bf16[2048,128]{1,0:T(8,128)(2,1)S(1)}, bf16[2048,128]{1,0:T(8,128)(2,1)}, u32[]{:S(2)}) copy-start(bf16[2048,128]{1,0:T(8,128)(2,1)} %cw.1) | copy-start | bytes 1572868
  59.9 20.1 %copy-start.3 = (bf16[2048,128]{1,0:T(8,128)(2,1)S(1)}, bf16[2048,128]{1,0:T(8,128)(2,1)}, u32[]{:S(2)}) copy-start(bf16[2048,128]{1,0:T(8,128)(2,1)} %uw.1) | copy-start | bytes 1572868
  62.1 34.2 %all-to-all-start.1 = ((bf16[128,4,128]{2,1,0:T(4,128)(2,1)}), bf16[128,4,128]{2,1,0:T(4,128)(2,1)S(1)}, u32[]{:S(2)}, u32[]{:S(2)}) async-start(bf16[128,4,128]{2,1,0:T(4,128)(2,1)} %get-tuple-element.27), calls=%async_computation.1 | async-start | bytes 262144 | tf_op jit(solution)/shard_map/all_to_all | solution.py:313
  80.0 7.1 %copy-start.4 = (bf16[128,2048]{1,0:T(8,128)(2,1)S(1)}, bf16[128,2048]{1,0:T(8,128)(2,1)}, u32[]{:S(2)}) copy-start(bf16[128,2048]{1,0:T(8,128)(2,1)} %weight.2) | copy-start | bytes 1572868
  80.6 6.5 %collective-permute-start = (bf16[16,128]{1,0:T(8,128)(2,1)S(1)}, bf16[16,128]{1,0:T(8,128)(2,1)S(1)}, u32[]{:S(2)}, u32[]{:S(2)}) collective-permute-start(bf16[16,128]{1,0:T(8,128)(2,1)S(1)} %get-tuple-element.31), channel_id=1, source_target_pairs={{0,8},{8,16},{16,24},{24,32},{32,40},{40,48},{48,56},{56,64},{64,7... | collective-permute-start | bytes 12296 | tf_op jit(solution)/shard_map/ppermute | solution.py:346
  87.4 8.9 %collective-permute-start.1 = (bf16[128,1024]{1,0:T(8,128)(2,1)S(1)}, bf16[128,1024]{1,0:T(8,128)(2,1)S(1)}, u32[]{:S(2)}, u32[]{:S(2)}) collective-permute-start(bf16[128,1024]{1,0:T(8,128)(2,1)S(1)} %get-tuple-element.36), channel_id=1, source_target_pairs={{0,1},{1,0},{2,3},{3,2},{4,5},{5,4},{6,7},{7,6},{8,9},{9,8},{10,11... | collective-permute-start | bytes 786440 | tf_op jit(solution)/shard_map/ppermute | solution.py:357
  92.4 3.9 %copy-start = (bf16[256,2048]{1,0:T(8,128)(2,1)S(1)}, bf16[256,2048]{1,0:T(8,128)(2,1)}, u32[]{:S(2)}) copy-start(bf16[256,2048]{1,0:T(8,128)(2,1)} %weight.3) | copy-start | bytes 3145732
  96.3 1.0 copy-start.5
